TPU v7x, 512 devices: a whole 4x8x8 slice. The times are simulated.
512 devices in a mesh: sp: 64 (over z, y), tp: 4 (over x), dp: 2 (over core).
Axes of the slice: x: 4, y: 8, z: 8, core: 2. Of those that a mesh axis runs over, the one named last changes fastest.
Arguments:
- latent: bfloat16 [2, 8192, 2048], P('dp', ('sp', 'tp')), may hold values from -10 to 10
- condition: bfloat16 [2, 2048], P('dp'), may hold values from -6 to 6
- context: bfloat16 [2, 512, 2048], P('dp', 'sp'), may hold values from -6 to 6
- context_source: bfloat16 [2048], replicated, may hold values from -6 to 6
- mod_weight: bfloat16 [3, 2048, 2048], P(None, 'sp', 'tp'), may hold values from -0.125 to 0.125
- norm_gain: bfloat16 [2048], replicated, may hold values from 0.099609375 to 1.8984375
- w_x: bfloat16 [2048, 2048], P('dp', 'tp'), may hold values from -0.125 to 0.125
- w_b: bfloat16 [2048, 512], P('dp', 'tp'), may hold values from -0.125 to 0.125
- w_c: bfloat16 [2048, 512], P('dp', 'tp'), may hold values from -0.125 to 0.125
- w_z: bfloat16 [2048, 2048], P('dp', 'tp'), may hold values from -0.125 to 0.125
- w_dt: bfloat16 [2, 2048, 32], P(None, 'dp', 'tp'), may hold values from -0.125 to 0.125
- conv_x: bfloat16 [3, 2048], P(None, 'tp'), may hold values from -3.5 to 3.5
- conv_b: bfloat16 [3, 512], P(None, 'tp'), may hold values from -3.5 to 3.5
- conv_c: bfloat16 [3, 512], P(None, 'tp'), may hold values from -3.5 to 3.5
- decay_rate: float32 [2, 32], P(None, 'tp'), may hold values from 0 to 1, as said below
- out_gain: bfloat16 [2048], P('tp'), may hold values from 0.099609375 to 1.8984375
- w_out: bfloat16 [2048, 2048], P(('tp', 'dp')), may hold values from -0.125 to 0.125
Outputs:
- update: bfloat16 [2, 8192, 2048], P('dp', ('sp', 'tp'))
Inputs may be any that keep to these rules, and one draw needn't show every extreme that they name: `decay_rate`: positive rates.
All inputs are finite; a program needn't handle non-finite values.
Results may differ from a plain program's by a relative error of at most 0.014.
Values may be sent and summed in bfloat16 or wider, within the bound.
A program may use at most 128 MiB of HBM per device.

v0:
```python
import functools

import jax
import jax.numpy as jnp
from jax import lax
from jax.sharding import Mesh
from jax.sharding import PartitionSpec as P

STATE = 128
BLOCK = 128
SP = ("sp_0", "sp_1")
SP_TP = ("sp_0", "sp_1", "tp")


EPSILON = 1e-06


def over_axes(x, axes):
    return functools.reduce(lax.psum, axes, x)


def laid_out(tiles, dim):
    tiles = jnp.moveaxis(tiles, 0, dim)
    dims = tiles.shape
    return tiles.reshape(*dims[:dim], dims[dim] * dims[dim + 1], *dims[dim + 2 :])


def sent_to_all(x, axis):
    peers = lax.axis_size(axis)
    return lax.all_to_all(jnp.broadcast_to(x[None], (peers, *x.shape)), axis, 0, 0, tiled=True)


def gather_directly(x, axis, dim):
    return laid_out(sent_to_all(x, axis), dim)


def sent_together(arrays, axis, dim, along):
    ends, at = ([], 0)
    for a in arrays[:-1]:
        at += a.shape[along]
        ends.append(at)
    both = jnp.concatenate(arrays, axis=along)
    return tuple(jnp.split(lax.all_gather(both, axis, axis=dim, tiled=True), ends, axis=along))


def with_halo(x, sides, width):
    for axis, dim in sides:
        peers, length = (lax.axis_size(axis), x.shape[dim])
        up = [(i, (i + 1) % peers) for i in range(peers - 1)]
        down = [(j, i) for i, j in up]
        last = lax.slice_in_dim(x, length - width, length, axis=dim)
        leading = lax.slice_in_dim(x, 0, width, axis=dim)
        before = lax.ppermute(last, axis, up)
        after = lax.ppermute(leading, axis, down)
        x = jnp.concatenate([before, x, after], axis=dim)
    return x


def neutral_like(x, identity):
    return jax.tree.map(
        lambda a, e: jnp.broadcast_to(jnp.asarray(e, a.dtype), a.shape), x, identity
    )


def entering_2(x, axes, combine, identity, reverse):
    before = start = neutral_like(x, identity)
    total = x
    for axis in reversed(axes):
        peers, place = (lax.axis_size(axis), lax.axis_index(axis))
        pieces = jax.tree.map(
            lambda part, kind: lax.all_gather(part.astype(kind), axis),
            total,
            (jnp.bfloat16, jnp.bfloat16),
        )
        inside, total = (start, start)
        for k in reversed(range(peers)) if reverse else range(peers):
            passed = k > place if reverse else k < place
            total = combine(
                total, jax.tree.map(lambda part, own: part[k].astype(own.dtype), pieces, x)
            )
            inside = jax.tree.map(lambda new, old: jnp.where(passed, new, old), total, inside)
        before = combine(inside, before)
    return before


def split_up(x, dim, peers):
    before, after = (x.shape[:dim], x.shape[dim + 1 :])
    return jnp.moveaxis(x.reshape(*before, peers, -1, *after), dim, 0)


def sum_at_owner(x, axis, dim):
    peers = lax.axis_size(axis)
    tiles = lax.all_to_all(split_up(x, dim, peers), axis, 0, 0, tiled=True)
    return jnp.sum(tiles.astype(jnp.float32), axis=0)


def rounded(values):
    return lax.optimization_barrier(values.astype(jnp.bfloat16)).astype(jnp.float32)


def modulated(source, gain_vec, shift_vec, scale_vec):
    values = source.astype(jnp.float32)
    normed = values * lax.rsqrt(jnp.mean(values * values, axis=-1, keepdims=True) + EPSILON)
    return (normed * gain_vec.astype(jnp.float32) * (1.0 + scale_vec) + shift_vec).astype(
        jnp.bfloat16
    )


def convolved(padded, weight, total_rows):
    wide_vals = padded.astype(jnp.float32)
    tap_weights = weight.astype(jnp.float32)
    summed = jnp.zeros((total_rows, wide_vals.shape[1]), jnp.float32)
    for offset in range(weight.shape[0]):
        summed = summed + wide_vals[offset : offset + total_rows] * tap_weights[offset]
    return jax.nn.silu(summed).astype(jnp.bfloat16)


def final_state(x_vals, b_vals, step_size, rate_head, groups):
    total_rows, head_count = step_size.shape
    per_group = head_count // groups
    moved_x = rounded(
        x_vals.reshape(total_rows, head_count, -1).astype(jnp.float32) * step_size[:, :, None]
    )
    running = jnp.cumsum(-rate_head * step_size, axis=0)
    weight = jnp.exp(running[-1:] - running)
    scaled = (moved_x * weight[:, :, None]).reshape(total_rows, groups, per_group, -1)
    b_wide = b_vals.reshape(total_rows, groups, -1).astype(jnp.float32)
    ctx_state = jnp.einsum("sgn,sghp->ghpn", b_wide, scaled)
    return (ctx_state, running[-1].reshape(groups, per_group))


def combine_states(earlier, later_part):
    return (
        earlier[0] + later_part[0],
        earlier[1] * jnp.exp(later_part[0])[:, :, None, None] + later_part[1],
    )


def direction_terms(x_vals, b_vals, c_vals, step_size, rate_head, groups):
    total_rows, head_count = step_size.shape
    per_group = head_count // groups
    blocks = total_rows // BLOCK
    moved_x = (
        x_vals.reshape(total_rows, head_count, -1).astype(jnp.float32) * step_size[:, :, None]
    ).astype(jnp.bfloat16)
    head_dim = moved_x.shape[2]
    x_blocks = moved_x.reshape(blocks, BLOCK, groups, per_group, head_dim)
    b_blocks = b_vals.reshape(blocks, BLOCK, groups, -1)
    c_blocks = c_vals.reshape(blocks, BLOCK, groups, -1)
    running = jnp.cumsum((-rate_head * step_size).reshape(blocks, BLOCK, head_count), axis=1)
    across = jnp.swapaxes(running, 1, 2)
    spread = across[:, :, :, None] - across[:, :, None, :]
    lower_part = lax.broadcasted_iota(jnp.int32, (BLOCK, BLOCK), 0) >= lax.broadcasted_iota(
        jnp.int32, (BLOCK, BLOCK), 1
    )
    decay_mask = jnp.where(lower_part, jnp.exp(jnp.minimum(spread, 0.0)), 0.0).reshape(
        blocks, groups, per_group, BLOCK, BLOCK
    )
    scores = jnp.einsum("clgn,csgn->cgls", c_blocks, b_blocks, preferred_element_type=jnp.float32)
    weights = (scores[:, :, None] * decay_mask).astype(jnp.bfloat16)
    inside = jnp.einsum("cghls,csghp->clghp", weights, x_blocks, preferred_element_type=jnp.float32)
    to_end = jnp.exp(running[:, -1:, :] - running).reshape(blocks, BLOCK, groups, per_group, 1)
    x_end = (x_blocks.astype(jnp.float32) * to_end).astype(jnp.bfloat16)
    fresh_state = jnp.einsum(
        "csgn,csghp->cghpn", b_blocks, x_end, preferred_element_type=jnp.float32
    )
    totals = running[:, -1, :].reshape(blocks, groups, per_group)

    def advance(carried_in, inputs):
        return (carried_in * jnp.exp(inputs[1])[:, :, None, None] + inputs[0], carried_in)

    ending, before = lax.scan(
        advance, jnp.zeros(fresh_state.shape[1:], jnp.float32), (fresh_state, totals)
    )
    return (inside, before, ending, totals, running, c_blocks)


def direction_output(terms, incoming):
    inside, before, ending, totals, running, c_blocks = terms
    blocks, length, groups, per_group, head_dim = inside.shape
    offset_sum = jnp.cumsum(totals, axis=0) - totals
    entering = before + jnp.exp(offset_sum)[:, :, :, None, None] * incoming[None]
    carried = jnp.einsum(
        "clgn,cghpn->clghp",
        c_blocks,
        entering.astype(jnp.bfloat16),
        preferred_element_type=jnp.float32,
    )
    growth = jnp.exp(running).reshape(blocks, length, groups, per_group, 1)
    return (inside + growth * carried).reshape(blocks * length, -1)


def shards(
    latent,
    condition,
    context,
    context_source,
    mod_weight,
    norm_gain,
    w_x,
    w_b,
    w_c,
    w_z,
    w_dt,
    conv_x,
    conv_b,
    conv_c,
    decay_rate,
    out_gain,
    w_out,
):
    row_count = mod_weight.shape[1]
    activations = jnp.stack(
        [
            jax.nn.silu(condition[0].astype(jnp.float32)),
            jax.nn.silu(context_source.astype(jnp.float32)),
        ]
    ).astype(jnp.bfloat16)
    own_rows = lax.dynamic_slice_in_dim(activations, lax.axis_index(SP) * row_count, row_count, 1)
    partial_value = jnp.einsum(
        "ar,krc->kac", own_rows, mod_weight, preferred_element_type=jnp.float32
    )
    summed = over_axes(partial_value, SP)
    mod_vectors = gather_directly(summed, "tp", 2)
    full_x, full_b, full_c, full_z, full_fwd, full_bwd, full_out = (
        *sent_together((w_x, w_b, w_c, w_z, w_dt[0], w_dt[1]), "dp", 0, 1),
        lax.all_gather(w_out, "dp", axis=0, tiled=True),
    )
    inner_cols = full_x.shape[1]
    gn_cols = full_b.shape[1]
    head_count = full_fwd.shape[1]
    groups = gn_cols // STATE
    mixed_cols = inner_cols + gn_cols
    reach_rows = conv_x.shape[0] // 2
    rate_fwd = decay_rate[0]
    rate_bwd = decay_rate[1]
    all_weights = jnp.concatenate([full_x, full_b, full_c, full_fwd, full_bwd, full_z], axis=1)
    ctx_weight = jnp.concatenate([full_x, full_b, full_fwd, full_bwd], axis=1)
    taps_all = jnp.concatenate([conv_x, conv_b, conv_c], axis=1)
    ctx_taps = jnp.concatenate([conv_x, conv_b], axis=1)
    ctx_rows = modulated(context[0], norm_gain, mod_vectors[0, 1], mod_vectors[1, 1])
    own_features = jnp.dot(ctx_rows, ctx_weight, preferred_element_type=jnp.float32).astype(
        jnp.bfloat16
    )
    features = gather_directly(own_features, SP, 0)
    total_rows = features.shape[0]
    padded = jnp.pad(features[:, :mixed_cols], ((reach_rows, reach_rows), (0, 0)))
    smoothed = convolved(padded, ctx_taps, total_rows)
    step_size = jax.nn.softplus(features[:, mixed_cols:].astype(jnp.float32))
    ctx_x = smoothed[:, :inner_cols]
    ctx_b = smoothed[:, inner_cols:]
    state_fwd, _ = final_state(ctx_x, ctx_b, step_size[:, :head_count], rate_fwd, groups)
    state_bwd, _ = final_state(
        jnp.flip(ctx_x, 0),
        jnp.flip(ctx_b, 0),
        jnp.flip(step_size[:, head_count:], 0),
        rate_bwd,
        groups,
    )
    latent_rows = modulated(latent[0], norm_gain, mod_vectors[0, 0], mod_vectors[1, 0])
    features = jnp.dot(
        gather_directly(latent_rows, "tp", 0), all_weights, preferred_element_type=jnp.float32
    ).astype(jnp.bfloat16)
    total_rows = features.shape[0]
    padded = with_halo(features[:, : mixed_cols + gn_cols], ((SP, 0),), reach_rows)
    smoothed = convolved(padded, taps_all, total_rows)
    x_vals = smoothed[:, :inner_cols]
    b_vals = smoothed[:, inner_cols:mixed_cols]
    c_vals = smoothed[:, mixed_cols:]
    base_col = mixed_cols + gn_cols
    step_size = jax.nn.softplus(
        features[:, base_col : base_col + 2 * head_count].astype(jnp.float32)
    )
    gate_in = features[:, base_col + 2 * head_count :]
    forward_terms = direction_terms(
        x_vals, b_vals, c_vals, step_size[:, :head_count], rate_fwd, groups
    )
    backward_terms = direction_terms(
        jnp.flip(x_vals, 0),
        jnp.flip(b_vals, 0),
        jnp.flip(c_vals, 0),
        jnp.flip(step_size[:, head_count:], 0),
        rate_bwd,
        groups,
    )
    fwd_total = jnp.sum(forward_terms[3], axis=0)
    bwd_total = jnp.sum(backward_terms[3], axis=0)
    empty = (jnp.zeros_like(fwd_total), jnp.zeros_like(forward_terms[2]))
    prefix_decay, prefix_state = entering_2(
        (fwd_total, forward_terms[2]), SP, combine_states, empty, False
    )
    suffix_decay, suffix_state = entering_2(
        (bwd_total, backward_terms[2]), SP, combine_states, empty, True
    )
    out_fwd = direction_output(
        forward_terms, prefix_state + jnp.exp(prefix_decay)[:, :, None, None] * state_fwd
    )
    out_bwd = jnp.flip(
        direction_output(
            backward_terms, suffix_state + jnp.exp(suffix_decay)[:, :, None, None] * state_bwd
        ),
        0,
    )
    gated = (out_fwd + out_bwd) * jax.nn.silu(gate_in.astype(jnp.float32))
    grouped = gated.reshape(total_rows, groups, -1)
    normed = (
        grouped
        * lax.rsqrt(jnp.mean(grouped * grouped, axis=-1, keepdims=True) + EPSILON)
        * out_gain.reshape(groups, -1).astype(jnp.float32)
    )
    normed_out = normed.reshape(total_rows, -1).astype(jnp.bfloat16)
    mixed = sum_at_owner(
        jnp.dot(normed_out, full_out, preferred_element_type=jnp.float32).astype(jnp.bfloat16),
        "tp",
        0,
    )
    return (mod_vectors[2, 0] * mixed).astype(jnp.bfloat16)[None]


def solution(mesh):
    torus = Mesh(
        mesh.devices.reshape(8, 8, mesh.shape["tp"], mesh.shape["dp"]), ("sp_0", "sp_1", "tp", "dp")
    )
    placed = (
        P("dp", SP_TP, None),
        P("dp", None),
        P("dp", SP, None),
        P(),
        P(None, SP, "tp"),
        P(),
        P("dp", "tp"),
        P("dp", "tp"),
        P("dp", "tp"),
        P("dp", "tp"),
        P(None, "dp", "tp"),
        P(None, "tp"),
        P(None, "tp"),
        P(None, "tp"),
        P(None, "tp"),
        P("tp"),
        P(("tp", "dp"), None),
    )
    return jax.shard_map(
        shards, mesh=torus, in_specs=placed, out_specs=P("dp", SP_TP, None), check_vma=False
    )
```

profile of v0, /device:TPU:6, one launch (start us, length us, event | category | flops | bytes accessed | tf_op | source)
XLA Modules:
  0.0 345.4 jit_solution(8498954441574411239)
XLA Ops:
  6.5 0.8 slice_bitcast_fusion.32
  7.7 5.4 %concatenate.20 = bf16[1024,1296]{1,0:T(8,128)(2,1)} concatenate(bf16[1024,512]{1,0:T(8,128)(2,1)} %param.23, bf16[1024,128]{1,0:T(8,128)(2,1)} %param.24, bf16[1024,128]{1,0:T(8,128)(2,1)} %param.25, bf16[1024,512]{1,0:T(8,128)(2,1)} %param.26, bf16[1024,8]{1,0:T(8,128)(2,1)S(1)} %copy.97, bf16[1024,8]{1,0:T(8,128)(2,1)S(1)} %copy.98), dimensions={1} | concatenate | bytes 5308416 | tf_op jit(solution)/shard_map/concatenate | solution.py:42
  14.0 35.9 %psum.14 = f32[3,2,512]{2,1,0:T(2,128)S(1)} all-reduce(f32[3,2,512]{2,1,0:T(2,128)S(1)} %convolution_bitcast_fusion.4), channel_id=1, replica_groups=mesh['sp_0'=8,'sp_1'=8,'tp'=4,'dp'=2] {'sp_0'}, use_global_device_ids=true, to_apply=%region_0.1 | all-reduce | flops 3072 | bytes 24576 | tf_op jit(solution)/shard_map/psum | solution.py:19
  50.0 30.3 %psum.15 = f32[3,2,512]{2,1,0:T(2,128)S(1)} all-reduce(f32[3,2,512]{2,1,0:T(2,128)S(1)} %psum.14), channel_id=1, replica_groups=mesh['sp_0'=8,'sp_1'=8,'tp'=4,'dp'=2] {'sp_1'}, use_global_device_ids=true, to_apply=%region_1.2 | all-reduce | flops 3072 | bytes 24576 | tf_op jit(solution)/shard_map/psum | solution.py:19
  80.9 4.8 %all-to-all-start = ((f32[4,3,2,512]{3,2,1,0:T(2,128)}), f32[4,3,2,512]{3,2,1,0:T(2,128)S(1)}, u32[]{:S(2)}, u32[]{:S(2)}) async-start(f32[4,3,2,512]{3,2,1,0:T(2,128)} %broadcast_in_dim.22), calls=%async_computation | async-start | bytes 98304 | tf_op jit(solution)/shard_map/all_to_all | solution.py:30
  85.9 3.3 all-to-all-done
  89.9 0.8 broadcast_in_dim.24
  90.8 6.2 %all-to-all-start.1 = ((bf16[4,32,2048]{2,1,0:T(8,128)(2,1)}), bf16[4,32,2048]{2,1,0:T(8,128)(2,1)}, u32[]{:S(2)}, u32[]{:S(2)}) async-start(bf16[4,32,2048]{2,1,0:T(8,128)(2,1)} %broadcast_in_dim.24), calls=%async_computation.1 | async-start | bytes 1048576 | tf_op jit(solution)/shard_map/all_to_all | solution.py:30
  97.1 1.9 split.19
  99.0 3.1 split.20
  102.0 2.1 split.18
  104.1 9.4 %concatenate.21 = bf16[2048,1296]{1,0:T(8,128)(2,1)} concatenate(bf16[2048,768]{1,0:T(8,128)(2,1)S(1)} %split.18, bf16[2048,16]{1,0:T(8,128)(2,1)} %split.19, bf16[2048,512]{1,0:T(8,128)(2,1)} %split.20), dimensions={1} | concatenate | bytes 10616832 | tf_op jit(solution)/shard_map/concatenate | solution.py:237
  113.5 5.1 %convolution_convert_fusion.1 = bf16[128,1296]{0,1:T(8,128)(2,1)S(1)} fusion(bf16[128,2048]{1,0:T(8,128)(2,1)} %bitcast.7, bf16[2048,1296]{1,0:T(8,128)(2,1)} %concatenate.21), kind=kOutput, calls=%fused_computation.5 | convolution fusion | flops 679643136 | bytes 6164480 | tf_op jit(solution)/shard_map/dot_general | solution.py:261
  120.0 1.5 collective-permute-start
  121.5 1.3 collective-permute-start.1
  123.4 1.2 collective-permute-done
  124.7 4.4 %collective-permute-done.1 = bf16[1,768]{0,1:T(8,128)(2,1)S(1)} collective-permute-done((bf16[1,768]{0,1:T(8,128)(2,1)S(1)}, bf16[1,768]{0,1:T(8,128)(2,1)S(1)}, u32[]{:S(2)}, u32[]{:S(2)}) %collective-permute-start.1) | collective-permute-done | bytes 1568 | tf_op jit(solution)/shard_map/ppermute | solution.py:54
  129.9 0.8 slice_convert_fusion.34
  131.2 0.8 fusion.15
  133.8 0.8 fusion.14
  134.7 17.0 %all_gather.48 = bf16[8,1,8]{2,1,0:T(2,128)(2,1)S(1)} all-gather(bf16[1,1,8]{2,1,0:T(2,128)(2,1)S(1)} %slice.999), channel_id=1, replica_groups=mesh['sp_0'=8,'sp_1'=8,'tp'=4,'dp'=2] {'sp_1'}, dimensions={0}, use_global_device_ids=true | all-gather | bytes 144 | tf_op jit(solution)/shard_map/all_gather | solution.py:71
  151.8 19.4 %all-gather.19.cloned.1.call-done = bf16[64,64,128]{2,1,0:T(8,128)(2,1)} async-done(((bf16[8,64,128]{2,1,0:T(8,128)(2,1)}), bf16[64,64,128]{2,1,0:T(8,128)(2,1)}) %all-gather.19.cloned.1.call-update) | async-done | bytes 1048592 | tf_op jit(solution)/shard_map/all_gather | solution.py:71
  171.2 2.3 fusion.159
  173.6 15.0 %all_gather.43 = bf16[8,1,8]{2,1,0:T(2,128)(2,1)S(1)} all-gather(bf16[1,1,8]{2,1,0:T(2,128)(2,1)S(1)} %slice.1000), channel_id=1, replica_groups=mesh['sp_0'=8,'sp_1'=8,'tp'=4,'dp'=2] {'sp_1'}, dimensions={0}, use_global_device_ids=true | all-gather | bytes 144 | tf_op jit(solution)/shard_map/all_gather | solution.py:71
  188.7 24.4 %all-gather.17.cloned.1.call-done = bf16[64,64,128]{2,1,0:T(8,128)(2,1)} async-done(((bf16[8,64,128]{2,1,0:T(8,128)(2,1)}), bf16[64,64,128]{2,1,0:T(8,128)(2,1)}) %all-gather.17.cloned.1.call-update) | async-done | bytes 1048592 | tf_op jit(solution)/shard_map/all_gather | solution.py:71
  213.0 2.2 fusion.160
  217.4 17.2 %all_gather.49 = bf16[8,1,8]{2,1,0:T(2,128)(2,1)S(1)} all-gather(bf16[1,1,8]{2,1,0:T(2,128)(2,1)S(1)} %get-tuple-element.103), channel_id=1, replica_groups=mesh['sp_0'=8,'sp_1'=8,'tp'=4,'dp'=2] {'sp_0'}, dimensions={0}, use_global_device_ids=true | all-gather | bytes 144 | tf_op jit(solution)/shard_map/all_gather | solution.py:71
  235.3 13.9 %all_gather.44 = bf16[8,1,8]{2,1,0:T(2,128)(2,1)S(1)} all-gather(bf16[1,1,8]{2,1,0:T(2,128)(2,1)S(1)} %get-tuple-element.83), channel_id=1, replica_groups=mesh['sp_0'=8,'sp_1'=8,'tp'=4,'dp'=2] {'sp_0'}, dimensions={0}, use_global_device_ids=true | all-gather | bytes 144 | tf_op jit(solution)/shard_map/all_gather | solution.py:71
  249.9 1.7 slice-done
  252.2 1.0 broadcast_in_dim.26
  253.2 8.6 %all-to-all-start.2 = ((bf16[64,8,656]{2,1,0:T(8,128)(2,1)}), bf16[64,8,656]{2,1,0:T(8,128)(2,1)S(1)}, u32[]{:S(2)}, u32[]{:S(2)}) async-start(bf16[64,8,656]{2,1,0:T(8,128)(2,1)} %broadcast_in_dim.26), calls=%async_computation.2 | async-start | bytes 1572864 | tf_op jit(solution)/shard_map/all_to_all | solution.py:30
  265.3 0.8 fusion.320
  266.1 0.8 fusion.332
  266.9 12.5 %all-to-all-done.2 = bf16[64,8,656]{2,1,0:T(8,128)(2,1)S(1)} async-done(((bf16[64,8,656]{2,1,0:T(8,128)(2,1)}), bf16[64,8,656]{2,1,0:T(8,128)(2,1)S(1)}, u32[]{:S(2)}, u32[]{:S(2)}) %all-to-all-start.2) | async-done | bytes 671776 | tf_op jit(solution)/shard_map/all_to_all | solution.py:30
  280.3 1.0 slice_convert_fusion.35
  282.0 1.1 reduce-window.14
  284.4 1.1 reduce-window.16
  286.4 1.3 rev.37
  288.0 1.7 multiply_convert_fusion.2
  289.8 6.3 %rev.35 = bf16[512,512]{1,0:T(8,128)(2,1)S(1)} reverse(bf16[512,512]{1,0:T(8,128)(2,1)} %get-tuple-element.48), dimensions={0} | reverse | bytes 1048576 | tf_op jit(solution)/shard_map/jit(_flip)/rev | solution.py:254
  297.3 3.3 fusion.13
  300.6 1.3 fusion.6
  302.3 2.1 all-gather.11.cloned.1.call-done
  304.6 2.6 fusion.12
  307.7 15.5 %all-gather.15.cloned.1.call-done = bf16[512,2048]{1,0:T(8,128)(2,1)} async-done(((bf16[256,2048]{1,0:T(8,128)(2,1)}), bf16[512,2048]{1,0:T(8,128)(2,1)}) %all-gather.15.cloned.1.call-update) | async-done | bytes 2097168 | tf_op jit(solution)/shard_map/all_gather | solution.py:227
  323.2 2.2 convolution_convert_fusion
  325.3 12.4 %all_to_all.20 = bf16[4,32,2048]{2,1,0:T(8,128)(2,1)S(1)} all-to-all(bf16[4,32,2048]{2,1,0:T(8,128)(2,1)S(1)} %bitcast.494), channel_id=1, replica_groups=mesh['sp_0'=8,'sp_1'=8,'tp'=4,'dp'=2] {'tp'}, dimensions={0} | all-to-all | bytes 1048576 | tf_op jit(solution)/shard_map/all_to_all | solution.py:93
  337.9 0.7 fusion.120
  (271 shorter events, 21.2 us)
Async XLA Ops:
  6.5 7.3 %copy-start = (bf16[3,32,512]{2,1,0:T(8,128)(2,1)S(1)}, bf16[3,32,512]{2,1,0:T(8,128)(2,1)}, u32[]{:S(2)}) copy-start(bf16[3,32,512]{2,1,0:T(8,128)(2,1)} %param.21) | copy-start | bytes 294916
  6.5 90.5 %all-gather.9.cloned.1.call-start = ((), (), s32[]{:S(2)}) async-start(), calls=%async_computation.4 | async-start | bytes 8650752 | tf_op jit(solution)/shard_map/all_gather | solution.py:43
  13.1 72.6 %copy-start.3 = (bf16[1,32,2048]{2,1,0:T(8,128)(2,1)S(1)}, bf16[1,32,2048]{2,1,0:T(8,128)(2,1)}, u32[]{:S(2)}) copy-start(bf16[1,32,2048]{2,1,0:T(8,128)(2,1)} %param.17) | copy-start | bytes 393220
  13.1 72.8 %copy-start.25 = (bf16[2048]{0:T(1024)(128)(2,1)S(1)}, bf16[2048]{0:T(1024)(128)(2,1)}, u32[]{:S(2)}) copy-start(bf16[2048]{0:T(1024)(128)(2,1)} %param.22) | copy-start | bytes 12292
  13.1 83.9 %copy-start.15 = (bf16[3,512]{1,0:T(4,128)(2,1)S(1)}, bf16[3,512]{1,0:T(4,128)(2,1)}, u32[]{:S(2)}) copy-start(bf16[3,512]{1,0:T(4,128)(2,1)} %param.28) | copy-start | bytes 9220
  13.1 83.9 %copy-start.30 = (bf16[3,128]{1,0:T(4,128)(2,1)S(1)}, bf16[3,128]{1,0:T(4,128)(2,1)}, u32[]{:S(2)}) copy-start(bf16[3,128]{1,0:T(4,128)(2,1)} %param.29) | copy-start | bytes 2308
  13.1 83.9 %copy-start.66 = (bf16[3,128]{1,0:T(4,128)(2,1)S(1)}, bf16[3,128]{1,0:T(4,128)(2,1)}, u32[]{:S(2)}) copy-start(bf16[3,128]{1,0:T(4,128)(2,1)} %param.30) | copy-start | bytes 2308
  13.1 83.9 %copy-start.68 = (f32[2,8]{1,0:T(2,128)S(1)}, f32[2,8]{1,0:T(2,128)}, u32[]{:S(2)}) copy-start(f32[2,8]{1,0:T(2,128)} %param.31) | copy-start | bytes 196
  80.9 8.2 %all-to-all-start = ((f32[4,3,2,512]{3,2,1,0:T(2,128)}), f32[4,3,2,512]{3,2,1,0:T(2,128)S(1)}, u32[]{:S(2)}, u32[]{:S(2)}) async-start(f32[4,3,2,512]{3,2,1,0:T(2,128)} %broadcast_in_dim.22), calls=%async_computation | async-start | bytes 98304 | tf_op jit(solution)/shard_map/all_to_all | solution.py:30
  90.8 22.8 %all-to-all-start.1 = ((bf16[4,32,2048]{2,1,0:T(8,128)(2,1)}), bf16[4,32,2048]{2,1,0:T(8,128)(2,1)}, u32[]{:S(2)}, u32[]{:S(2)}) async-start(bf16[4,32,2048]{2,1,0:T(8,128)(2,1)} %broadcast_in_dim.24), calls=%async_computation.1 | async-start | bytes 1048576 | tf_op jit(solution)/shard_map/all_to_all | solution.py:30
  96.9 74.2 %all-gather.19.cloned.1.call-start = ((), (), s32[]{:S(2)}) async-start(), calls=%async_computation.9 | async-start | bytes 1179648 | tf_op jit(solution)/shard_map/all_gather | solution.py:71
  97.0 21.7 %copy-start.23 = (f32[8]{0:T(128)}, f32[8]{0:T(128)S(1)}, u32[]{:S(2)}) copy-start(f32[8]{0:T(128)S(1)} %get-tuple-element.112) | copy-start | bytes 100
  97.0 21.8 %copy-start.21 = (f32[8]{0:T(128)}, f32[8]{0:T(128)S(1)}, u32[]{:S(2)}) copy-start(f32[8]{0:T(128)S(1)} %get-tuple-element.113) | copy-start | bytes 100
  118.8 14.9 %copy-start.12 = (f32[128,8]{0,1:T(8,128)}, f32[128,8]{0,1:T(8,128)S(1)}, u32[]{:S(2)}) copy-start(f32[128,8]{0,1:T(8,128)S(1)} %get-tuple-element.69) | copy-start | bytes 12292
  120.0 4.7 %collective-permute-start = (bf16[1,768]{0,1:T(8,128)(2,1)S(1)}, bf16[1,768]{0,1:T(8,128)(2,1)S(1)}, u32[]{:S(2)}, u32[]{:S(2)}) collective-permute-start(bf16[1,768]{0,1:T(8,128)(2,1)S(1)} %get-tuple-element.49), channel_id=1, source_target_pairs={{0,8},{8,16},{16,24},{24,32},{32,40},{40,48},{48,56},{56,64},{64,7... | collective-permute-start | bytes 4616 | tf_op jit(solution)/shard_map/ppermute | solution.py:53
  121.5 7.6 %collective-permute-start.1 = (bf16[1,768]{0,1:T(8,128)(2,1)S(1)}, bf16[1,768]{0,1:T(8,128)(2,1)S(1)}, u32[]{:S(2)}, u32[]{:S(2)}) collective-permute-start(bf16[1,768]{0,1:T(8,128)(2,1)S(1)} %get-tuple-element.50), channel_id=1, source_target_pairs={{8,0},{16,8},{24,16},{32,24},{40,32},{48,40},{56,48},{64,56},{72,6... | collective-permute-start | bytes 4616 | tf_op jit(solution)/shard_map/ppermute | solution.py:54
  132.1 80.9 %all-gather.17.cloned.1.call-start = ((), (), s32[]{:S(2)}) async-start(), calls=%async_computation.8 | async-start | bytes 1179648 | tf_op jit(solution)/shard_map/all_gather | solution.py:71
  133.7 82.3 %copy-start.16 = (bf16[3,512]{1,0:T(4,128)(2,1)S(1)}, bf16[3,512]{1,0:T(4,128)(2,1)}, u32[]{:S(2)}) copy-start(bf16[3,512]{1,0:T(4,128)(2,1)} %param.28) | copy-start | bytes 9220
  133.7 82.3 %copy-start.31 = (bf16[3,128]{1,0:T(4,128)(2,1)S(1)}, bf16[3,128]{1,0:T(4,128)(2,1)}, u32[]{:S(2)}) copy-start(bf16[3,128]{1,0:T(4,128)(2,1)} %param.29) | copy-start | bytes 2308
  133.7 82.9 %copy-start.11 = (bf16[1,8,2048]{2,1,0:T(8,128)(2,1)S(1)}, bf16[1,8,2048]{2,1,0:T(8,128)(2,1)}, u32[]{:S(2)}) copy-start(bf16[1,8,2048]{2,1,0:T(8,128)(2,1)} %param.19) | copy-start | bytes 98308
  133.7 83.0 %copy-start.67 = (bf16[512]{0:T(512)(128)(2,1)S(1)}, bf16[512]{0:T(512)(128)(2,1)}, u32[]{:S(2)}) copy-start(bf16[512]{0:T(512)(128)(2,1)} %param.32) | copy-start | bytes 3076
  134.6 162.3 %all-gather.13.cloned.1.call-start = ((), (), s32[]{:S(2)}) async-start(), calls=%async_computation.6 | async-start | bytes 1179648 | tf_op jit(solution)/shard_map/all_gather | solution.py:71
  151.7 21.8 %copy-start.49 = (f32[8]{0:T(128)}, f32[8]{0:T(128)S(1)}, u32[]{:S(2)}) copy-start(f32[8]{0:T(128)S(1)} %get-tuple-element.104) | copy-start | bytes 100
  151.7 21.8 %copy-start.51 = (f32[8]{0:T(128)}, f32[8]{0:T(128)S(1)}, u32[]{:S(2)}) copy-start(f32[8]{0:T(128)S(1)} %get-tuple-element.105) | copy-start | bytes 100
  151.7 21.8 %copy-start.53 = (f32[8]{0:T(128)}, f32[8]{0:T(128)S(1)}, u32[]{:S(2)}) copy-start(f32[8]{0:T(128)S(1)} %get-tuple-element.106) | copy-start | bytes 100
  151.7 21.8 %copy-start.55 = (f32[8]{0:T(128)}, f32[8]{0:T(128)S(1)}, u32[]{:S(2)}) copy-start(f32[8]{0:T(128)S(1)} %get-tuple-element.107) | copy-start | bytes 100
  151.7 21.8 %copy-start.57 = (f32[8]{0:T(128)}, f32[8]{0:T(128)S(1)}, u32[]{:S(2)}) copy-start(f32[8]{0:T(128)S(1)} %get-tuple-element.108) | copy-start | bytes 100
  151.7 21.8 %copy-start.59 = (f32[8]{0:T(128)}, f32[8]{0:T(128)S(1)}, u32[]{:S(2)}) copy-start(f32[8]{0:T(128)S(1)} %get-tuple-element.109) | copy-start | bytes 100
  151.8 21.8 %copy-start.61 = (f32[8]{0:T(128)}, f32[8]{0:T(128)S(1)}, u32[]{:S(2)}) copy-start(f32[8]{0:T(128)S(1)} %get-tuple-element.110) | copy-start | bytes 100
  151.8 21.8 %copy-start.63 = (f32[8]{0:T(128)}, f32[8]{0:T(128)S(1)}, u32[]{:S(2)}) copy-start(f32[8]{0:T(128)S(1)} %get-tuple-element.111) | copy-start | bytes 100
  173.4 130.9 %all-gather.11.cloned.1.call-start = ((), (), s32[]{:S(2)}) async-start(), calls=%async_computation.5 | async-start | bytes 1179648 | tf_op jit(solution)/shard_map/all_gather | solution.py:71
  188.6 27.4 %copy-start.33 = (f32[8]{0:T(128)}, f32[8]{0:T(128)S(1)}, u32[]{:S(2)}) copy-start(f32[8]{0:T(128)S(1)} %get-tuple-element.84) | copy-start | bytes 100
  188.6 27.4 %copy-start.35 = (f32[8]{0:T(128)}, f32[8]{0:T(128)S(1)}, u32[]{:S(2)}) copy-start(f32[8]{0:T(128)S(1)} %get-tuple-element.85) | copy-start | bytes 100
  188.6 61.2 %copy-start.37 = (f32[8]{0:T(128)}, f32[8]{0:T(128)S(1)}, u32[]{:S(2)}) copy-start(f32[8]{0:T(128)S(1)} %get-tuple-element.86) | copy-start | bytes 100
  188.6 61.2 %copy-start.39 = (f32[8]{0:T(128)}, f32[8]{0:T(128)S(1)}, u32[]{:S(2)}) copy-start(f32[8]{0:T(128)S(1)} %get-tuple-element.87) | copy-start | bytes 100
  188.6 61.2 %copy-start.41 = (f32[8]{0:T(128)}, f32[8]{0:T(128)S(1)}, u32[]{:S(2)}) copy-start(f32[8]{0:T(128)S(1)} %get-tuple-element.88) | copy-start | bytes 100
  188.6 61.2 %copy-start.43 = (f32[8]{0:T(128)}, f32[8]{0:T(128)S(1)}, u32[]{:S(2)}) copy-start(f32[8]{0:T(128)S(1)} %get-tuple-element.89) | copy-start | bytes 100
  188.7 61.2 %copy-start.45 = (f32[8]{0:T(128)}, f32[8]{0:T(128)S(1)}, u32[]{:S(2)}) copy-start(f32[8]{0:T(128)S(1)} %get-tuple-element.90) | copy-start | bytes 100
  188.7 61.2 %copy-start.47 = (f32[8]{0:T(128)}, f32[8]{0:T(128)S(1)}, u32[]{:S(2)}) copy-start(f32[8]{0:T(128)S(1)} %get-tuple-element.91) | copy-start | bytes 100
  215.3 107.9 %all-gather.15.cloned.1.call-start = ((), (), s32[]{:S(2)}) async-start(), calls=%async_computation.7 | async-start | bytes 3145728 | tf_op jit(solution)/shard_map/all_gather | solution.py:227
  253.2 26.2 %all-to-all-start.2 = ((bf16[64,8,656]{2,1,0:T(8,128)(2,1)}), bf16[64,8,656]{2,1,0:T(8,128)(2,1)S(1)}, u32[]{:S(2)}, u32[]{:S(2)}) async-start(bf16[64,8,656]{2,1,0:T(8,128)(2,1)} %broadcast_in_dim.26), calls=%async_computation.2 | async-start | bytes 1572864 | tf_op jit(solution)/shard_map/all_to_all | solution.py:30
  265.2 14.4 %copy-start.6 = (bf16[128,128]{0,1:T(8,128)(2,1)}, bf16[128,128]{0,1:T(8,128)(2,1)S(1)}, u32[]{:S(2)}) copy-start(bf16[128,128]{0,1:T(8,128)(2,1)S(1)} %rev.33) | copy-start | bytes 98308
  297.1 7.3 %copy-start.2 = (bf16[512,8,64]{0,2,1:T(8,128)(2,1)S(1)}, bf16[512,8,64]{0,2,1:T(8,128)(2,1)}, u32[]{:S(2)}) copy-start(bf16[512,8,64]{0,2,1:T(8,128)(2,1)} %multiply_convert_fusion.2) | copy-start | bytes 1572868
  297.1 7.3 %copy-start.26 = (f32[128,8]{0,1:T(8,128)S(1)}, f32[128,8]{0,1:T(8,128)}, u32[]{:S(2)}) copy-start(f32[128,8]{0,1:T(8,128)} %get-tuple-element.72) | copy-start | bytes 12292
  297.1 7.3 %copy-start.34 = (f32[8]{0:T(128)S(1)}, f32[8]{0:T(128)}, u32[]{:S(2)}) copy-start(f32[8]{0:T(128)} %copy-done.33) | copy-start | bytes 100
  297.1 7.3 %copy-start.36 = (f32[8]{0:T(128)S(1)}, f32[8]{0:T(128)}, u32[]{:S(2)}) copy-start(f32[8]{0:T(128)} %copy-done.35) | copy-start | bytes 100
  297.1 7.3 %copy-start.38 = (f32[8]{0:T(128)S(1)}, f32[8]{0:T(128)}, u32[]{:S(2)}) copy-start(f32[8]{0:T(128)} %copy-done.37) | copy-start | bytes 100
  304.6 18.6 %copy-start.20 = (f32[512]{0:T(512)S(1)}, f32[512]{0:T(512)}, u32[]{:S(2)}) copy-start(f32[512]{0:T(512)} %convert_element_type.1335) | copy-start | bytes 6148
  (47 other events, 266.1 us)
Sparse Core Ops, SparseCore 0:
  13.3 28.7 all-gather.8
  132.2 38.8 all-gather.18
  173.3 39.7 all-gather.16
  215.0 41.2 all-gather.12
  258.1 46.1 all-gather.10
  306.3 16.8 all-gather.14
where the time goes:
time: 349 us; the launch traced here: 345 us
  blocking collectives  142 us (41%)
  waiting for transfers between devices  83.4 us (24%)
  local copies, waits for them, and re-layouts  40.7 us (12%)
  other arithmetic  23 us (7%)
  starting transfers between devices  22.5 us (6%)
  matrix products  18.9 us (5%)
  between operations  14.9 us (4%)
    psum x2, blocking collectives, over_axes(): return functools.reduce(lax.psum, axes, x)  66.3 us
    all_gather x4, blocking collectives, entering_2(): lax.all_gather(part.astype(kind), axis)  63.1 us
    all_gather x4, waiting for transfers between devices, entering_2(): lax.all_gather(part.astype(kind), axis)  45.8 us
    all_to_all x3, starting transfers between devices, sent_to_all(): lax.all_to_all(jnp.broadcast_to(x[None], (peers, *x.shape)), axis, 0, 0,...  19.6 us
    all_to_all x3, waiting for transfers between devices, sent_to_all(): lax.all_to_all(jnp.broadcast_to(x[None], (peers, *x.shape)), axis, 0, 0,...  15.9 us
    all_gather x1, waiting for transfers between devices, shards(): lax.all_gather(w_out, 'dp', axis=0, tiled=True)  15.5 us
    all_to_all x1, blocking collectives, sum_at_owner(): tiles = lax.all_to_all(split_up(x, dim, peers), axis, 0, 0, tiled=True)  12.4 us
    concatenate x1, local copies, waits for them, and re-layouts, shards(): jnp.concatenate([full_x, full_b, full_c, full_fwd, full_bwd, full_z], axi...  9.42 us
  transfers between devices with their start and end apart: 11, of which 8 were waited for; matrix products, arithmetic and copies ran while one was open for 18% of the time, Pallas kernels for 0%

commit v1 on v0

v1 whole, which is shorter than its diff:
```python
import functools

import jax
import jax.numpy as jnp
from jax import lax
from jax.experimental import pallas as pl
from jax.experimental.pallas import tpu as pltpu
from jax.sharding import Mesh
from jax.sharding import PartitionSpec as P

SP = ("sp_0", "sp_1")
SP_TP = ("sp_0", "sp_1", "tp")
MESH = pl.DeviceIdType.MESH
EPSILON = 1e-06
F32 = jnp.float32
BF16 = jnp.bfloat16
TOKENS = 128
STATE = 128
LANES = 128
HEADS = 8
PAIRS = HEADS // 2
INNER = 512
MIXED = INNER + 2 * STATE
COL_Z = MIXED
COL_DT = COL_Z + INNER
COLS = COL_DT + LANES
ROWS = TOKENS + 16
CTX_ROWS = 8
CTX_COLS = INNER + STATE + LANES


def rounded(v):
    return v.astype(BF16).astype(F32)


def silu(v):
    return v / (1.0 + jnp.exp(-v))


def softplus(v):
    return jnp.maximum(v, 0.0) + jnp.log1p(jnp.exp(-jnp.abs(v)))


def rows_of(shape):
    return lax.broadcasted_iota(jnp.int32, shape, 0)


def lanes_of(shape):
    return lax.broadcasted_iota(jnp.int32, shape, 1)


def running_sums(v, heads):
    n = v.shape[0]
    row = rows_of(v.shape)
    down = up = v
    step = 1
    while step < n:
        down = down + jnp.where(row >= step, pltpu.roll(down, step, 0), 0.0)
        up = up + jnp.where(row < n - step, pltpu.roll(up, n - step, 0), 0.0)
        step *= 2
    return jnp.where(lanes_of(v.shape) < heads, down, up)


def spread(v, head):
    shape = (v.shape[0], LANES)
    left = jnp.broadcast_to(v[:, head : head + 1], shape)
    right = jnp.broadcast_to(v[:, head + 1 : head + 2], shape)
    return jnp.where(lanes_of(shape) < LANES // 2, left, right)


def convolved(mid, low, high, taps):
    n = mid.shape[0]
    row = rows_of(mid.shape)
    before = jnp.where(row == 0, low, pltpu.roll(mid, 1, 0))
    after = jnp.where(row == n - 1, high, pltpu.roll(mid, n - 1, 0))
    summed = before * taps[0:1] + mid * taps[1:2] + after * taps[2:3]
    return rounded(silu(summed))


class Exchange:
    def __init__(self, axis, size, place, source, target, sent, got):
        self.copies = []
        for k in range(1, size):
            peer = lax.rem(place + k, size)
            self.copies.append(
                pltpu.make_async_remote_copy(
                    src_ref=source(peer),
                    dst_ref=target(),
                    send_sem=sent(k - 1),
                    recv_sem=got(k - 1),
                    device_id={axis: peer},
                    device_id_type=MESH,
                )
            )

    def start(self):
        for c in self.copies:
            c.start()
        return self

    def arrived(self):
        for c in self.copies:
            c.wait_recv()

    def left(self):
        for c in self.copies:
            c.wait_send()


def mixer(
    dims,
    small,
    modw,
    latent,
    context,
    w_x,
    w_b,
    w_c,
    w_z,
    w_dt,
    w_out,
    out,
    weights,
    out_weights,
    lat,
    ctx,
    placed,
    mod_z,
    mod_y,
    mod_x,
    edge_send,
    edge_recv,
    misc,
    hidden,
    feats,
    moved,
    growth,
    inside,
    ctx_gather,
    ctx_full,
    ctx_z,
    ctx_dz,
    state_send,
    state_recv,
    decay_y,
    tot_z,
    tot_dz,
    before,
    enter_send,
    enter_recv,
    normed,
    part_send,
    part_recv,
    local_sem,
    core_send,
    core_recv,
    mod_sems,
    lat_sems,
    edge_sems,
    y_sems,
    z_sems,
    part_sems,
):
    nz, ny, nx, model = dims
    width = model // nx
    own_rows = TOKENS // nx
    slab = STATE // ny
    z = lax.axis_index("sp_0")
    y = lax.axis_index("sp_1")
    x = lax.axis_index("tp")
    core = lax.axis_index("dp")
    place = z * ny + y
    count = nz * ny

    half = model // 2
    own_half = pl.ds(pl.multiple_of(core * half, half), half)
    out_half = pl.ds(pl.multiple_of(core * (INNER // 2), INNER // 2), INNER // 2)
    pieces = (
        (w_x, weights.at[own_half, pl.ds(0, INNER)]),
        (w_b, weights.at[own_half, pl.ds(INNER, STATE)]),
        (w_c, weights.at[own_half, pl.ds(INNER + STATE, STATE)]),
        (w_dt, weights.at[own_half, pl.ds(COL_DT, LANES)]),
        (w_z, weights.at[own_half, pl.ds(COL_Z, INNER)]),
        (w_out, out_weights.at[out_half, :]),
    )
    local = [
        pltpu.make_async_copy(source, target, local_sem.at[i])
        for i, (source, target) in enumerate(pieces)
    ]
    own_latent = pltpu.make_async_copy(latent, lat.at[x], local_sem.at[len(pieces)])
    own_latent.start()
    barrier = pltpu.get_barrier_semaphore()
    up_place = lax.rem(place + 1, count)
    down_place = lax.rem(place + count - 1, count)
    above = {"sp_0": up_place // ny, "sp_1": lax.rem(up_place, ny)}
    below = {"sp_0": down_place // ny, "sp_1": lax.rem(down_place, ny)}
    peers = [{"sp_0": lax.rem(z + k, nz)} for k in range(1, nz)]
    peers += [{"sp_1": lax.rem(y + k, ny)} for k in range(1, ny)]
    peers += [{"tp": lax.rem(x + k, nx)} for k in range(1, nx)]
    peers += [{"dp": 1 - core}, above, below]
    for peer in peers:
        pl.semaphore_signal(barrier, inc=1, device_id=peer, device_id_type=MESH)
    for c in local:
        c.start()

    rows = modw.shape[1]
    chunk = placed.shape[1]
    per = chunk // rows
    placed[...] = jnp.zeros_like(placed)
    at = pl.ds(pl.multiple_of(lax.rem(place, per) * rows, rows), rows)
    placed[:, at, :] = modw[...]
    lane_at = pl.ds(pl.multiple_of((place // per) * chunk, chunk), chunk)
    act = jnp.broadcast_to(rounded(silu(small[0:1, lane_at])), (8, chunk))
    act_ctx = jnp.broadcast_to(rounded(silu(small[1:2, lane_at])), (8, chunk))
    row8 = rows_of((8, chunk))
    partial = jnp.zeros((8, width), F32)
    for k in range(3):
        left = jnp.where(row8 == k, act, 0.0)
        if k < 2:
            left = jnp.where(row8 == 3 + k, act_ctx, left)
        partial = partial + jnp.dot(
            left.astype(BF16), placed[k], preferred_element_type=F32
        )
    mod_z[z] = partial

    ctx[...] = context[...].astype(F32)
    edge_send[0] = ctx[0:1, :]
    edge_send[1] = ctx[CTX_ROWS - 1 : CTX_ROWS, :]

    pl.semaphore_wait(barrier, len(peers))
    mods = [
        Exchange(
            axis,
            size,
            me,
            lambda peer, buf=buf, me=me: buf.at[me],
            lambda buf=buf, me=me: buf.at[me],
            lambda k, i=i: mod_sems.at[0, i, k],
            lambda k, i=i: mod_sems.at[1, i, k],
        )
        for i, (axis, size, me, buf) in enumerate(
            (("sp_0", nz, z, mod_z), ("sp_1", ny, y, mod_y), ("tp", nx, x, mod_x))
        )
    ]
    mods[0].start()
    lat_copies = Exchange(
        "tp",
        nx,
        x,
        lambda peer: latent,
        lambda: lat.at[x],
        lambda k: lat_sems.at[0, k],
        lambda k: lat_sems.at[1, k],
    ).start()

    def edge(slot, to):
        return pltpu.make_async_remote_copy(
            src_ref=edge_send.at[slot],
            dst_ref=edge_recv.at[slot],
            send_sem=edge_sems.at[0, slot],
            recv_sem=edge_sems.at[1, slot],
            device_id=to,
            device_id_type=MESH,
        )

    edges = [edge(0, below), edge(1, above), edge(2, below), edge(3, above)]
    edges[0].start()
    edges[1].start()
    swaps = [
        pltpu.make_async_remote_copy(
            src_ref=source,
            dst_ref=target,
            send_sem=core_send.at[i],
            recv_sem=core_recv.at[i],
            device_id={"dp": 1 - core},
            device_id_type=MESH,
        )
        for i, (source, target) in enumerate(pieces)
    ]
    for c in swaps:
        c.start()

    mods[0].arrived()
    total = mod_z[0]
    for k in range(1, nz):
        total = total + mod_z[k]
    mod_y[y] = total
    mods[1].start()

    own_latent.wait()
    lat_copies.arrived()
    edge_send[2] = lat[0].astype(F32)[0:1, :]
    edge_send[3] = lat[nx - 1].astype(F32)[own_rows - 1 : own_rows, :]
    edges[2].start()
    edges[3].start()

    def inverse(v):
        return lax.rsqrt(jnp.mean(v * v, axis=1, keepdims=True) + EPSILON)

    scales = [inverse(lat[t].astype(F32)) for t in range(nx)]

    mods[1].arrived()
    total = mod_y[0]
    for k in range(1, ny):
        total = total + mod_y[k]
    mod_x[x] = total
    mods[2].start()

    misc[...] = jnp.zeros_like(misc)
    misc[8:16, :] = ctx[...]
    for e in edges:
        e.wait_recv()
    misc[0:1, :] = jnp.where(place > 0, edge_recv[3], 0.0)
    misc[1:2, :] = jnp.where(place < count - 1, edge_recv[2], 0.0)
    misc[2:3, :] = jnp.where(place > 0, edge_recv[1], 0.0)
    misc[3:4, :] = jnp.where(place < count - 1, edge_recv[0], 0.0)
    misc_scale = inverse(misc[...])
    row16 = rows_of((16, 1))
    is_lat = row16 < 2
    kept = jnp.logical_or(
        row16 >= 8,
        jnp.logical_or(
            jnp.logical_and(row16 % 2 == 0, place > 0),
            jnp.logical_and(row16 % 2 == 1, place < count - 1),
        ),
    )

    mods[2].arrived()
    for c in range(nx):
        cols = slice(c * width, (c + 1) * width)
        mod = mod_x[c]
        gain = small[2:3, cols]
        scale = gain * (1.0 + mod[1:2])
        shift = mod[0:1]
        scale_ctx = gain * (1.0 + mod[4:5])
        shift_ctx = mod[3:4]
        for t in range(nx):
            value = lat[t, :, cols].astype(F32) * scales[t] * scale + shift
            hidden[t * own_rows : (t + 1) * own_rows, cols] = value.astype(BF16)
        value = misc[:, cols] * misc_scale * jnp.where(is_lat, scale, scale_ctx)
        value = value + jnp.where(is_lat, shift, shift_ctx)
        hidden[TOKENS:ROWS, cols] = jnp.where(kept, value, 0.0).astype(BF16)

    for i in range(len(pieces)):
        local[i].wait()
        swaps[i].wait_recv()

    left = 0
    while left < COLS:
        wide = min(256, COLS - left)
        cols = slice(left, left + wide)
        feats[:, cols] = rounded(
            jnp.dot(hidden[...], weights[:, cols], preferred_element_type=F32)
        )
        left += wide

    for b in range((INNER + STATE) // LANES):
        cols = slice(b * LANES, (b + 1) * LANES)
        ctx_gather[y, :, cols] = convolved(
            feats[TOKENS + 8 : TOKENS + 16, cols],
            feats[TOKENS + 2 : TOKENS + 3, cols],
            feats[TOKENS + 3 : TOKENS + 4, cols],
            small[4:7, cols],
        )
    ctx_gather[y, :, INNER + STATE : CTX_COLS] = feats[TOKENS + 8 : TOKENS + 16, COL_DT:COLS]

    def along(axis, size, me, sems, index, source, target):
        return Exchange(
            axis,
            size,
            me,
            source,
            target,
            lambda k: sems.at[0, index, k],
            lambda k: sems.at[1, index, k],
        )

    ctx_copies = along(
        "sp_1", ny, y, y_sems, 0, lambda peer: ctx_gather.at[y], lambda: ctx_gather.at[y]
    ).start()

    rates = small[3:4, INNER : INNER + LANES]
    for b in range(MIXED // LANES):
        cols = slice(b * LANES, (b + 1) * LANES)
        feats[0:TOKENS, cols] = convolved(
            feats[0:TOKENS, cols],
            feats[TOKENS : TOKENS + 1, cols],
            feats[TOKENS + 1 : TOKENS + 2, cols],
            small[4:7, cols],
        )
    b_turned = feats[0:TOKENS, INNER : INNER + STATE].T.astype(BF16)
    c_vals = feats[0:TOKENS, INNER + STATE : MIXED].astype(BF16)
    steps = softplus(feats[0:TOKENS, COL_DT:COLS])
    sums = running_sums(-rates * steps, HEADS)
    for q in range(PAIRS):
        cols = slice(q * LANES, (q + 1) * LANES)
        x_vals = feats[0:TOKENS, cols]
        for way in range(2):
            head = way * HEADS + 2 * q
            step = spread(steps, head)
            decay = spread(sums, head)
            end = decay[TOKENS - 1 : TOKENS] if way == 0 else decay[0:1]
            moved_x = rounded(x_vals * step)
            moved[way * TOKENS : (way + 1) * TOKENS, cols] = moved_x.astype(BF16)
            growth[way, :, cols] = jnp.exp(decay)
            at_end = (moved_x * jnp.exp(end - decay)).astype(BF16)
            state = jnp.dot(b_turned, at_end, preferred_element_type=F32).astype(BF16)
            for p in range(ny):
                state_send[p, way * slab : (way + 1) * slab, cols] = state[
                    p * slab : (p + 1) * slab
                ]
            decay_y[y, way * PAIRS + q : way * PAIRS + q + 1, :] = end
    decay_copies = along(
        "sp_1", ny, y, y_sems, 1, lambda peer: decay_y.at[y], lambda: decay_y.at[y]
    ).start()
    state_copies = along(
        "sp_1", ny, y, y_sems, 2, lambda peer: state_send.at[peer], lambda: state_recv.at[y]
    ).start()
    state_recv[y] = state_send[y]

    ctx_copies.arrived()
    lines = ny * CTX_ROWS
    ctx_b = ctx_gather[:, :, INNER : INNER + STATE].reshape(lines, STATE).T
    ctx_steps = softplus(ctx_gather[:, :, INNER + STATE : CTX_COLS].reshape(lines, LANES))
    ctx_sums = running_sums(-rates * ctx_steps, HEADS)
    for q in range(PAIRS):
        cols = slice(q * LANES, (q + 1) * LANES)
        x_vals = ctx_gather[:, :, cols].reshape(lines, LANES)
        for way in range(2):
            head = way * HEADS + 2 * q
            decay = spread(ctx_sums, head)
            end = decay[lines - 1 : lines] if way == 0 else decay[0:1]
            scaled = rounded(x_vals * spread(ctx_steps, head)) * jnp.exp(end - decay)
            ctx_full[way, :, cols] = jnp.dot(
                ctx_b, scaled, preferred_element_type=F32, precision=lax.Precision.HIGHEST
            )
            ctx_dz[z, way * PAIRS + q : way * PAIRS + q + 1, :] = end
    own_slab = pl.ds(pl.multiple_of(y * slab, slab), slab)
    for way in range(2):
        ctx_z[z, way * slab : (way + 1) * slab, :] = ctx_full[way, own_slab, :].astype(BF16)
    ctx_dz_copies = along(
        "sp_0", nz, z, z_sems, 0, lambda peer: ctx_dz.at[z], lambda: ctx_dz.at[z]
    ).start()
    ctx_z_copies = along(
        "sp_0", nz, z, z_sems, 1, lambda peer: ctx_z.at[z], lambda: ctx_z.at[z]
    ).start()

    def attend():
        scores = jnp.dot(c_vals, b_turned, preferred_element_type=F32)
        turned = sums.T
        square = (TOKENS, TOKENS)
        lower = rows_of(square) >= lanes_of(square)
        upper = rows_of(square) <= lanes_of(square)
        for q in range(PAIRS):
            cols = slice(q * LANES, (q + 1) * LANES)
            halves = []
            for h in (2 * q, 2 * q + 1):
                both = []
                for way, mask in ((0, lower), (1, upper)):
                    lane = way * HEADS + h
                    gap = sums[:, lane : lane + 1] - turned[lane : lane + 1, :]
                    decayed = scores * jnp.exp(jnp.minimum(gap, 0.0))
                    both.append(jnp.where(mask, decayed, 0.0).astype(BF16))
                halves.append(
                    jnp.dot(
                        jnp.concatenate(both, axis=1),
                        moved[:, cols],
                        preferred_element_type=F32,
                    )
                )
            inside[:, cols] = jnp.where(lanes_of(square) < LANES // 2, halves[0], halves[1])

    attend()

    decay_copies.arrived()
    state_copies.arrived()
    decays = [decay_y[j] for j in range(ny)]
    is_fwd = rows_of((8, LANES)) < PAIRS
    ahead = [None] * ny
    acc_f = acc_b = jnp.zeros((8, LANES), F32)
    for j in range(ny):
        ahead[j] = acc_f
        acc_f = acc_f + decays[j]
    for j in reversed(range(ny)):
        ahead[j] = jnp.exp(jnp.where(is_fwd, ahead[j], acc_b))
        acc_b = acc_b + decays[j]
    tot_dz[z] = acc_f
    tot_dz_copies = along(
        "sp_0", nz, z, z_sems, 2, lambda peer: tot_dz.at[z], lambda: tot_dz.at[z]
    ).start()
    factors = [jnp.exp(d) for d in decays]
    for way in range(2):
        part = slice(way * slab, (way + 1) * slab)
        for q in range(PAIRS):
            cols = slice(q * LANES, (q + 1) * LANES)
            r = way * PAIRS + q
            state = jnp.zeros((slab, LANES), F32)
            for j in range(ny) if way == 0 else reversed(range(ny)):
                before[j, part, cols] = state
                state = state * factors[j][r : r + 1] + state_recv[j, part, cols].astype(F32)
            tot_z[z, part, cols] = state.astype(BF16)
    tot_z_copies = along(
        "sp_0", nz, z, z_sems, 3, lambda peer: tot_z.at[z], lambda: tot_z.at[z]
    ).start()

    ctx_dz_copies.arrived()
    ctx_z_copies.arrived()
    ctx_factors = [jnp.exp(ctx_dz[j]) for j in range(nz)]
    starts = {}
    for way in range(2):
        part = slice(way * slab, (way + 1) * slab)
        for q in range(PAIRS):
            cols = slice(q * LANES, (q + 1) * LANES)
            r = way * PAIRS + q
            state = jnp.zeros((slab, LANES), F32)
            for j in range(nz) if way == 0 else reversed(range(nz)):
                state = state * ctx_factors[j][r : r + 1] + ctx_z[j, part, cols].astype(F32)
            starts[way, q] = state

    tot_dz_copies.arrived()
    tot_z_copies.arrived()
    tot_factors = [jnp.exp(tot_dz[j]) for j in range(nz)]
    for way in range(2):
        part = slice(way * slab, (way + 1) * slab)
        for q in range(PAIRS):
            cols = slice(q * LANES, (q + 1) * LANES)
            r = way * PAIRS + q
            state = starts[way, q]
            for j in range(nz) if way == 0 else reversed(range(nz)):
                passed = j < z if way == 0 else j > z
                later = state * tot_factors[j][r : r + 1] + tot_z[j, part, cols].astype(F32)
                state = jnp.where(passed, later, state)
            for j in range(ny):
                enter_send[j, part, cols] = (
                    before[j, part, cols] + ahead[j][r : r + 1] * state
                ).astype(BF16)
    enter_copies = along(
        "sp_1", ny, y, y_sems, 3, lambda peer: enter_send.at[peer], lambda: enter_recv.at[y]
    ).start()
    enter_recv[y] = enter_send[y]

    enter_copies.arrived()
    carried = [
        jnp.dot(
            c_vals,
            enter_recv[:, way * slab : (way + 1) * slab, :].reshape(STATE, INNER),
            preferred_element_type=F32,
        )
        for way in range(2)
    ]
    squares = jnp.zeros((TOKENS, 1), F32)
    for q in range(PAIRS):
        cols = slice(q * LANES, (q + 1) * LANES)
        value = inside[:, cols]
        for way in range(2):
            value = value + growth[way, :, cols] * carried[way][:, cols]
        value = value * silu(feats[0:TOKENS, COL_Z + q * LANES : COL_Z + (q + 1) * LANES])
        inside[:, cols] = value
        squares = squares + jnp.sum(value * value, axis=1, keepdims=True)
    scale = lax.rsqrt(squares / INNER + EPSILON)
    for q in range(PAIRS):
        cols = slice(q * LANES, (q + 1) * LANES)
        normed[:, cols] = (inside[:, cols] * scale * small[3:4, cols]).astype(BF16)

    part_copies = []
    for c in range(nx):
        cols = slice(c * width, (c + 1) * width)
        term = jnp.dot(normed[...], out_weights[:, cols], preferred_element_type=F32)
        term = term.astype(BF16)
        for t in range(nx):
            part_send[t, :, cols] = term[t * own_rows : (t + 1) * own_rows]
        part_copies.append(
            along(
                "tp",
                nx,
                x,
                part_sems,
                c,
                lambda peer, cols=cols: part_send.at[peer, :, cols],
                lambda cols=cols: part_recv.at[x, :, cols],
            ).start()
        )
        part_recv[x, :, cols] = part_send[x, :, cols]
    for c in range(nx):
        cols = slice(c * width, (c + 1) * width)
        part_copies[c].arrived()
        value = part_recv[0, :, cols].astype(F32)
        for t in range(1, nx):
            value = value + part_recv[t, :, cols].astype(F32)
        out[:, cols] = (mod_x[c, 2:3, :] * value).astype(BF16)

    for e in edges + swaps:
        e.wait_send()
    everything = mods + part_copies + [lat_copies, ctx_copies, decay_copies, state_copies]
    everything += [ctx_dz_copies, ctx_z_copies, tot_dz_copies, tot_z_copies, enter_copies]
    for e in everything:
        e.left()


def shards(
    sizes,
    latent,
    condition,
    context,
    context_source,
    mod_weight,
    norm_gain,
    w_x,
    w_b,
    w_c,
    w_z,
    w_dt,
    conv_x,
    conv_b,
    conv_c,
    decay_rate,
    out_gain,
    w_out,
):
    nz, ny, nx = sizes
    model = latent.shape[-1]
    own_rows = latent.shape[1]
    width = model // nx
    slab = STATE // ny
    span = max(model, 1024)

    def row(*pieces):
        flat = jnp.concatenate([p.astype(F32) for p in pieces])
        return jnp.pad(flat, (0, span - flat.shape[0]))

    small = jnp.stack(
        [
            row(condition[0]),
            row(context_source),
            row(norm_gain),
            row(out_gain, decay_rate[0], decay_rate[1]),
            *[row(conv_x[k], conv_b[k], conv_c[k]) for k in range(3)],
            jnp.zeros((span,), F32),
        ]
    )
    step_weights = jnp.pad(
        jnp.concatenate([w_dt[0], w_dt[1]], axis=1), ((0, 0), (0, LANES - 2 * HEADS))
    )
    rows = mod_weight.shape[1]
    vmem = pl.BlockSpec(memory_space=pltpu.VMEM)
    hbm = pl.BlockSpec(memory_space=pl.ANY)
    dma = pltpu.SemaphoreType.DMA
    most = max(nz, ny, nx) - 1
    scratch = [
        pltpu.VMEM((model, COLS), BF16),
        pltpu.VMEM((INNER, model), BF16),
        pltpu.VMEM((nx, own_rows, model), BF16),
        pltpu.VMEM((CTX_ROWS, model), F32),
        pltpu.VMEM((3, max(rows, LANES), width), BF16),
        pltpu.VMEM((nz, 8, width), F32),
        pltpu.VMEM((ny, 8, width), F32),
        pltpu.VMEM((nx, 8, width), F32),
        pltpu.VMEM((4, 1, model), F32),
        pltpu.VMEM((4, 1, model), F32),
        pltpu.VMEM((16, model), F32),
        pltpu.VMEM((ROWS, model), BF16),
        pltpu.VMEM((ROWS, COLS), F32),
        pltpu.VMEM((2 * TOKENS, INNER), BF16),
        pltpu.VMEM((2, TOKENS, INNER), F32),
        pltpu.VMEM((TOKENS, INNER), F32),
        pltpu.VMEM((ny, CTX_ROWS, CTX_COLS), F32),
        pltpu.VMEM((2, STATE, INNER), F32),
        pltpu.VMEM((nz, 2 * slab, INNER), BF16),
        pltpu.VMEM((nz, 8, LANES), F32),
        pltpu.VMEM((ny, 2 * slab, INNER), BF16),
        pltpu.VMEM((ny, 2 * slab, INNER), BF16),
        pltpu.VMEM((ny, 8, LANES), F32),
        pltpu.VMEM((nz, 2 * slab, INNER), BF16),
        pltpu.VMEM((nz, 8, LANES), F32),
        pltpu.VMEM((ny, 2 * slab, INNER), F32),
        pltpu.VMEM((ny, 2 * slab, INNER), BF16),
        pltpu.VMEM((ny, 2 * slab, INNER), BF16),
        pltpu.VMEM((TOKENS, INNER), BF16),
        pltpu.VMEM((nx, own_rows, model), BF16),
        pltpu.VMEM((nx, own_rows, model), BF16),
        dma((7,)),
        dma((6,)),
        dma((6,)),
        dma((2, 3, most)),
        dma((2, nx - 1)),
        dma((2, 4)),
        dma((2, 4, ny - 1)),
        dma((2, 4, nz - 1)),
        dma((2, nx, nx - 1)),
    ]
    update = pl.pallas_call(
        functools.partial(mixer, (nz, ny, nx, model)),
        out_shape=jax.ShapeDtypeStruct((own_rows, model), BF16),
        in_specs=[vmem, vmem, hbm, vmem] + [hbm] * 6,
        out_specs=vmem,
        scratch_shapes=scratch,
        compiler_params=pltpu.CompilerParams(
            collective_id=0, has_side_effects=True, vmem_limit_bytes=56 * 1024 * 1024
        ),
    )(small, mod_weight, latent[0], context[0], w_x, w_b, w_c, w_z, step_weights, w_out)
    return update[None]


def solution(mesh):
    nx = mesh.shape["tp"]
    ny = 8
    nz = mesh.shape["sp"] // ny
    return program(mesh, nz, ny, nx)


def program(mesh, nz, ny, nx):
    torus = Mesh(
        mesh.devices.reshape(nz, ny, nx, mesh.shape["dp"]), ("sp_0", "sp_1", "tp", "dp")
    )
    placed = (
        P("dp", SP_TP, None),
        P("dp", None),
        P("dp", SP, None),
        P(),
        P(None, SP, "tp"),
        P(),
        P("dp", "tp"),
        P("dp", "tp"),
        P("dp", "tp"),
        P("dp", "tp"),
        P(None, "dp", "tp"),
        P(None, "tp"),
        P(None, "tp"),
        P(None, "tp"),
        P(None, "tp"),
        P("tp"),
        P(("tp", "dp"), None),
    )
    return jax.shard_map(
        functools.partial(shards, (nz, ny, nx)),
        mesh=torus,
        in_specs=placed,
        out_specs=P("dp", SP_TP, None),
        check_vma=False,
    )
```

time: 349 us -> 75.6 us (0.22)
  blocking collectives: 142 us -> 0 us
  waiting for transfers between devices: 83.4 us -> 0 us
  Pallas kernels: 0 us -> 66.5 us
  local copies, waits for them, and re-layouts: 40.7 us -> 8.08 us
  other arithmetic: 23 us -> 0.11 us
  starting transfers between devices: 22.5 us -> 0 us
  matrix products: 18.9 us -> 0 us
  between operations: 14.9 us -> 0.06 us
    pallas_call x0 -> x1, Pallas kernels: none -> 66.5 us  [shards(): pl.pallas_call(functools.partial(mixer, (nz, ny, nx, model)), out_shape=j...]
    psum x2 -> x0, blocking collectives: 66.3 us -> none  [over_axes(): return functools.reduce(lax.psum, axes, x)]
    all_gather x4 -> x0, blocking collectives: 63.1 us -> none  [entering_2(): lax.all_gather(part.astype(kind), axis)]
    all_gather x6 -> x0, waiting for transfers between devices: 61.3 us -> none  [the longest x4 45.8 us: entering_2(): lax.all_gather(part.astype(kind), axis)]
    all_to_all x3 -> x0, starting transfers between devices: 19.6 us -> none  [sent_to_all(): lax.all_to_all(jnp.broadcast_to(x[None], (peers, *x.shape)), axis, 0, 0,...]
    dot_general x12 -> x0, matrix products: 18.9 us -> none  [the longest x2 5.87 us: direction_output(): jnp.einsum('clgn,cghpn->clghp', c_blocks, entering.astype(jnp.bfloat16),...]
    all_to_all x3 -> x0, waiting for transfers between devices: 15.9 us -> none  [sent_to_all(): lax.all_to_all(jnp.broadcast_to(x[None], (peers, *x.shape)), axis, 0, 0,...]
    concatenate x2 -> x1, local copies, waits for them, and re-layouts: 14.8 us -> 0.17 us  [shards(): jnp.concatenate([w_dt[0], w_dt[1]], axis=1)]
  transfers between devices with their start and end apart: 11 -> 0, of which waited for: 8 -> 0; matrix products, arithmetic and copies ran while one was open for 18% -> 0% of each run, Pallas kernels for 0% -> 0%
where the time goes in v1:
time: 75.6 us; the launch traced here: 74.7 us
  Pallas kernels  66.5 us (88%)
  local copies, waits for them, and re-layouts  8.08 us (11%)
    pallas_call x1, Pallas kernels, shards(): pl.pallas_call(functools.partial(mixer, (nz, ny, nx, model)), out_shape=j...  66.5 us
    unnamed x19, local copies, waits for them, and re-layouts  6.36 us

profile of v1, /device:TPU:6, one launch (start us, length us, event | category | flops | bytes accessed | tf_op | source)
XLA Modules:
  0.0 74.7 jit_solution(1497967917947279664)
XLA Ops:
  0.0 0.0 copy-start.8
  0.0 0.7 copy-done.8
  0.7 0.0 copy-start.5
  0.7 0.7 copy-done.5
  1.4 0.0 copy-start.6
  1.4 0.7 copy-done.6
  2.1 0.0 copy-start.1
  2.1 0.0 copy-start.7
  2.1 0.7 copy-done.7
  2.8 0.0 copy-done.1
  2.8 0.1 select_maximum_fusion
  2.9 0.0 copy-start.3
  2.9 0.7 copy-done.3
  3.6 0.0 copy-start.4
  3.6 0.7 copy-done.4
  4.3 0.0 copy-start.2
  4.3 0.7 copy-done.2
  5.0 0.0 copy-start
  5.0 0.7 stack.48.small
  5.7 0.0 copy-done
  5.7 0.2 copy.20
  5.9 0.8 %pad.25.w_dt = bf16[1024,128]{1,0:T(8,128)(2,1)} pad(bf16[1024,16]{1,0:T(8,128)(2,1)S(1)} %copy.20, bf16[]{:T(256)} %constant.6.clone.1), padding=0_0x0_112 | pad | bytes 294914 | tf_op jit(solution)/shard_map/jit(_pad)/pad | solution.py:641
  6.7 66.5 %shard_map.163 = bf16[32,2048]{1,0:T(8,128)(2,1)} custom-call(f32[8,2048]{1,0:T(8,128)} %stack.48.small, bf16[3,32,512]{2,1,0:T(8,128)(2,1)} %modw.1, bf16[32,2048]{1,0:T(8,128)(2,1)} %bitcast.30, bf16[8,2048]{1,0:T(8,128)(2,1)} %bitcast.31, bf16[1024,512]{1,0:T(8,128)(2,1)} %w_x.1, bf16[1024,128]{1,0:T(8,128)(2,1)} %w_b.1, bf16[1024,128]{1,0:T(8,128)(2,1)} %w_c.1, ...), custom_call_target="tpu_custom_call" | custom-call | tf_op jit(solution)/shard_map/pallas_call | solution.py:691
  73.2 1.6 %copy.22 = bf16[1,32,2048]{2,1,0:T(8,128)(2,1)} copy(bf16[1,32,2048]{2,1,0:T(8,128)(2,1)} %bitcast.29) | data formatting | bytes 262144
  (12 shorter events, 0.1 us)
Async XLA Ops:
  0.0 0.7 copy-start.8
  0.7 0.7 copy-start.5
  1.4 0.7 copy-start.6
  2.1 0.7 copy-start.1
  2.1 0.7 copy-start.7
  2.9 0.7 copy-start.3
  3.6 0.7 copy-start.4
  4.3 0.7 copy-start.2
  5.0 0.8 %copy-start = (bf16[2,1024,8]{1,2,0:T(8,128)(2,1)S(1)}, bf16[2,1024,8]{1,2,0:T(8,128)(2,1)}, u32[]{:S(2)}) copy-start(bf16[2,1024,8]{1,2,0:T(8,128)(2,1)} %param.27) | copy-start | bytes 98308

commit v2 on v1

v2 whole, which is shorter than its diff:
```python
import functools

import jax
import jax.numpy as jnp
from jax import lax
from jax.experimental import pallas as pl
from jax.experimental.pallas import tpu as pltpu
from jax.sharding import Mesh
from jax.sharding import PartitionSpec as P

SP = ("sp_0", "sp_1")
SP_TP = ("sp_0", "sp_1", "tp")
MESH = pl.DeviceIdType.MESH
EPSILON = 1e-06
F32 = jnp.float32
BF16 = jnp.bfloat16
TOKENS = 128
STATE = 128
LANES = 128
HEADS = 8
PAIRS = HEADS // 2
INNER = 512
MIXED = INNER + 2 * STATE
COL_Z = MIXED
COL_DT = COL_Z + INNER
COLS = COL_DT + LANES
CTX_ROWS = 8


def rounded(v):
    return v.astype(BF16).astype(F32)


def silu(v):
    return v / (1.0 + jnp.exp(-v))


def softplus(v):
    return jnp.maximum(v, 0.0) + jnp.log1p(jnp.exp(-jnp.abs(v)))


def rows_of(shape):
    return lax.broadcasted_iota(jnp.int32, shape, 0)


def lanes_of(shape):
    return lax.broadcasted_iota(jnp.int32, shape, 1)


def running_sums(v, heads):
    n = v.shape[0]
    row = rows_of(v.shape)
    down = up = v
    step = 1
    while step < n:
        down = down + jnp.where(row >= step, pltpu.roll(down, step, 0), 0.0)
        up = up + jnp.where(row < n - step, pltpu.roll(up, n - step, 0), 0.0)
        step *= 2
    return jnp.where(lanes_of(v.shape) < heads, down, up)


def spread(v, head):
    shape = (v.shape[0], LANES)
    left = jnp.broadcast_to(v[:, head : head + 1], shape)
    right = jnp.broadcast_to(v[:, head + 1 : head + 2], shape)
    return jnp.where(lanes_of(shape) < LANES // 2, left, right)


def convolved(mid, low, high, taps):
    n = mid.shape[0]
    row = rows_of(mid.shape)
    before = jnp.where(row == 0, low, pltpu.roll(mid, 1, 0))
    after = jnp.where(row == n - 1, high, pltpu.roll(mid, n - 1, 0))
    summed = before * taps[0:1] + mid * taps[1:2] + after * taps[2:3]
    return rounded(silu(summed))


class Exchange:
    def __init__(self, axis, size, place, source, target, sent, got, sends=None, gets=None):
        self.sends, self.gets = sends, gets
        self.copies = []
        for k in range(1, size):
            peer = lax.rem(place + k, size)
            self.copies.append(
                pltpu.make_async_remote_copy(
                    src_ref=source(peer),
                    dst_ref=target(),
                    send_sem=sent(k - 1),
                    recv_sem=got(k - 1),
                    device_id={axis: peer},
                    device_id_type=MESH,
                )
            )

    def each(self, taken, act):
        for k, c in enumerate(self.copies, 1):
            if taken is None:
                act(c)
            else:
                pl.when(taken(k))(functools.partial(act, c))

    def start(self):
        self.each(self.sends, lambda c: c.start())
        return self

    def arrived(self):
        self.each(self.gets, lambda c: c.wait_recv())

    def left(self):
        self.each(self.sends, lambda c: c.wait_send())


def mixer(
    dims,
    condition,
    source,
    gain_in,
    out_gain,
    conv_x,
    conv_b,
    conv_c,
    rate,
    modw,
    context,
    latent,
    w_x,
    w_b,
    w_c,
    w_z,
    w_dt,
    w_out,
    parts,
    gate,
    weights,
    out_weights,
    dt_rows,
    dt_wide,
    small,
    lat,
    ctx,
    placed,
    mod_z,
    mod_y,
    mod_x,
    edge_send,
    edge_recv,
    misc,
    hidden,
    feats,
    moved,
    growth,
    inside,
    ctx_full,
    ctx_z,
    ctx_dz,
    state_send,
    state_recv,
    decay_y,
    tot_z,
    tot_dz,
    before,
    enter_send,
    enter_recv,
    normed,
    part_send,
    local_sem,
    core_send,
    core_recv,
    mod_sems,
    lat_sems,
    edge_sems,
    edge_got,
    y_sems,
    z_sems,
    part_sems,
):
    nz, ny, nx, model = dims
    width = model // nx
    own_rows = TOKENS // nx
    slab = STATE // ny
    lines = ny * CTX_ROWS
    ctx_at = TOKENS + 16
    z = lax.axis_index("sp_0")
    y = lax.axis_index("sp_1")
    x = lax.axis_index("tp")
    core = lax.axis_index("dp")
    place = z * ny + y
    count = nz * ny

    own_latent = pltpu.make_async_copy(latent, lat.at[x], local_sem.at[6])
    own_latent.start()
    half = model // 2
    own_half = pl.ds(pl.multiple_of(core * half, half), half)
    out_half = pl.ds(pl.multiple_of(core * (INNER // 2), INNER // 2), INNER // 2)
    pieces = (
        (w_dt, dt_rows.at[:, :, own_half]),
        (w_x, weights.at[own_half, pl.ds(0, INNER)]),
        (w_b, weights.at[own_half, pl.ds(INNER, STATE)]),
        (w_c, weights.at[own_half, pl.ds(INNER + STATE, STATE)]),
        (w_z, weights.at[own_half, pl.ds(COL_Z, INNER)]),
        (w_out, out_weights.at[out_half, :]),
    )
    local = [
        pltpu.make_async_copy(origin, target, local_sem.at[i])
        for i, (origin, target) in enumerate(pieces)
    ]
    barrier = pltpu.get_barrier_semaphore()
    up_place = lax.rem(place + 1, count)
    down_place = lax.rem(place + count - 1, count)
    above = {"sp_0": up_place // ny, "sp_1": lax.rem(up_place, ny)}
    below = {"sp_0": down_place // ny, "sp_1": lax.rem(down_place, ny)}
    peers = [{"sp_0": lax.rem(z + k, nz)} for k in range(1, nz)]
    peers += [{"sp_1": lax.rem(y + k, ny)} for k in range(1, ny)]
    peers += [{"tp": lax.rem(x + k, nx)} for k in range(1, nx)]
    peers += [{"dp": 1 - core}]
    for k in range(nx):
        peers += [dict(above, tp=k), dict(below, tp=k)]
    for peer in peers:
        pl.semaphore_signal(barrier, inc=1, device_id=peer, device_id_type=MESH)

    small[...] = jnp.zeros_like(small)
    for r, ref in ((1, source), (2, gain_in), (3, out_gain)):
        piece = ref[...].astype(F32)
        for k in range(piece.shape[0]):
            small[r : r + 1, k * LANES : (k + 1) * LANES] = piece[k : k + 1]
    small[0:1, 0:model] = condition[...].astype(F32)
    small[4:7, 0:INNER] = conv_x[...].astype(F32)
    small[4:7, INNER : INNER + STATE] = conv_b[...].astype(F32)
    small[4:7, INNER + STATE : MIXED] = conv_c[...].astype(F32)

    rows = modw.shape[1]
    chunk = placed.shape[1]
    per = chunk // rows
    placed[...] = jnp.zeros_like(placed)
    at = pl.ds(pl.multiple_of(lax.rem(place, per) * rows, rows), rows)
    placed[:, at, :] = modw[...]
    lane_at = pl.ds(pl.multiple_of((place // per) * chunk, chunk), chunk)
    act = jnp.broadcast_to(rounded(silu(small[0:1, lane_at])), (8, chunk))
    act_ctx = jnp.broadcast_to(rounded(silu(small[1:2, lane_at])), (8, chunk))
    row8 = rows_of((8, chunk))
    partial = jnp.zeros((8, width), F32)
    for k in range(3):
        left = jnp.where(row8 == k, act, 0.0)
        if k < 2:
            left = jnp.where(row8 == 3 + k, act_ctx, left)
        partial = partial + jnp.dot(
            left.astype(BF16), placed[k], preferred_element_type=F32
        )
    for r in range(5):
        mod_z[z, r] = partial[r : r + 1]

    pl.semaphore_wait(barrier, len(peers))
    mods = [
        Exchange(
            axis,
            size,
            me,
            lambda peer, buf=buf, me=me: buf.at[me],
            lambda buf=buf, me=me: buf.at[me],
            lambda k, i=i: mod_sems.at[0, i, k],
            lambda k, i=i: mod_sems.at[1, i, k],
        )
        for i, (axis, size, me, buf) in enumerate(
            (("sp_0", nz, z, mod_z), ("sp_1", ny, y, mod_y), ("tp", nx, x, mod_x))
        )
    ]

    def along(axis, size, me, sems, index, origin, target, sends=None, gets=None):
        return Exchange(
            axis,
            size,
            me,
            origin,
            target,
            lambda k: sems.at[0, index, k],
            lambda k: sems.at[1, index, k],
            sends,
            gets,
        )

    mods[0].start()
    ctx_copies = along(
        "sp_1", ny, y, y_sems, 0, lambda peer: context, lambda: ctx.at[y]
    ).start()
    lat_copies = along(
        "tp", nx, x, lat_sems, 0, lambda peer: latent, lambda: lat.at[x]
    ).start()
    swaps = [
        pltpu.make_async_remote_copy(
            src_ref=origin,
            dst_ref=target,
            send_sem=core_send.at[i],
            recv_sem=core_recv.at[i],
            device_id={"dp": 1 - core},
            device_id_type=MESH,
        )
        for i, (origin, target) in enumerate(pieces)
    ]
    for c, d in zip(swaps, local):
        c.start()
        d.start()
    ctx[y] = context[...]

    def edge(slot, k, to):
        return pltpu.make_async_remote_copy(
            src_ref=edge_send.at[slot],
            dst_ref=edge_recv.at[slot],
            send_sem=edge_sems.at[slot, k],
            recv_sem=edge_got.at[slot],
            device_id=to,
            device_id_type=MESH,
        )

    to_above = [edge(0, k, dict(above, tp=k)) for k in range(nx)]
    to_below = [edge(1, k, dict(below, tp=k)) for k in range(nx)]
    own_latent.wait()

    @pl.when(x == nx - 1)
    def _():
        edge_send[0] = lat[x].astype(F32)[own_rows - 1 : own_rows, :]
        for c in to_above:
            c.start()

    @pl.when(x == 0)
    def _():
        edge_send[1] = lat[x].astype(F32)[0:1, :]
        for c in to_below:
            c.start()

    mods[0].arrived()
    total = mod_z[0]
    for k in range(1, nz):
        total = total + mod_z[k]
    mod_y[y] = total
    mods[1].start()

    ctx_copies.arrived()
    edge_send[2] = ctx[ny - 1].astype(F32)[CTX_ROWS - 1 : CTX_ROWS, :]
    edge_send[3] = ctx[0].astype(F32)[0:1, :]
    ctx_edges = [
        edge(2, 0, {"sp_0": lax.rem(z + 1, nz)}),
        edge(3, 0, {"sp_0": lax.rem(z + nz - 1, nz)}),
    ]
    for c in ctx_edges:
        c.start()

    def inverse(v):
        return lax.rsqrt(jnp.mean(v * v, axis=1, keepdims=True) + EPSILON)

    ctx_scales = [inverse(ctx[j].astype(F32)) for j in range(ny)]

    mods[1].arrived()
    total = mod_y[0]
    for k in range(1, ny):
        total = total + mod_y[k]
    mod_x[x] = total
    mods[2].start()

    lat_copies.arrived()
    scales = [inverse(lat[t].astype(F32)) for t in range(nx)]
    misc[...] = jnp.zeros_like(misc)
    for c in (to_above[0], to_below[0], *ctx_edges):
        c.wait_recv()
    has = (place > 0, place < count - 1, z > 0, z < nz - 1)
    for slot in range(4):
        misc[slot : slot + 1, :] = jnp.where(has[slot], edge_recv[slot], 0.0)
    misc_scale = inverse(misc[...])
    row16 = rows_of((16, 1))
    kept = jnp.zeros((16, 1), jnp.bool_)
    for slot in range(4):
        kept = jnp.logical_or(kept, jnp.logical_and(row16 == slot, has[slot]))
    local[0].wait()
    swaps[0].wait_recv()
    dt_wide[...] = jnp.zeros_like(dt_wide)
    for way in range(2):
        dt_wide[way * HEADS : (way + 1) * HEADS, :] = dt_rows[way].astype(F32)
    for b in range(model // LANES):
        at = slice(b * LANES, (b + 1) * LANES)
        weights[at, COL_DT:COLS] = dt_wide[:, at].T.astype(BF16)
    for i in range(1, len(pieces) - 1):
        local[i].wait()
        swaps[i].wait_recv()

    mods[2].arrived()
    for c in range(nx):
        cols = slice(c * width, (c + 1) * width)
        mod = [mod_x[c, r] for r in range(5)]
        gain = small[2:3, cols]
        scale = gain * (1.0 + mod[1])
        shift = mod[0]
        scale_ctx = gain * (1.0 + mod[4])
        shift_ctx = mod[3]
        gate[:, cols] = mod[2]
        for t in range(nx):
            value = lat[t, :, cols].astype(F32) * scales[t] * scale + shift
            hidden[t * own_rows : (t + 1) * own_rows, cols] = value.astype(BF16)
        value = misc[:, cols] * misc_scale * jnp.where(row16 < 2, scale, scale_ctx)
        value = value + jnp.where(row16 < 2, shift, shift_ctx)
        hidden[TOKENS:ctx_at, cols] = jnp.where(kept, value, 0.0).astype(BF16)
        for j in range(0, ny, 2):
            pair = [
                ctx[i, :, cols].astype(F32) * ctx_scales[i] * scale_ctx + shift_ctx
                for i in (j, j + 1)
            ]
            at = ctx_at + j * CTX_ROWS
            hidden[at : at + 2 * CTX_ROWS, cols] = jnp.concatenate(pair, axis=0).astype(BF16)

    def project(left, right):
        while left < right:
            wide = min(256, right - left)
            cols = slice(left, left + wide)
            feats[:, cols] = rounded(
                jnp.dot(hidden[...], weights[:, cols], preferred_element_type=F32)
            )
            left += wide

    project(0, COL_Z)
    project(COL_DT, COLS)

    lane = lanes_of((1, LANES))
    rates = jnp.zeros((1, LANES), F32)
    for way in range(2):
        for h in range(HEADS):
            rates = jnp.where(lane == way * HEADS + h, rate[way : way + 1, h : h + 1], rates)
    ctx_rows = slice(ctx_at, ctx_at + lines)
    for b in range((INNER + STATE) // LANES):
        cols = slice(b * LANES, (b + 1) * LANES)
        feats[ctx_rows, cols] = convolved(
            feats[ctx_rows, cols],
            feats[TOKENS + 2 : TOKENS + 3, cols],
            feats[TOKENS + 3 : TOKENS + 4, cols],
            small[4:7, cols],
        )
    ctx_b = feats[ctx_rows, INNER : INNER + STATE].T
    ctx_steps = softplus(feats[ctx_rows, COL_DT:COLS])
    ctx_sums = running_sums(-rates * ctx_steps, HEADS)
    own_slab = pl.ds(pl.multiple_of(y * slab, slab), slab)
    for way in range(2):
        for q in range(PAIRS):
            cols = slice(q * LANES, (q + 1) * LANES)
            head = way * HEADS + 2 * q
            decay = spread(ctx_sums, head)
            end = decay[lines - 1 : lines] if way == 0 else decay[0:1]
            moved_x = rounded(feats[ctx_rows, cols] * spread(ctx_steps, head))
            ctx_full[way, :, cols] = jnp.dot(
                ctx_b,
                moved_x * jnp.exp(end - decay),
                preferred_element_type=F32,
                precision=lax.Precision.HIGHEST,
            )
            ctx_dz[z, way * PAIRS + q : way * PAIRS + q + 1, :] = end
        ctx_z[z, way * slab : (way + 1) * slab, :] = ctx_full[way, own_slab, :].astype(BF16)
    ctx_dz_copies = along(
        "sp_0", nz, z, z_sems, 0, lambda peer: ctx_dz.at[z], lambda: ctx_dz.at[z]
    ).start()
    ctx_z_copies = along(
        "sp_0", nz, z, z_sems, 1, lambda peer: ctx_z.at[z], lambda: ctx_z.at[z]
    ).start()

    for b in range(MIXED // LANES):
        cols = slice(b * LANES, (b + 1) * LANES)
        feats[0:TOKENS, cols] = convolved(
            feats[0:TOKENS, cols],
            feats[TOKENS : TOKENS + 1, cols],
            feats[TOKENS + 1 : TOKENS + 2, cols],
            small[4:7, cols],
        )
    b_turned = feats[0:TOKENS, INNER : INNER + STATE].T.astype(BF16)
    c_vals = feats[0:TOKENS, INNER + STATE : MIXED].astype(BF16)
    steps = softplus(feats[0:TOKENS, COL_DT:COLS])
    sums = running_sums(-rates * steps, HEADS)
    ends = jnp.where(lane < HEADS, sums[TOKENS - 1 : TOKENS], sums[0:1])
    for way in range(2):
        for q in range(PAIRS):
            r = way * PAIRS + q
            decay_y[y, r : r + 1, :] = spread(ends, 2 * r)
    decay_copies = along(
        "sp_1", ny, y, y_sems, 1, lambda peer: decay_y.at[y], lambda: decay_y.at[y]
    ).start()
    state_copies = []
    for way in range(2):
        for q in range(PAIRS):
            cols = slice(q * LANES, (q + 1) * LANES)
            head = way * HEADS + 2 * q
            step = spread(steps, head)
            decay = spread(sums, head)
            end = decay[TOKENS - 1 : TOKENS] if way == 0 else decay[0:1]
            moved_x = rounded(feats[0:TOKENS, cols] * step)
            moved[way * TOKENS : (way + 1) * TOKENS, cols] = moved_x.astype(BF16)
            growth[way, :, cols] = jnp.exp(decay)
            at_end = (moved_x * jnp.exp(end - decay)).astype(BF16)
            state = jnp.dot(b_turned, at_end, preferred_element_type=F32).astype(BF16)
            for p in range(ny):
                state_send[way, p, :, cols] = state[p * slab : (p + 1) * slab]
        state_copies.append(
            along(
                "sp_1",
                ny,
                y,
                y_sems,
                2 + way,
                lambda peer, way=way: state_send.at[way, peer],
                lambda way=way: state_recv.at[way, y],
            ).start()
        )
        state_recv[way, y] = state_send[way, y]

    project(COL_Z, COL_DT)
    scores = jnp.dot(c_vals, b_turned, preferred_element_type=F32)
    turned = sums.T
    square = (TOKENS, TOKENS)
    lower = rows_of(square) >= lanes_of(square)
    upper = rows_of(square) <= lanes_of(square)
    for q in range(PAIRS):
        cols = slice(q * LANES, (q + 1) * LANES)
        halves = []
        for h in (2 * q, 2 * q + 1):
            both = []
            for way, mask in ((0, lower), (1, upper)):
                col = way * HEADS + h
                gap = sums[:, col : col + 1] - turned[col : col + 1, :]
                decayed = scores * jnp.exp(jnp.minimum(gap, 0.0))
                both.append(jnp.where(mask, decayed, 0.0).astype(BF16))
            halves.append(
                jnp.dot(
                    jnp.concatenate(both, axis=1),
                    moved[:, cols],
                    preferred_element_type=F32,
                )
            )
        inside[:, cols] = jnp.where(lanes_of(square) < LANES // 2, halves[0], halves[1])

    decay_copies.arrived()
    decays = [decay_y[j] for j in range(ny)]
    is_fwd = rows_of((8, LANES)) < PAIRS
    ahead = [None] * ny
    acc_f = acc_b = jnp.zeros((8, LANES), F32)
    for j in range(ny):
        ahead[j] = acc_f
        acc_f = acc_f + decays[j]
    for j in reversed(range(ny)):
        ahead[j] = jnp.exp(jnp.where(is_fwd, ahead[j], acc_b))
        acc_b = acc_b + decays[j]
    tot_dz[z] = acc_f
    tot_dz_copies = along(
        "sp_0", nz, z, z_sems, 2, lambda peer: tot_dz.at[z], lambda: tot_dz.at[z]
    ).start()
    factors = [jnp.exp(d) for d in decays]
    tot_copies = []
    for way in range(2):
        state_copies[way].arrived()
        for q in range(PAIRS):
            cols = slice(q * LANES, (q + 1) * LANES)
            r = way * PAIRS + q
            state = jnp.zeros((slab, LANES), F32)
            for j in range(ny) if way == 0 else reversed(range(ny)):
                before[way, j, :, cols] = state
                state = state * factors[j][r : r + 1] + state_recv[way, j, :, cols].astype(F32)
            tot_z[way, z, :, cols] = state.astype(BF16)
        tot_copies.append(
            along(
                "sp_0",
                nz,
                z,
                z_sems,
                3 + way,
                lambda peer, way=way: tot_z.at[way, z],
                lambda way=way: tot_z.at[way, z],
                (lambda k: z + k < nz) if way == 0 else (lambda k: z + k >= nz),
                (lambda k: z >= k) if way == 0 else (lambda k: z < k),
            ).start()
        )

    ctx_dz_copies.arrived()
    ctx_z_copies.arrived()
    ctx_factors = [jnp.exp(ctx_dz[j]) for j in range(nz)]
    tot_dz_copies.arrived()
    tot_factors = [jnp.exp(tot_dz[j]) for j in range(nz)]
    enter_copies = []
    for way in range(2):
        part = slice(way * slab, (way + 1) * slab)
        starts = []
        for q in range(PAIRS):
            cols = slice(q * LANES, (q + 1) * LANES)
            r = way * PAIRS + q
            state = jnp.zeros((slab, LANES), F32)
            for j in range(nz) if way == 0 else reversed(range(nz)):
                state = state * ctx_factors[j][r : r + 1] + ctx_z[j, part, cols].astype(F32)
            starts.append(state)
        tot_copies[way].arrived()
        for q in range(PAIRS):
            cols = slice(q * LANES, (q + 1) * LANES)
            r = way * PAIRS + q
            state = starts[q]
            for j in range(nz) if way == 0 else reversed(range(nz)):
                passed = j < z if way == 0 else j > z
                later = state * tot_factors[j][r : r + 1] + tot_z[way, j, :, cols].astype(F32)
                state = jnp.where(passed, later, state)
            for j in range(ny):
                enter_send[way, j, :, cols] = (
                    before[way, j, :, cols] + ahead[j][r : r + 1] * state
                ).astype(BF16)
        enter_copies.append(
            along(
                "sp_1",
                ny,
                y,
                y_sems,
                4 + way,
                lambda peer, way=way: enter_send.at[way, peer],
                lambda way=way: enter_recv.at[way, y],
            ).start()
        )
        enter_recv[way, y] = enter_send[way, y]

    squares = jnp.zeros((TOKENS, 1), F32)
    for way in range(2):
        enter_copies[way].arrived()
        carried = jnp.dot(
            c_vals, enter_recv[way].reshape(STATE, INNER), preferred_element_type=F32
        )
        for q in range(PAIRS):
            cols = slice(q * LANES, (q + 1) * LANES)
            value = inside[:, cols] + growth[way, :, cols] * carried[:, cols]
            if way == 1:
                at = COL_Z + q * LANES
                value = value * silu(feats[0:TOKENS, at : at + LANES])
                squares = squares + jnp.sum(value * value, axis=1, keepdims=True)
            inside[:, cols] = value
    scale = lax.rsqrt(squares / INNER + EPSILON)
    for q in range(PAIRS):
        cols = slice(q * LANES, (q + 1) * LANES)
        normed[:, cols] = (inside[:, cols] * scale * small[3:4, cols]).astype(BF16)

    local[-1].wait()
    swaps[-1].wait_recv()
    part_copies = []
    for c in range(nx):
        cols = slice(c * width, (c + 1) * width)
        term = jnp.dot(normed[...], out_weights[:, cols], preferred_element_type=F32)
        term = term.astype(BF16)
        for t in range(nx):
            part_send[t, :, cols] = term[t * own_rows : (t + 1) * own_rows]
        part_copies.append(
            along(
                "tp",
                nx,
                x,
                part_sems,
                c,
                lambda peer, cols=cols: part_send.at[peer, :, cols],
                lambda cols=cols: parts.at[x, :, cols],
            ).start()
        )
    own_part = pltpu.make_async_copy(part_send.at[x], parts.at[x], local_sem.at[7])
    own_part.start()
    for e in swaps + ctx_edges:
        e.wait_send()

    @pl.when(x == nx - 1)
    def _():
        for c in to_above:
            c.wait_send()

    @pl.when(x == 0)
    def _():
        for c in to_below:
            c.wait_send()

    done = mods + [ctx_copies, lat_copies, decay_copies, ctx_dz_copies, ctx_z_copies]
    done += [tot_dz_copies] + state_copies + tot_copies + enter_copies
    for e in done + part_copies:
        e.left()
    own_part.wait()
    for e in part_copies:
        e.arrived()


def shards(
    sizes,
    latent,
    condition,
    context,
    context_source,
    mod_weight,
    norm_gain,
    w_x,
    w_b,
    w_c,
    w_z,
    w_dt,
    conv_x,
    conv_b,
    conv_c,
    decay_rate,
    out_gain,
    w_out,
):
    nz, ny, nx = sizes
    model = latent.shape[-1]
    own_rows = latent.shape[1]
    width = model // nx
    slab = STATE // ny
    span = max(model, 1024)
    rows = mod_weight.shape[1]
    lines = ny * CTX_ROWS
    total_rows = TOKENS + 16 + lines
    vmem = pl.BlockSpec(memory_space=pltpu.VMEM)
    hbm = pl.BlockSpec(memory_space=pl.ANY)
    dma = pltpu.SemaphoreType.DMA
    most = max(nz, ny, nx) - 1
    scratch = [
        pltpu.VMEM((model, COLS), BF16),
        pltpu.VMEM((INNER, model), BF16),
        pltpu.VMEM((2, HEADS, model), BF16),
        pltpu.VMEM((LANES, model), F32),
        pltpu.VMEM((8, span), F32),
        pltpu.VMEM((nx, own_rows, model), BF16),
        pltpu.VMEM((ny, CTX_ROWS, model), BF16),
        pltpu.VMEM((3, max(rows, LANES), width), BF16),
        pltpu.VMEM((nz, 5, 1, width), F32),
        pltpu.VMEM((ny, 5, 1, width), F32),
        pltpu.VMEM((nx, 5, 1, width), F32),
        pltpu.VMEM((4, 1, model), F32),
        pltpu.VMEM((4, 1, model), F32),
        pltpu.VMEM((16, model), F32),
        pltpu.VMEM((total_rows, model), BF16),
        pltpu.VMEM((total_rows, COLS), F32),
        pltpu.VMEM((2 * TOKENS, INNER), BF16),
        pltpu.VMEM((2, TOKENS, INNER), F32),
        pltpu.VMEM((TOKENS, INNER), F32),
        pltpu.VMEM((2, STATE, INNER), F32),
        pltpu.VMEM((nz, 2 * slab, INNER), BF16),
        pltpu.VMEM((nz, 8, LANES), F32),
        pltpu.VMEM((2, ny, slab, INNER), BF16),
        pltpu.VMEM((2, ny, slab, INNER), BF16),
        pltpu.VMEM((ny, 8, LANES), F32),
        pltpu.VMEM((2, nz, slab, INNER), BF16),
        pltpu.VMEM((nz, 8, LANES), F32),
        pltpu.VMEM((2, ny, slab, INNER), F32),
        pltpu.VMEM((2, ny, slab, INNER), BF16),
        pltpu.VMEM((2, ny, slab, INNER), BF16),
        pltpu.VMEM((TOKENS, INNER), BF16),
        pltpu.VMEM((nx, own_rows, model), BF16),
        dma((8,)),
        dma((6,)),
        dma((6,)),
        dma((2, 3, most)),
        dma((2, 1, nx - 1)),
        dma((4, nx)),
        dma((4,)),
        dma((2, 6, ny - 1)),
        dma((2, 5, nz - 1)),
        dma((2, nx, nx - 1)),
    ]
    parts, gate = pl.pallas_call(
        functools.partial(mixer, (nz, ny, nx, model)),
        out_shape=(
            jax.ShapeDtypeStruct((nx, own_rows, model), BF16),
            jax.ShapeDtypeStruct((1, model), F32),
        ),
        in_specs=[vmem] * 10 + [hbm] * 7,
        out_specs=(hbm, vmem),
        scratch_shapes=scratch,
        compiler_params=pltpu.CompilerParams(
            collective_id=0, has_side_effects=True, vmem_limit_bytes=56 * 1024 * 1024
        ),
    )(
        condition,
        context_source.reshape(-1, LANES),
        norm_gain.reshape(-1, LANES),
        out_gain.reshape(-1, LANES),
        conv_x,
        conv_b,
        conv_c,
        decay_rate,
        mod_weight,
        context[0],
        latent[0],
        w_x,
        w_b,
        w_c,
        w_z,
        jnp.swapaxes(w_dt, 1, 2),
        w_out,
    )
    mixed = jnp.sum(parts.astype(F32), axis=0)
    return (gate * mixed).astype(BF16)[None]


def solution(mesh):
    nx = mesh.shape["tp"]
    ny = 8
    nz = mesh.shape["sp"] // ny
    return program(mesh, nz, ny, nx)


def program(mesh, nz, ny, nx):
    torus = Mesh(
        mesh.devices.reshape(nz, ny, nx, mesh.shape["dp"]), ("sp_0", "sp_1", "tp", "dp")
    )
    placed = (
        P("dp", SP_TP, None),
        P("dp", None),
        P("dp", SP, None),
        P(),
        P(None, SP, "tp"),
        P(),
        P("dp", "tp"),
        P("dp", "tp"),
        P("dp", "tp"),
        P("dp", "tp"),
        P(None, "dp", "tp"),
        P(None, "tp"),
        P(None, "tp"),
        P(None, "tp"),
        P(None, "tp"),
        P("tp"),
        P(("tp", "dp"), None),
    )
    return jax.shard_map(
        functools.partial(shards, (nz, ny, nx)),
        mesh=torus,
        in_specs=placed,
        out_specs=P("dp", SP_TP, None),
        check_vma=False,
    )
```

time: 75.6 us -> 62.2 us (0.82)
  local copies, waits for them, and re-layouts: 8.08 us -> 0.01 us
  Pallas kernels: 66.5 us -> 60.2 us
  other arithmetic: 0.11 us -> 1.81 us
    unnamed x19 -> x2, local copies, waits for them, and re-layouts: 6.36 us -> 0.01 us
    pallas_call x1, Pallas kernels: 66.5 us -> 60.2 us  [shards(): pl.pallas_call(functools.partial(mixer, (nz, ny, nx, model)), out_shape=(...]
    reduce_sum x0 -> x1, other arithmetic: none -> 1.14 us  [shards(): mixed = jnp.sum(parts.astype(F32), axis=0)]
    pad x1 -> x0, local copies, waits for them, and re-layouts: 0.76 us -> none  [shards(): jnp.pad(jnp.concatenate([w_dt[0], w_dt[1]], axis=1), ((0, 0), (0, LANES -...]
where the time goes in v2:
time: 62.2 us; the launch traced here: 62.1 us
  Pallas kernels  60.2 us (97%)
  other arithmetic  1.81 us (3%)
    pallas_call x1, Pallas kernels, shards(): pl.pallas_call(functools.partial(mixer, (nz, ny, nx, model)), out_shape=(...  60.2 us

profile of v2, /device:TPU:6, one launch (start us, length us, event | category | flops | bytes accessed | tf_op | source)
XLA Modules:
  0.0 62.1 jit_solution(17838671137303763900)
XLA Ops:
  0.0 60.2 %shard_map.163 = (bf16[4,32,2048]{2,1,0:T(8,128)(2,1)}, f32[1,2048]{1,0:T(1,128)}) custom-call(bf16[1,2048]{1,0:T(2,128)(2,1)} %condition.1, bf16[16,128]{1,0:T(8,128)(2,1)} %bitcast.15, bf16[16,128]{1,0:T(8,128)(2,1)} %bitcast.16, bf16[4,128]{1,0:T(4,128)(2,1)} %bitcast.17, bf16[3,512]{1,0:T(4,128)(2,1)} %conv_x.1, bf16[3,128]{1,0:T(4,128)(2,1)} %conv_b.1, ...), custom_call_target="tpu_custom_call" | custom-call | tf_op jit(solution)/shard_map/pallas_call | solution.py:756
  60.2 0.0 copy-start
  60.2 1.1 %convert_reduce_fusion = f32[32,2048]{1,0:T(8,128)S(1)} fusion(bf16[4,32,2048]{2,1,0:T(8,128)(2,1)} %get-tuple-element.8), kind=kLoop, calls=%fused_computation | loop fusion | flops 458752 | bytes 786432 | tf_op jit(solution)/shard_map/reduce_sum | solution.py:787
  61.4 0.0 copy-done
  61.4 0.7 %fusion = bf16[1,32,2048]{2,1,0:T(8,128)(2,1)} fusion(f32[32,2048]{1,0:T(8,128)S(1)} %convert_reduce_fusion, f32[2048]{0:T(1024)S(1)} %bitcast.14), kind=kLoop, calls=%fused_computation.2 | loop fusion | flops 131072 | bytes 401408 | tf_op jit(solution)/shard_map/convert_element_type | solution.py:788
Async XLA Ops:
  60.2 1.2 %copy-start = (f32[1,2048]{1,0:T(1,128)S(1)}, f32[1,2048]{1,0:T(1,128)}, u32[]{:S(2)}) copy-start(f32[1,2048]{1,0:T(1,128)} %get-tuple-element.7) | copy-start | bytes 24580

commit v3 on v2

--- a/solution.py
+++ b/solution.py
@@ -21,9 +21,11 @@
 PAIRS = HEADS // 2
 INNER = 512
 MIXED = INNER + 2 * STATE
-COL_Z = MIXED
-COL_DT = COL_Z + INNER
-COLS = COL_DT + LANES
+COL_B = INNER
+COL_DT = COL_B + STATE
+COL_C = COL_DT + LANES
+COL_Z = COL_C + STATE
+COLS = COL_Z + INNER
 CTX_ROWS = 8
 
 
@@ -76,38 +78,64 @@
 
 
 class Exchange:
-    def __init__(self, axis, size, place, source, target, sent, got, sends=None, gets=None):
-        self.sends, self.gets = sends, gets
-        self.copies = []
+    def __init__(self, axis, size, place, source, target, sems, bulk):
+        def copy(peer, origin, end):
+            return pltpu.make_async_remote_copy(
+                src_ref=origin,
+                dst_ref=end,
+                send_sem=sems.at[0],
+                recv_sem=sems.at[1],
+                device_id={axis: peer},
+                device_id_type=MESH,
+            )
+
+        peers = [lax.rem(place + k, size) for k in range(1, size)]
+        self.copies = [copy(peer, source(peer), target) for peer in peers]
+        self.whole = copy(peers[0], bulk, bulk)
+
+    def start(self):
+        for c in self.copies:
+            c.start()
+        return self
+
+    def arrived(self):
+        self.whole.wait_recv()
+
+    def left(self):
+        self.whole.wait_send()
+
+
+class Totals:
+    def __init__(self, way, buf, size, place, sems):
+        self.sends, self.gets, self.copies = [], [], []
         for k in range(1, size):
-            peer = lax.rem(place + k, size)
+            later = place + k < size
+            passed = place >= k
+            self.sends.append(later if way == 0 else jnp.logical_not(later))
+            self.gets.append(passed if way == 0 else jnp.logical_not(passed))
             self.copies.append(
                 pltpu.make_async_remote_copy(
-                    src_ref=source(peer),
-                    dst_ref=target(),
-                    send_sem=sent(k - 1),
-                    recv_sem=got(k - 1),
-                    device_id={axis: peer},
+                    src_ref=buf.at[way, place],
+                    dst_ref=buf.at[way, place],
+                    send_sem=sems.at[0, k - 1],
+                    recv_sem=sems.at[1, k - 1],
+                    device_id={"sp_0": lax.rem(place + k, size)},
                     device_id_type=MESH,
                 )
             )
 
-    def each(self, taken, act):
-        for k, c in enumerate(self.copies, 1):
-            if taken is None:
-                act(c)
-            else:
-                pl.when(taken(k))(functools.partial(act, c))
-
     def start(self):
-        self.each(self.sends, lambda c: c.start())
+        for taken, c in zip(self.sends, self.copies):
+            pl.when(taken)(c.start)
         return self
 
     def arrived(self):
-        self.each(self.gets, lambda c: c.wait_recv())
+        for taken, c in zip(self.gets, self.copies):
+            pl.when(taken)(c.wait_recv)
 
     def left(self):
-        self.each(self.sends, lambda c: c.wait_send())
+        for taken, c in zip(self.sends, self.copies):
+            pl.when(taken)(c.wait_send)
 
 
 def mixer(
@@ -166,13 +194,10 @@
     local_sem,
     core_send,
     core_recv,
-    mod_sems,
-    lat_sems,
+    pair_sems,
     edge_sems,
     edge_got,
-    y_sems,
-    z_sems,
-    part_sems,
+    tot_sems,
 ):
     nz, ny, nx, model = dims
     width = model // nx
@@ -187,7 +212,7 @@
     place = z * ny + y
     count = nz * ny
 
-    own_latent = pltpu.make_async_copy(latent, lat.at[x], local_sem.at[6])
+    own_latent = pltpu.make_async_copy(latent, lat.at[x], local_sem.at[3])
     own_latent.start()
     half = model // 2
     own_half = pl.ds(pl.multiple_of(core * half, half), half)
@@ -195,14 +220,21 @@
     pieces = (
         (w_dt, dt_rows.at[:, :, own_half]),
         (w_x, weights.at[own_half, pl.ds(0, INNER)]),
-        (w_b, weights.at[own_half, pl.ds(INNER, STATE)]),
-        (w_c, weights.at[own_half, pl.ds(INNER + STATE, STATE)]),
+        (w_b, weights.at[own_half, pl.ds(COL_B, STATE)]),
+        (w_c, weights.at[own_half, pl.ds(COL_C, STATE)]),
         (w_z, weights.at[own_half, pl.ds(COL_Z, INNER)]),
         (w_out, out_weights.at[out_half, :]),
     )
+    groups = (0, 1, 1, 1, 1, 2)
     local = [
         pltpu.make_async_copy(origin, target, local_sem.at[i])
-        for i, (origin, target) in enumerate(pieces)
+        for i, (origin, target) in zip(groups, pieces)
+    ]
+    in_bulk = weights.at[own_half, pl.ds(0, COLS - LANES)]
+    bulk_local = [
+        local[0],
+        pltpu.make_async_copy(in_bulk, in_bulk, local_sem.at[1]),
+        local[-1],
     ]
     barrier = pltpu.get_barrier_semaphore()
     up_place = lax.rem(place + 1, count)
@@ -218,15 +250,13 @@
     for peer in peers:
         pl.semaphore_signal(barrier, inc=1, device_id=peer, device_id_type=MESH)
 
-    small[...] = jnp.zeros_like(small)
-    for r, ref in ((1, source), (2, gain_in), (3, out_gain)):
+    def unpack(r, ref):
         piece = ref[...].astype(F32)
         for k in range(piece.shape[0]):
             small[r : r + 1, k * LANES : (k + 1) * LANES] = piece[k : k + 1]
+
+    unpack(1, source)
     small[0:1, 0:model] = condition[...].astype(F32)
-    small[4:7, 0:INNER] = conv_x[...].astype(F32)
-    small[4:7, INNER : INNER + STATE] = conv_b[...].astype(F32)
-    small[4:7, INNER + STATE : MIXED] = conv_c[...].astype(F32)
 
     rows = modw.shape[1]
     chunk = placed.shape[1]
@@ -247,43 +277,29 @@
             left.astype(BF16), placed[k], preferred_element_type=F32
         )
     for r in range(5):
-        mod_z[z, r] = partial[r : r + 1]
+        mod_y[y, r] = partial[r : r + 1]
 
     pl.semaphore_wait(barrier, len(peers))
+    pairs = iter(range(32))
+
+    def along(axis, size, me, origin, target, bulk):
+        return Exchange(axis, size, me, origin, target, pair_sems.at[next(pairs)], bulk)
+
+    def gather(axis, size, me, buf):
+        own = buf.at[me]
+        return along(axis, size, me, lambda peer: own, own, buf.at[pl.ds(0, size - 1)])
+
     mods = [
-        Exchange(
-            axis,
-            size,
-            me,
-            lambda peer, buf=buf, me=me: buf.at[me],
-            lambda buf=buf, me=me: buf.at[me],
-            lambda k, i=i: mod_sems.at[0, i, k],
-            lambda k, i=i: mod_sems.at[1, i, k],
-        )
-        for i, (axis, size, me, buf) in enumerate(
-            (("sp_0", nz, z, mod_z), ("sp_1", ny, y, mod_y), ("tp", nx, x, mod_x))
-        )
+        gather("sp_1", ny, y, mod_y),
+        gather("sp_0", nz, z, mod_z),
+        gather("tp", nx, x, mod_x),
     ]
-
-    def along(axis, size, me, sems, index, origin, target, sends=None, gets=None):
-        return Exchange(
-            axis,
-            size,
-            me,
-            origin,
-            target,
-            lambda k: sems.at[0, index, k],
-            lambda k: sems.at[1, index, k],
-            sends,
-            gets,
-        )
-
     mods[0].start()
     ctx_copies = along(
-        "sp_1", ny, y, y_sems, 0, lambda peer: context, lambda: ctx.at[y]
+        "sp_1", ny, y, lambda peer: context, ctx.at[y], ctx.at[pl.ds(0, ny - 1)]
     ).start()
     lat_copies = along(
-        "tp", nx, x, lat_sems, 0, lambda peer: latent, lambda: lat.at[x]
+        "tp", nx, x, lambda peer: latent, lat.at[x], lat.at[pl.ds(0, nx - 1)]
     ).start()
     swaps = [
         pltpu.make_async_remote_copy(
@@ -294,7 +310,19 @@
             device_id={"dp": 1 - core},
             device_id_type=MESH,
         )
-        for i, (origin, target) in enumerate(pieces)
+        for i, (origin, target) in zip(groups, pieces)
+    ]
+    bulk_swaps = [
+        swaps[0],
+        pltpu.make_async_remote_copy(
+            src_ref=in_bulk,
+            dst_ref=in_bulk,
+            send_sem=core_send.at[1],
+            recv_sem=core_recv.at[1],
+            device_id={"dp": 1 - core},
+            device_id_type=MESH,
+        ),
+        swaps[-1],
     ]
     for c, d in zip(swaps, local):
         c.start()
@@ -327,12 +355,34 @@
         for c in to_below:
             c.start()
 
+    small[2:7, :] = jnp.zeros((5, small.shape[1]), F32)
+    unpack(2, gain_in)
+    unpack(3, out_gain)
+    small[4:7, 0:INNER] = conv_x[...].astype(F32)
+    small[4:7, INNER : INNER + STATE] = conv_b[...].astype(F32)
+    small[4:7, INNER + STATE : MIXED] = conv_c[...].astype(F32)
+    lane = lanes_of((1, LANES))
+    rates = jnp.zeros((1, LANES), F32)
+    for way in range(2):
+        for h in range(HEADS):
+            rates = jnp.where(lane == way * HEADS + h, rate[way : way + 1, h : h + 1], rates)
+
     mods[0].arrived()
+    total = mod_y[0]
+    for k in range(1, ny):
+        total = total + mod_y[k]
+    mod_z[z] = total
+    mods[1].start()
+
+    def inverse(v):
+        return lax.rsqrt(jnp.mean(v * v, axis=1, keepdims=True) + EPSILON)
+
+    mods[1].arrived()
     total = mod_z[0]
     for k in range(1, nz):
         total = total + mod_z[k]
-    mod_y[y] = total
-    mods[1].start()
+    mod_x[x] = total
+    mods[2].start()
 
     ctx_copies.arrived()
     edge_send[2] = ctx[ny - 1].astype(F32)[CTX_ROWS - 1 : CTX_ROWS, :]
@@ -344,95 +394,136 @@
     for c in ctx_edges:
         c.start()
 
-    def inverse(v):
-        return lax.rsqrt(jnp.mean(v * v, axis=1, keepdims=True) + EPSILON)
-
-    ctx_scales = [inverse(ctx[j].astype(F32)) for j in range(ny)]
-
-    mods[1].arrived()
-    total = mod_y[0]
-    for k in range(1, ny):
-        total = total + mod_y[k]
-    mod_x[x] = total
-    mods[2].start()
-
     lat_copies.arrived()
     scales = [inverse(lat[t].astype(F32)) for t in range(nx)]
     misc[...] = jnp.zeros_like(misc)
-    for c in (to_above[0], to_below[0], *ctx_edges):
+    for c in (to_above[0], to_below[0]):
         c.wait_recv()
     has = (place > 0, place < count - 1, z > 0, z < nz - 1)
-    for slot in range(4):
+    for slot in range(2):
         misc[slot : slot + 1, :] = jnp.where(has[slot], edge_recv[slot], 0.0)
-    misc_scale = inverse(misc[...])
-    row16 = rows_of((16, 1))
-    kept = jnp.zeros((16, 1), jnp.bool_)
-    for slot in range(4):
-        kept = jnp.logical_or(kept, jnp.logical_and(row16 == slot, has[slot]))
-    local[0].wait()
-    swaps[0].wait_recv()
+    misc_scale = inverse(misc[0:8, :])
+    row8 = rows_of((8, 1))
+
+    def kept(low, high):
+        return jnp.logical_or(
+            jnp.logical_and(row8 == 0, low), jnp.logical_and(row8 == 1, high)
+        )
+
+    bulk_local[0].wait()
+    bulk_swaps[0].wait_recv()
     dt_wide[...] = jnp.zeros_like(dt_wide)
     for way in range(2):
         dt_wide[way * HEADS : (way + 1) * HEADS, :] = dt_rows[way].astype(F32)
     for b in range(model // LANES):
         at = slice(b * LANES, (b + 1) * LANES)
-        weights[at, COL_DT:COLS] = dt_wide[:, at].T.astype(BF16)
-    for i in range(1, len(pieces) - 1):
-        local[i].wait()
-        swaps[i].wait_recv()
+        weights[at, COL_DT:COL_C] = dt_wide[:, at].T.astype(BF16)
+    bulk_local[1].wait()
+    bulk_swaps[1].wait_recv()
 
     mods[2].arrived()
+
+    def modulations(c, shift, scale):
+        cols = slice(c * width, (c + 1) * width)
+        return cols, small[2:3, cols] * (1.0 + mod_x[c, scale]), mod_x[c, shift]
+
+    def edge_rows(cols, scale, shift, known, at):
+        value = misc[at : at + 8, cols] * misc_scale * scale + shift
+        value = jnp.where(known, value, 0.0)
+        return jnp.concatenate([value, jnp.zeros_like(value)], axis=0).astype(BF16)
+
     for c in range(nx):
-        cols = slice(c * width, (c + 1) * width)
-        mod = [mod_x[c, r] for r in range(5)]
-        gain = small[2:3, cols]
-        scale = gain * (1.0 + mod[1])
-        shift = mod[0]
-        scale_ctx = gain * (1.0 + mod[4])
-        shift_ctx = mod[3]
-        gate[:, cols] = mod[2]
+        cols, scale, shift = modulations(c, 0, 1)
         for t in range(nx):
             value = lat[t, :, cols].astype(F32) * scales[t] * scale + shift
             hidden[t * own_rows : (t + 1) * own_rows, cols] = value.astype(BF16)
-        value = misc[:, cols] * misc_scale * jnp.where(row16 < 2, scale, scale_ctx)
-        value = value + jnp.where(row16 < 2, shift, shift_ctx)
-        hidden[TOKENS:ctx_at, cols] = jnp.where(kept, value, 0.0).astype(BF16)
+        hidden[TOKENS:ctx_at, cols] = edge_rows(cols, scale, shift, kept(has[0], has[1]), 0)
+
+    def project(rows, left, right):
+        while left < right:
+            wide = min(256, right - left)
+            cols = slice(left, left + wide)
+            feats[rows, cols] = rounded(
+                jnp.dot(hidden[rows, :], weights[:, cols], preferred_element_type=F32)
+            )
+            left += wide
+
+    def smooth(rows, low, at, tap_at):
+        cols = slice(at, at + LANES)
+        feats[rows, cols] = convolved(
+            feats[rows, cols],
+            feats[low : low + 1, cols],
+            feats[low + 1 : low + 2, cols],
+            small[4:7, tap_at : tap_at + LANES],
+        )
+
+    own = slice(0, TOKENS)
+    project(slice(0, ctx_at), 0, COL_C)
+    for at in range(0, COL_DT, LANES):
+        smooth(own, TOKENS, at, at)
+    b_turned = feats[own, COL_B:COL_DT].T.astype(BF16)
+    steps = softplus(feats[own, COL_DT:COL_C])
+    sums = running_sums(-rates * steps, HEADS)
+    ends = jnp.where(lane < HEADS, sums[TOKENS - 1 : TOKENS], sums[0:1])
+    for way in range(2):
+        for q in range(PAIRS):
+            r = way * PAIRS + q
+            decay_y[y, r : r + 1, :] = spread(ends, 2 * r)
+    decay_copies = gather("sp_1", ny, y, decay_y).start()
+
+    def slabs(axis, size, me, origin, target, way):
+        return along(
+            axis,
+            size,
+            me,
+            lambda peer: origin.at[way, peer],
+            target.at[way, me],
+            target.at[way, pl.ds(0, size - 1)],
+        )
+
+    state_copies = []
+    for way in range(2):
+        for q in range(PAIRS):
+            cols = slice(q * LANES, (q + 1) * LANES)
+            head = way * HEADS + 2 * q
+            step = spread(steps, head)
+            decay = spread(sums, head)
+            end = decay[TOKENS - 1 : TOKENS] if way == 0 else decay[0:1]
+            moved_x = rounded(feats[own, cols] * step)
+            moved[way * TOKENS : (way + 1) * TOKENS, cols] = moved_x.astype(BF16)
+            growth[way, :, cols] = jnp.exp(decay)
+            at_end = (moved_x * jnp.exp(end - decay)).astype(BF16)
+            state = jnp.dot(b_turned, at_end, preferred_element_type=F32).astype(BF16)
+            for p in range(ny):
+                state_send[way, p, :, cols] = state[p * slab : (p + 1) * slab]
+        state_copies.append(slabs("sp_1", ny, y, state_send, state_recv, way).start())
+        state_recv[way, y] = state_send[way, y]
+
+    project(slice(0, ctx_at), COL_C, COL_Z)
+
+    for c in ctx_edges:
+        c.wait_recv()
+    for slot in (2, 3):
+        at = 6 + slot
+        misc[at : at + 1, :] = jnp.where(has[slot], edge_recv[slot], 0.0)
+    misc_scale = inverse(misc[8:16, :])
+    ctx_scales = [inverse(ctx[j].astype(F32)) for j in range(ny)]
+    for c in range(nx):
+        cols, scale, shift = modulations(c, 3, 4)
+        hidden[TOKENS:ctx_at, cols] = edge_rows(cols, scale, shift, kept(has[2], has[3]), 8)
         for j in range(0, ny, 2):
-            pair = [
-                ctx[i, :, cols].astype(F32) * ctx_scales[i] * scale_ctx + shift_ctx
+            two = [
+                ctx[i, :, cols].astype(F32) * ctx_scales[i] * scale + shift
                 for i in (j, j + 1)
             ]
             at = ctx_at + j * CTX_ROWS
-            hidden[at : at + 2 * CTX_ROWS, cols] = jnp.concatenate(pair, axis=0).astype(BF16)
-
-    def project(left, right):
-        while left < right:
-            wide = min(256, right - left)
-            cols = slice(left, left + wide)
-            feats[:, cols] = rounded(
-                jnp.dot(hidden[...], weights[:, cols], preferred_element_type=F32)
-            )
-            left += wide
-
-    project(0, COL_Z)
-    project(COL_DT, COLS)
-
-    lane = lanes_of((1, LANES))
-    rates = jnp.zeros((1, LANES), F32)
-    for way in range(2):
-        for h in range(HEADS):
-            rates = jnp.where(lane == way * HEADS + h, rate[way : way + 1, h : h + 1], rates)
+            hidden[at : at + 2 * CTX_ROWS, cols] = jnp.concatenate(two, axis=0).astype(BF16)
+    project(slice(TOKENS, ctx_at + lines), 0, COL_C)
     ctx_rows = slice(ctx_at, ctx_at + lines)
-    for b in range((INNER + STATE) // LANES):
-        cols = slice(b * LANES, (b + 1) * LANES)
-        feats[ctx_rows, cols] = convolved(
-            feats[ctx_rows, cols],
-            feats[TOKENS + 2 : TOKENS + 3, cols],
-            feats[TOKENS + 3 : TOKENS + 4, cols],
-            small[4:7, cols],
-        )
-    ctx_b = feats[ctx_rows, INNER : INNER + STATE].T
-    ctx_steps = softplus(feats[ctx_rows, COL_DT:COLS])
+    for at in range(0, COL_DT, LANES):
+        smooth(ctx_rows, TOKENS, at, at)
+    ctx_b = feats[ctx_rows, COL_B:COL_DT].T
+    ctx_steps = softplus(feats[ctx_rows, COL_DT:COL_C])
     ctx_sums = running_sums(-rates * ctx_steps, HEADS)
     own_slab = pl.ds(pl.multiple_of(y * slab, slab), slab)
     for way in range(2):
@@ -450,62 +541,16 @@
             )
             ctx_dz[z, way * PAIRS + q : way * PAIRS + q + 1, :] = end
         ctx_z[z, way * slab : (way + 1) * slab, :] = ctx_full[way, own_slab, :].astype(BF16)
-    ctx_dz_copies = along(
-        "sp_0", nz, z, z_sems, 0, lambda peer: ctx_dz.at[z], lambda: ctx_dz.at[z]
-    ).start()
-    ctx_z_copies = along(
-        "sp_0", nz, z, z_sems, 1, lambda peer: ctx_z.at[z], lambda: ctx_z.at[z]
-    ).start()
-
-    for b in range(MIXED // LANES):
-        cols = slice(b * LANES, (b + 1) * LANES)
-        feats[0:TOKENS, cols] = convolved(
-            feats[0:TOKENS, cols],
-            feats[TOKENS : TOKENS + 1, cols],
-            feats[TOKENS + 1 : TOKENS + 2, cols],
-            small[4:7, cols],
-        )
-    b_turned = feats[0:TOKENS, INNER : INNER + STATE].T.astype(BF16)
-    c_vals = feats[0:TOKENS, INNER + STATE : MIXED].astype(BF16)
-    steps = softplus(feats[0:TOKENS, COL_DT:COLS])
-    sums = running_sums(-rates * steps, HEADS)
-    ends = jnp.where(lane < HEADS, sums[TOKENS - 1 : TOKENS], sums[0:1])
-    for way in range(2):
-        for q in range(PAIRS):
-            r = way * PAIRS + q
-            decay_y[y, r : r + 1, :] = spread(ends, 2 * r)
-    decay_copies = along(
-        "sp_1", ny, y, y_sems, 1, lambda peer: decay_y.at[y], lambda: decay_y.at[y]
-    ).start()
-    state_copies = []
-    for way in range(2):
-        for q in range(PAIRS):
-            cols = slice(q * LANES, (q + 1) * LANES)
-            head = way * HEADS + 2 * q
-            step = spread(steps, head)
-            decay = spread(sums, head)
-            end = decay[TOKENS - 1 : TOKENS] if way == 0 else decay[0:1]
-            moved_x = rounded(feats[0:TOKENS, cols] * step)
-            moved[way * TOKENS : (way + 1) * TOKENS, cols] = moved_x.astype(BF16)
-            growth[way, :, cols] = jnp.exp(decay)
-            at_end = (moved_x * jnp.exp(end - decay)).astype(BF16)
-            state = jnp.dot(b_turned, at_end, preferred_element_type=F32).astype(BF16)
-            for p in range(ny):
-                state_send[way, p, :, cols] = state[p * slab : (p + 1) * slab]
-        state_copies.append(
-            along(
-                "sp_1",
-                ny,
-                y,
-                y_sems,
-                2 + way,
-                lambda peer, way=way: state_send.at[way, peer],
-                lambda way=way: state_recv.at[way, y],
-            ).start()
-        )
-        state_recv[way, y] = state_send[way, y]
-
-    project(COL_Z, COL_DT)
+    ctx_dz_copies = gather("sp_0", nz, z, ctx_dz).start()
+    ctx_z_copies = gather("sp_0", nz, z, ctx_z).start()
+
+    smooth(own, TOKENS, COL_C, INNER + STATE)
+    c_vals = feats[own, COL_C:COL_Z].astype(BF16)
+    project(own, COL_Z, COLS)
+    for at in range(COL_Z, COLS, LANES):
+        feats[own, at : at + LANES] = silu(feats[own, at : at + LANES])
+    for c in range(nx):
+        gate[:, c * width : (c + 1) * width] = mod_x[c, 2]
     scores = jnp.dot(c_vals, b_turned, preferred_element_type=F32)
     turned = sums.T
     square = (TOKENS, TOKENS)
@@ -542,9 +587,7 @@
         ahead[j] = jnp.exp(jnp.where(is_fwd, ahead[j], acc_b))
         acc_b = acc_b + decays[j]
     tot_dz[z] = acc_f
-    tot_dz_copies = along(
-        "sp_0", nz, z, z_sems, 2, lambda peer: tot_dz.at[z], lambda: tot_dz.at[z]
-    ).start()
+    tot_dz_copies = gather("sp_0", nz, z, tot_dz).start()
     factors = [jnp.exp(d) for d in decays]
     tot_copies = []
     for way in range(2):
@@ -557,19 +600,7 @@
                 before[way, j, :, cols] = state
                 state = state * factors[j][r : r + 1] + state_recv[way, j, :, cols].astype(F32)
             tot_z[way, z, :, cols] = state.astype(BF16)
-        tot_copies.append(
-            along(
-                "sp_0",
-                nz,
-                z,
-                z_sems,
-                3 + way,
-                lambda peer, way=way: tot_z.at[way, z],
-                lambda way=way: tot_z.at[way, z],
-                (lambda k: z + k < nz) if way == 0 else (lambda k: z + k >= nz),
-                (lambda k: z >= k) if way == 0 else (lambda k: z < k),
-            ).start()
-        )
+        tot_copies.append(Totals(way, tot_z, nz, z, tot_sems).start())
 
     ctx_dz_copies.arrived()
     ctx_z_copies.arrived()
@@ -600,17 +631,7 @@
                 enter_send[way, j, :, cols] = (
                     before[way, j, :, cols] + ahead[j][r : r + 1] * state
                 ).astype(BF16)
-        enter_copies.append(
-            along(
-                "sp_1",
-                ny,
-                y,
-                y_sems,
-                4 + way,
-                lambda peer, way=way: enter_send.at[way, peer],
-                lambda way=way: enter_recv.at[way, y],
-            ).start()
-        )
+        enter_copies.append(slabs("sp_1", ny, y, enter_send, enter_recv, way).start())
         enter_recv[way, y] = enter_send[way, y]
 
     squares = jnp.zeros((TOKENS, 1), F32)
@@ -624,7 +645,7 @@
             value = inside[:, cols] + growth[way, :, cols] * carried[:, cols]
             if way == 1:
                 at = COL_Z + q * LANES
-                value = value * silu(feats[0:TOKENS, at : at + LANES])
+                value = value * feats[own, at : at + LANES]
                 squares = squares + jnp.sum(value * value, axis=1, keepdims=True)
             inside[:, cols] = value
     scale = lax.rsqrt(squares / INNER + EPSILON)
@@ -632,8 +653,8 @@
         cols = slice(q * LANES, (q + 1) * LANES)
         normed[:, cols] = (inside[:, cols] * scale * small[3:4, cols]).astype(BF16)
 
-    local[-1].wait()
-    swaps[-1].wait_recv()
+    bulk_local[-1].wait()
+    bulk_swaps[-1].wait_recv()
     part_copies = []
     for c in range(nx):
         cols = slice(c * width, (c + 1) * width)
@@ -646,15 +667,14 @@
                 "tp",
                 nx,
                 x,
-                part_sems,
-                c,
                 lambda peer, cols=cols: part_send.at[peer, :, cols],
-                lambda cols=cols: parts.at[x, :, cols],
+                parts.at[x, :, cols],
+                parts.at[pl.ds(0, nx - 1), :, cols],
             ).start()
         )
-    own_part = pltpu.make_async_copy(part_send.at[x], parts.at[x], local_sem.at[7])
+    own_part = pltpu.make_async_copy(part_send.at[x], parts.at[x], local_sem.at[4])
     own_part.start()
-    for e in swaps + ctx_edges:
+    for e in bulk_swaps + ctx_edges:
         e.wait_send()
 
     @pl.when(x == nx - 1)
@@ -708,7 +728,6 @@
     vmem = pl.BlockSpec(memory_space=pltpu.VMEM)
     hbm = pl.BlockSpec(memory_space=pl.ANY)
     dma = pltpu.SemaphoreType.DMA
-    most = max(nz, ny, nx) - 1
     scratch = [
         pltpu.VMEM((model, COLS), BF16),
         pltpu.VMEM((INNER, model), BF16),
@@ -742,16 +761,13 @@
         pltpu.VMEM((2, ny, slab, INNER), BF16),
         pltpu.VMEM((TOKENS, INNER), BF16),
         pltpu.VMEM((nx, own_rows, model), BF16),
-        dma((8,)),
-        dma((6,)),
-        dma((6,)),
-        dma((2, 3, most)),
-        dma((2, 1, nx - 1)),
+        dma((5,)),
+        dma((3,)),
+        dma((3,)),
+        dma((13 + nx, 2)),
         dma((4, nx)),
         dma((4,)),
-        dma((2, 6, ny - 1)),
-        dma((2, 5, nz - 1)),
-        dma((2, nx, nx - 1)),
+        dma((2, nz - 1)),
     ]
     parts, gate = pl.pallas_call(
         functools.partial(mixer, (nz, ny, nx, model)),
@@ -784,7 +800,9 @@
         jnp.swapaxes(w_dt, 1, 2),
         w_out,
     )
-    mixed = jnp.sum(parts.astype(F32), axis=0)
+    mixed = parts[0].astype(F32)
+    for k in range(1, nx):
+        mixed = mixed + parts[k].astype(F32)
     return (gate * mixed).astype(BF16)[None]
 
 

time: 62.2 us -> 59.2 us (0.952); the launches traced: 62.1 us -> 58.4 us
  Pallas kernels: 60.2 us -> 56.5 us
    pallas_call x1, Pallas kernels: 60.2 us -> 56.5 us  [shards(): pl.pallas_call(functools.partial(mixer, (nz, ny, nx, model)), out_shape=(...]
    convert_element_type x1, other arithmetic: 0.67 us -> 1.83 us  [shards(): return (gate * mixed).astype(BF16)[None]]
    reduce_sum x1 -> x0, other arithmetic: 1.14 us -> none  [shards(): mixed = jnp.sum(parts.astype(F32), axis=0)]
where the time goes in v3:
time: 59.2 us; the launch traced here: 58.4 us
  Pallas kernels  56.5 us (95%)
  other arithmetic  1.83 us (3%)
    pallas_call x1, Pallas kernels, shards(): pl.pallas_call(functools.partial(mixer, (nz, ny, nx, model)), out_shape=(...  56.5 us
    convert_element_type x1, other arithmetic, shards(): return (gate * mixed).astype(BF16)[None]  1.83 us

profile of v3, /device:TPU:6, one launch (start us, length us, event | category | flops | bytes accessed | tf_op | source)
XLA Modules:
  0.0 58.4 jit_solution(16338198117020384986)
XLA Ops:
  0.0 56.5 %shard_map.163 = (bf16[4,32,2048]{2,1,0:T(8,128)(2,1)}, f32[1,2048]{1,0:T(1,128)}) custom-call(bf16[1,2048]{1,0:T(2,128)(2,1)} %condition.1, bf16[16,128]{1,0:T(8,128)(2,1)} %bitcast.11, bf16[16,128]{1,0:T(8,128)(2,1)} %bitcast.12, bf16[4,128]{1,0:T(4,128)(2,1)} %bitcast.13, bf16[3,512]{1,0:T(4,128)(2,1)} %conv_x.1, bf16[3,128]{1,0:T(4,128)(2,1)} %conv_b.1, ...), custom_call_target="tpu_custom_call" | custom-call | tf_op jit(solution)/shard_map/pallas_call | solution.py:772
  56.5 1.8 %multiply_convert_fusion = bf16[1,32,2048]{2,1,0:T(8,128)(2,1)} fusion(bf16[4,32,2048]{2,1,0:T(8,128)(2,1)} %get-tuple-element.8, f32[2048]{0:T(1024)} %bitcast.10), kind=kLoop, calls=%fused_computation | loop fusion | flops 589824 | bytes 663552 | tf_op jit(solution)/shard_map/convert_element_type | solution.py:806

commit v4 on v3

--- a/solution.py
+++ b/solution.py
@@ -26,6 +26,7 @@
 COL_C = COL_DT + LANES
 COL_Z = COL_C + STATE
 COLS = COL_Z + INNER
+PIECE = 2 * LANES
 CTX_ROWS = 8
 
 
@@ -115,8 +116,8 @@
             self.gets.append(passed if way == 0 else jnp.logical_not(passed))
             self.copies.append(
                 pltpu.make_async_remote_copy(
-                    src_ref=buf.at[way, place],
-                    dst_ref=buf.at[way, place],
+                    src_ref=buf.at[place],
+                    dst_ref=buf.at[place],
                     send_sem=sems.at[0, k - 1],
                     recv_sem=sems.at[1, k - 1],
                     device_id={"sp_0": lax.rem(place + k, size)},
@@ -140,15 +141,15 @@
 
 def mixer(
     dims,
-    condition,
-    source,
+    condition_in,
+    source_in,
     gain_in,
-    out_gain,
-    conv_x,
-    conv_b,
-    conv_c,
-    rate,
-    modw,
+    out_gain_in,
+    conv_x_in,
+    conv_b_in,
+    conv_c_in,
+    rate_in,
+    modw_in,
     context,
     latent,
     w_x,
@@ -159,6 +160,15 @@
     w_out,
     parts,
     gate,
+    condition,
+    source,
+    gain,
+    out_gain,
+    conv_x,
+    conv_b,
+    conv_c,
+    rate,
+    modw,
     weights,
     out_weights,
     dt_rows,
@@ -178,7 +188,7 @@
     moved,
     growth,
     inside,
-    ctx_full,
+    ctx_bt,
     ctx_z,
     ctx_dz,
     state_send,
@@ -212,8 +222,43 @@
     place = z * ny + y
     count = nz * ny
 
+    barrier = pltpu.get_barrier_semaphore()
+    up_place = lax.rem(place + 1, count)
+    down_place = lax.rem(place + count - 1, count)
+    above = {"sp_0": up_place // ny, "sp_1": lax.rem(up_place, ny)}
+    below = {"sp_0": down_place // ny, "sp_1": lax.rem(down_place, ny)}
+    peers = [{"sp_1": lax.rem(y + k, ny)} for k in range(1, ny)]
+    peers += [{"sp_0": lax.rem(z + k, nz)} for k in range(1, nz)]
+    peers += [{"tp": lax.rem(x + k, nx)} for k in range(1, nx)]
+    peers += [{"dp": 1 - core}]
+    for k in range(nx):
+        peers += [dict(above, tp=k), dict(below, tp=k)]
+    for peer in peers:
+        pl.semaphore_signal(barrier, inc=1, device_id=peer, device_id_type=MESH)
+
+    loads = [
+        pltpu.make_async_copy(origin, target, local_sem.at[5 + i])
+        for i, (origin, target) in enumerate(
+            (
+                (modw_in, modw),
+                (condition_in, condition),
+                (source_in, source),
+                (gain_in, gain),
+                (out_gain_in, out_gain),
+                (conv_x_in, conv_x),
+                (conv_b_in, conv_b),
+                (conv_c_in, conv_c),
+                (rate_in, rate),
+                (context, ctx.at[y]),
+            )
+        )
+    ]
     own_latent = pltpu.make_async_copy(latent, lat.at[x], local_sem.at[3])
+    for c in loads[:3]:
+        c.start()
     own_latent.start()
+    for c in loads[3:]:
+        c.start()
     half = model // 2
     own_half = pl.ds(pl.multiple_of(core * half, half), half)
     out_half = pl.ds(pl.multiple_of(core * (INNER // 2), INNER // 2), INNER // 2)
@@ -236,32 +281,20 @@
         pltpu.make_async_copy(in_bulk, in_bulk, local_sem.at[1]),
         local[-1],
     ]
-    barrier = pltpu.get_barrier_semaphore()
-    up_place = lax.rem(place + 1, count)
-    down_place = lax.rem(place + count - 1, count)
-    above = {"sp_0": up_place // ny, "sp_1": lax.rem(up_place, ny)}
-    below = {"sp_0": down_place // ny, "sp_1": lax.rem(down_place, ny)}
-    peers = [{"sp_0": lax.rem(z + k, nz)} for k in range(1, nz)]
-    peers += [{"sp_1": lax.rem(y + k, ny)} for k in range(1, ny)]
-    peers += [{"tp": lax.rem(x + k, nx)} for k in range(1, nx)]
-    peers += [{"dp": 1 - core}]
-    for k in range(nx):
-        peers += [dict(above, tp=k), dict(below, tp=k)]
-    for peer in peers:
-        pl.semaphore_signal(barrier, inc=1, device_id=peer, device_id_type=MESH)
-
     def unpack(r, ref):
         piece = ref[...].astype(F32)
         for k in range(piece.shape[0]):
             small[r : r + 1, k * LANES : (k + 1) * LANES] = piece[k : k + 1]
 
+    placed[...] = jnp.zeros_like(placed)
+    for c in loads[:3]:
+        c.wait()
     unpack(1, source)
     small[0:1, 0:model] = condition[...].astype(F32)
 
     rows = modw.shape[1]
     chunk = placed.shape[1]
     per = chunk // rows
-    placed[...] = jnp.zeros_like(placed)
     at = pl.ds(pl.multiple_of(lax.rem(place, per) * rows, rows), rows)
     placed[:, at, :] = modw[...]
     lane_at = pl.ds(pl.multiple_of((place // per) * chunk, chunk), chunk)
@@ -327,7 +360,6 @@
     for c, d in zip(swaps, local):
         c.start()
         d.start()
-    ctx[y] = context[...]
 
     def edge(slot, k, to):
         return pltpu.make_async_remote_copy(
@@ -356,7 +388,9 @@
             c.start()
 
     small[2:7, :] = jnp.zeros((5, small.shape[1]), F32)
-    unpack(2, gain_in)
+    for c in loads[3:]:
+        c.wait()
+    unpack(2, gain)
     unpack(3, out_gain)
     small[4:7, 0:INNER] = conv_x[...].astype(F32)
     small[4:7, INNER : INNER + STATE] = conv_b[...].astype(F32)
@@ -397,18 +431,17 @@
     lat_copies.arrived()
     scales = [inverse(lat[t].astype(F32)) for t in range(nx)]
     misc[...] = jnp.zeros_like(misc)
-    for c in (to_above[0], to_below[0]):
+    for c in (to_above[0], to_below[0], *ctx_edges):
         c.wait_recv()
     has = (place > 0, place < count - 1, z > 0, z < nz - 1)
-    for slot in range(2):
+    for slot in range(4):
         misc[slot : slot + 1, :] = jnp.where(has[slot], edge_recv[slot], 0.0)
-    misc_scale = inverse(misc[0:8, :])
-    row8 = rows_of((8, 1))
-
-    def kept(low, high):
-        return jnp.logical_or(
-            jnp.logical_and(row8 == 0, low), jnp.logical_and(row8 == 1, high)
-        )
+    misc_scale = inverse(misc[...])
+    ctx_scales = [inverse(ctx[j].astype(F32)) for j in range(ny)]
+    row16 = rows_of((16, 1))
+    kept = jnp.zeros((16, 1), jnp.bool_)
+    for slot in range(4):
+        kept = jnp.logical_or(kept, jnp.logical_and(row16 == slot, has[slot]))
 
     bulk_local[0].wait()
     bulk_swaps[0].wait_recv()
@@ -427,17 +460,22 @@
         cols = slice(c * width, (c + 1) * width)
         return cols, small[2:3, cols] * (1.0 + mod_x[c, scale]), mod_x[c, shift]
 
-    def edge_rows(cols, scale, shift, known, at):
-        value = misc[at : at + 8, cols] * misc_scale * scale + shift
-        value = jnp.where(known, value, 0.0)
-        return jnp.concatenate([value, jnp.zeros_like(value)], axis=0).astype(BF16)
-
     for c in range(nx):
         cols, scale, shift = modulations(c, 0, 1)
+        _, scale_ctx, shift_ctx = modulations(c, 3, 4)
         for t in range(nx):
             value = lat[t, :, cols].astype(F32) * scales[t] * scale + shift
             hidden[t * own_rows : (t + 1) * own_rows, cols] = value.astype(BF16)
-        hidden[TOKENS:ctx_at, cols] = edge_rows(cols, scale, shift, kept(has[0], has[1]), 0)
+        value = misc[:, cols] * misc_scale * jnp.where(row16 < 2, scale, scale_ctx)
+        value = value + jnp.where(row16 < 2, shift, shift_ctx)
+        hidden[TOKENS:ctx_at, cols] = jnp.where(kept, value, 0.0).astype(BF16)
+        for j in range(0, ny, 2):
+            two = [
+                ctx[i, :, cols].astype(F32) * ctx_scales[i] * scale_ctx + shift_ctx
+                for i in (j, j + 1)
+            ]
+            at = ctx_at + j * CTX_ROWS
+            hidden[at : at + 2 * CTX_ROWS, cols] = jnp.concatenate(two, axis=0).astype(BF16)
 
     def project(rows, left, right):
         while left < right:
@@ -458,7 +496,7 @@
         )
 
     own = slice(0, TOKENS)
-    project(slice(0, ctx_at), 0, COL_C)
+    project(slice(0, ctx_at + lines), 0, COL_C)
     for at in range(0, COL_DT, LANES):
         smooth(own, TOKENS, at, at)
     b_turned = feats[own, COL_B:COL_DT].T.astype(BF16)
@@ -471,20 +509,23 @@
             decay_y[y, r : r + 1, :] = spread(ends, 2 * r)
     decay_copies = gather("sp_1", ny, y, decay_y).start()
 
-    def slabs(axis, size, me, origin, target, way):
+    def slabs(axis, size, me, origin, target, piece):
         return along(
             axis,
             size,
             me,
-            lambda peer: origin.at[way, peer],
-            target.at[way, me],
-            target.at[way, pl.ds(0, size - 1)],
+            lambda peer: origin.at[piece, peer],
+            target.at[piece, me],
+            target.at[piece, pl.ds(0, size - 1)],
         )
 
     state_copies = []
-    for way in range(2):
+
+    def send_states(way):
         for q in range(PAIRS):
             cols = slice(q * LANES, (q + 1) * LANES)
+            piece = way * 2 + q // 2
+            at = slice(q % 2 * LANES, (q % 2 + 1) * LANES)
             head = way * HEADS + 2 * q
             step = spread(steps, head)
             decay = spread(sums, head)
@@ -495,37 +536,27 @@
             at_end = (moved_x * jnp.exp(end - decay)).astype(BF16)
             state = jnp.dot(b_turned, at_end, preferred_element_type=F32).astype(BF16)
             for p in range(ny):
-                state_send[way, p, :, cols] = state[p * slab : (p + 1) * slab]
-        state_copies.append(slabs("sp_1", ny, y, state_send, state_recv, way).start())
-        state_recv[way, y] = state_send[way, y]
-
-    project(slice(0, ctx_at), COL_C, COL_Z)
-
-    for c in ctx_edges:
-        c.wait_recv()
-    for slot in (2, 3):
-        at = 6 + slot
-        misc[at : at + 1, :] = jnp.where(has[slot], edge_recv[slot], 0.0)
-    misc_scale = inverse(misc[8:16, :])
-    ctx_scales = [inverse(ctx[j].astype(F32)) for j in range(ny)]
-    for c in range(nx):
-        cols, scale, shift = modulations(c, 3, 4)
-        hidden[TOKENS:ctx_at, cols] = edge_rows(cols, scale, shift, kept(has[2], has[3]), 8)
-        for j in range(0, ny, 2):
-            two = [
-                ctx[i, :, cols].astype(F32) * ctx_scales[i] * scale + shift
-                for i in (j, j + 1)
-            ]
-            at = ctx_at + j * CTX_ROWS
-            hidden[at : at + 2 * CTX_ROWS, cols] = jnp.concatenate(two, axis=0).astype(BF16)
-    project(slice(TOKENS, ctx_at + lines), 0, COL_C)
+                state_send[piece, p, :, at] = state[p * slab : (p + 1) * slab]
+            if q % 2 == 1:
+                state_copies.append(
+                    slabs("sp_1", ny, y, state_send, state_recv, piece).start()
+                )
+                state_recv[piece, y] = state_send[piece, y]
+
+    send_states(0)
+
     ctx_rows = slice(ctx_at, ctx_at + lines)
     for at in range(0, COL_DT, LANES):
-        smooth(ctx_rows, TOKENS, at, at)
-    ctx_b = feats[ctx_rows, COL_B:COL_DT].T
+        smooth(ctx_rows, TOKENS + 2, at, at)
+    ctx_bt[...] = feats[ctx_rows, COL_B:COL_DT].T
+    ctx_b = ctx_bt[pl.ds(pl.multiple_of(y * slab, slab), slab), :]
     ctx_steps = softplus(feats[ctx_rows, COL_DT:COL_C])
     ctx_sums = running_sums(-rates * ctx_steps, HEADS)
-    own_slab = pl.ds(pl.multiple_of(y * slab, slab), slab)
+    ctx_ends = jnp.where(lane < HEADS, ctx_sums[lines - 1 : lines], ctx_sums[0:1])
+    for r in range(2 * PAIRS):
+        ctx_dz[z, r : r + 1, :] = spread(ctx_ends, 2 * r)
+    ctx_dz_copies = gather("sp_0", nz, z, ctx_dz).start()
+    ctx_copies_z = []
     for way in range(2):
         for q in range(PAIRS):
             cols = slice(q * LANES, (q + 1) * LANES)
@@ -533,16 +564,16 @@
             decay = spread(ctx_sums, head)
             end = decay[lines - 1 : lines] if way == 0 else decay[0:1]
             moved_x = rounded(feats[ctx_rows, cols] * spread(ctx_steps, head))
-            ctx_full[way, :, cols] = jnp.dot(
+            ctx_z[way, z, :, cols] = jnp.dot(
                 ctx_b,
                 moved_x * jnp.exp(end - decay),
                 preferred_element_type=F32,
                 precision=lax.Precision.HIGHEST,
-            )
-            ctx_dz[z, way * PAIRS + q : way * PAIRS + q + 1, :] = end
-        ctx_z[z, way * slab : (way + 1) * slab, :] = ctx_full[way, own_slab, :].astype(BF16)
-    ctx_dz_copies = gather("sp_0", nz, z, ctx_dz).start()
-    ctx_z_copies = gather("sp_0", nz, z, ctx_z).start()
+            ).astype(BF16)
+        ctx_copies_z.append(gather("sp_0", nz, z, ctx_z.at[way]).start())
+
+    send_states(1)
+    project(slice(0, ctx_at), COL_C, COL_Z)
 
     smooth(own, TOKENS, COL_C, INNER + STATE)
     c_vals = feats[own, COL_C:COL_Z].astype(BF16)
@@ -590,62 +621,71 @@
     tot_dz_copies = gather("sp_0", nz, z, tot_dz).start()
     factors = [jnp.exp(d) for d in decays]
     tot_copies = []
-    for way in range(2):
-        state_copies[way].arrived()
-        for q in range(PAIRS):
+    for piece in range(4):
+        way = piece // 2
+        state_copies[piece].arrived()
+        for q in range(2):
             cols = slice(q * LANES, (q + 1) * LANES)
-            r = way * PAIRS + q
+            r = piece * 2 + q
             state = jnp.zeros((slab, LANES), F32)
             for j in range(ny) if way == 0 else reversed(range(ny)):
-                before[way, j, :, cols] = state
-                state = state * factors[j][r : r + 1] + state_recv[way, j, :, cols].astype(F32)
-            tot_z[way, z, :, cols] = state.astype(BF16)
-        tot_copies.append(Totals(way, tot_z, nz, z, tot_sems).start())
+                before[piece, j, :, cols] = state
+                state = state * factors[j][r : r + 1] + state_recv[piece, j, :, cols].astype(F32)
+            tot_z[piece, z, :, cols] = state.astype(BF16)
+        tot_copies.append(
+            Totals(way, tot_z.at[piece], nz, z, tot_sems.at[piece % 2]).start()
+        )
 
     ctx_dz_copies.arrived()
-    ctx_z_copies.arrived()
     ctx_factors = [jnp.exp(ctx_dz[j]) for j in range(nz)]
     tot_dz_copies.arrived()
     tot_factors = [jnp.exp(tot_dz[j]) for j in range(nz)]
     enter_copies = []
-    for way in range(2):
-        part = slice(way * slab, (way + 1) * slab)
+    for piece in range(4):
+        way = piece // 2
+        order = list(range(nz)) if way == 0 else list(reversed(range(nz)))
+        if piece % 2 == 0:
+            ctx_copies_z[way].arrived()
         starts = []
-        for q in range(PAIRS):
+        for q in range(2):
             cols = slice(q * LANES, (q + 1) * LANES)
-            r = way * PAIRS + q
+            r = piece * 2 + q
+            at = (piece % 2) * PIECE + q * LANES
             state = jnp.zeros((slab, LANES), F32)
-            for j in range(nz) if way == 0 else reversed(range(nz)):
-                state = state * ctx_factors[j][r : r + 1] + ctx_z[j, part, cols].astype(F32)
+            for j in order:
+                fresh = ctx_z[way, j, :, at : at + LANES].astype(F32)
+                state = state * ctx_factors[j][r : r + 1] + fresh
             starts.append(state)
-        tot_copies[way].arrived()
-        for q in range(PAIRS):
+        tot_copies[piece].arrived()
+        for q in range(2):
             cols = slice(q * LANES, (q + 1) * LANES)
-            r = way * PAIRS + q
+            r = piece * 2 + q
             state = starts[q]
-            for j in range(nz) if way == 0 else reversed(range(nz)):
+            for j in order:
                 passed = j < z if way == 0 else j > z
-                later = state * tot_factors[j][r : r + 1] + tot_z[way, j, :, cols].astype(F32)
+                later = state * tot_factors[j][r : r + 1] + tot_z[piece, j, :, cols].astype(F32)
                 state = jnp.where(passed, later, state)
             for j in range(ny):
-                enter_send[way, j, :, cols] = (
-                    before[way, j, :, cols] + ahead[j][r : r + 1] * state
+                enter_send[piece, j, :, cols] = (
+                    before[piece, j, :, cols] + ahead[j][r : r + 1] * state
                 ).astype(BF16)
-        enter_copies.append(slabs("sp_1", ny, y, enter_send, enter_recv, way).start())
-        enter_recv[way, y] = enter_send[way, y]
+        enter_copies.append(slabs("sp_1", ny, y, enter_send, enter_recv, piece).start())
+        enter_recv[piece, y] = enter_send[piece, y]
 
     squares = jnp.zeros((TOKENS, 1), F32)
-    for way in range(2):
-        enter_copies[way].arrived()
+    for piece in range(4):
+        way = piece // 2
+        enter_copies[piece].arrived()
         carried = jnp.dot(
-            c_vals, enter_recv[way].reshape(STATE, INNER), preferred_element_type=F32
+            c_vals, enter_recv[piece].reshape(STATE, PIECE), preferred_element_type=F32
         )
-        for q in range(PAIRS):
-            cols = slice(q * LANES, (q + 1) * LANES)
-            value = inside[:, cols] + growth[way, :, cols] * carried[:, cols]
+        for q in range(2):
+            at = (piece % 2) * PIECE + q * LANES
+            cols = slice(at, at + LANES)
+            value = inside[:, cols]
+            value = value + growth[way, :, cols] * carried[:, q * LANES : (q + 1) * LANES]
             if way == 1:
-                at = COL_Z + q * LANES
-                value = value * feats[own, at : at + LANES]
+                value = value * feats[own, COL_Z + at : COL_Z + at + LANES]
                 squares = squares + jnp.sum(value * value, axis=1, keepdims=True)
             inside[:, cols] = value
     scale = lax.rsqrt(squares / INNER + EPSILON)
@@ -687,8 +727,8 @@
         for c in to_below:
             c.wait_send()
 
-    done = mods + [ctx_copies, lat_copies, decay_copies, ctx_dz_copies, ctx_z_copies]
-    done += [tot_dz_copies] + state_copies + tot_copies + enter_copies
+    done = mods + [ctx_copies, lat_copies, decay_copies, ctx_dz_copies, tot_dz_copies]
+    done += ctx_copies_z + state_copies + tot_copies + enter_copies
     for e in done + part_copies:
         e.left()
     own_part.wait()
@@ -729,6 +769,15 @@
     hbm = pl.BlockSpec(memory_space=pl.ANY)
     dma = pltpu.SemaphoreType.DMA
     scratch = [
+        pltpu.VMEM((1, model), BF16),
+        pltpu.VMEM((model // LANES, LANES), BF16),
+        pltpu.VMEM((model // LANES, LANES), BF16),
+        pltpu.VMEM((INNER // LANES, LANES), BF16),
+        pltpu.VMEM((3, INNER), BF16),
+        pltpu.VMEM((3, STATE), BF16),
+        pltpu.VMEM((3, STATE), BF16),
+        pltpu.VMEM((2, HEADS), F32),
+        pltpu.VMEM((3, rows, width), BF16),
         pltpu.VMEM((model, COLS), BF16),
         pltpu.VMEM((INNER, model), BF16),
         pltpu.VMEM((2, HEADS, model), BF16),
@@ -748,26 +797,26 @@
         pltpu.VMEM((2 * TOKENS, INNER), BF16),
         pltpu.VMEM((2, TOKENS, INNER), F32),
         pltpu.VMEM((TOKENS, INNER), F32),
-        pltpu.VMEM((2, STATE, INNER), F32),
-        pltpu.VMEM((nz, 2 * slab, INNER), BF16),
-        pltpu.VMEM((nz, 8, LANES), F32),
-        pltpu.VMEM((2, ny, slab, INNER), BF16),
-        pltpu.VMEM((2, ny, slab, INNER), BF16),
-        pltpu.VMEM((ny, 8, LANES), F32),
+        pltpu.VMEM((STATE, lines), F32),
         pltpu.VMEM((2, nz, slab, INNER), BF16),
         pltpu.VMEM((nz, 8, LANES), F32),
-        pltpu.VMEM((2, ny, slab, INNER), F32),
-        pltpu.VMEM((2, ny, slab, INNER), BF16),
-        pltpu.VMEM((2, ny, slab, INNER), BF16),
+        pltpu.VMEM((4, ny, slab, PIECE), BF16),
+        pltpu.VMEM((4, ny, slab, PIECE), BF16),
+        pltpu.VMEM((ny, 8, LANES), F32),
+        pltpu.VMEM((4, nz, slab, PIECE), BF16),
+        pltpu.VMEM((nz, 8, LANES), F32),
+        pltpu.VMEM((4, ny, slab, PIECE), F32),
+        pltpu.VMEM((4, ny, slab, PIECE), BF16),
+        pltpu.VMEM((4, ny, slab, PIECE), BF16),
         pltpu.VMEM((TOKENS, INNER), BF16),
         pltpu.VMEM((nx, own_rows, model), BF16),
-        dma((5,)),
+        dma((15,)),
         dma((3,)),
         dma((3,)),
-        dma((13 + nx, 2)),
+        dma((18 + nx, 2)),
         dma((4, nx)),
         dma((4,)),
-        dma((2, nz - 1)),
+        dma((2, 2, nz - 1)),
     ]
     parts, gate = pl.pallas_call(
         functools.partial(mixer, (nz, ny, nx, model)),
@@ -775,7 +824,7 @@
             jax.ShapeDtypeStruct((nx, own_rows, model), BF16),
             jax.ShapeDtypeStruct((1, model), F32),
         ),
-        in_specs=[vmem] * 10 + [hbm] * 7,
+        in_specs=[hbm] * 17,
         out_specs=(hbm, vmem),
         scratch_shapes=scratch,
         compiler_params=pltpu.CompilerParams(

time: 59.2 us -> 57.7 us (0.975)
  Pallas kernels: 56.5 us -> 55.3 us
    pallas_call x1, Pallas kernels: 56.5 us -> 55.3 us  [shards(): pl.pallas_call(functools.partial(mixer, (nz, ny, nx, model)), out_shape=(...]
where the time goes in v4:
time: 57.7 us; the launch traced here: 57.2 us
  Pallas kernels  55.3 us (96%)
  other arithmetic  1.83 us (3%)
    pallas_call x1, Pallas kernels, shards(): pl.pallas_call(functools.partial(mixer, (nz, ny, nx, model)), out_shape=(...  55.3 us
    convert_element_type x1, other arithmetic, shards(): return (gate * mixed).astype(BF16)[None]  1.83 us

profile of v4, /device:TPU:6, one launch (start us, length us, event | category | flops | bytes accessed | tf_op | source)
XLA Modules:
  0.0 57.2 jit_solution(4459965365579813391)
XLA Ops:
  0.0 55.3 %shard_map.163 = (bf16[4,32,2048]{2,1,0:T(8,128)(2,1)}, f32[1,2048]{1,0:T(1,128)}) custom-call(bf16[1,2048]{1,0:T(2,128)(2,1)} %condition_in.1, bf16[16,128]{1,0:T(8,128)(2,1)} %bitcast.11, bf16[16,128]{1,0:T(8,128)(2,1)} %bitcast.12, bf16[4,128]{1,0:T(4,128)(2,1)} %bitcast.13, bf16[3,512]{1,0:T(4,128)(2,1)} %conv_x_in.1, bf16[3,128]{1,0:T(4,128)(2,1)} %conv_b_in.1, ...), custom_call_target="tpu_custom_call" | custom-call | tf_op jit(solution)/shard_map/pallas_call | solution.py:821
  55.3 1.8 %multiply_convert_fusion = bf16[1,32,2048]{2,1,0:T(8,128)(2,1)} fusion(bf16[4,32,2048]{2,1,0:T(8,128)(2,1)} %get-tuple-element.8, f32[2048]{0:T(1024)} %bitcast.10), kind=kLoop, calls=%fused_computation | loop fusion | flops 589824 | bytes 663552 | tf_op jit(solution)/shard_map/convert_element_type | solution.py:855

commit v5 on v4

--- a/solution.py
+++ b/solution.py
@@ -158,8 +158,7 @@
     w_z,
     w_dt,
     w_out,
-    parts,
-    gate,
+    update,
     condition,
     source,
     gain,
@@ -201,6 +200,7 @@
     enter_recv,
     normed,
     part_send,
+    parts,
     local_sem,
     core_send,
     core_recv,
@@ -580,8 +580,6 @@
     project(own, COL_Z, COLS)
     for at in range(COL_Z, COLS, LANES):
         feats[own, at : at + LANES] = silu(feats[own, at : at + LANES])
-    for c in range(nx):
-        gate[:, c * width : (c + 1) * width] = mod_x[c, 2]
     scores = jnp.dot(c_vals, b_turned, preferred_element_type=F32)
     turned = sums.T
     square = (TOKENS, TOKENS)
@@ -712,8 +710,7 @@
                 parts.at[pl.ds(0, nx - 1), :, cols],
             ).start()
         )
-    own_part = pltpu.make_async_copy(part_send.at[x], parts.at[x], local_sem.at[4])
-    own_part.start()
+    parts[x] = part_send[x]
     for e in bulk_swaps + ctx_edges:
         e.wait_send()
 
@@ -731,9 +728,13 @@
     done += ctx_copies_z + state_copies + tot_copies + enter_copies
     for e in done + part_copies:
         e.left()
-    own_part.wait()
-    for e in part_copies:
-        e.arrived()
+    for c in range(nx):
+        cols = slice(c * width, (c + 1) * width)
+        part_copies[c].arrived()
+        value = parts[0, :, cols].astype(F32)
+        for t in range(1, nx):
+            value = value + parts[t, :, cols].astype(F32)
+        update[:, cols] = (mod_x[c, 2] * value).astype(BF16)
 
 
 def shards(
@@ -810,6 +811,7 @@
         pltpu.VMEM((4, ny, slab, PIECE), BF16),
         pltpu.VMEM((TOKENS, INNER), BF16),
         pltpu.VMEM((nx, own_rows, model), BF16),
+        pltpu.VMEM((nx, own_rows, model), BF16),
         dma((15,)),
         dma((3,)),
         dma((3,)),
@@ -818,14 +820,11 @@
         dma((4,)),
         dma((2, 2, nz - 1)),
     ]
-    parts, gate = pl.pallas_call(
+    update = pl.pallas_call(
         functools.partial(mixer, (nz, ny, nx, model)),
-        out_shape=(
-            jax.ShapeDtypeStruct((nx, own_rows, model), BF16),
-            jax.ShapeDtypeStruct((1, model), F32),
-        ),
+        out_shape=pltpu.VMEM((own_rows, model), BF16),
         in_specs=[hbm] * 17,
-        out_specs=(hbm, vmem),
+        out_specs=vmem,
         scratch_shapes=scratch,
         compiler_params=pltpu.CompilerParams(
             collective_id=0, has_side_effects=True, vmem_limit_bytes=56 * 1024 * 1024
@@ -849,10 +848,7 @@
         jnp.swapaxes(w_dt, 1, 2),
         w_out,
     )
-    mixed = parts[0].astype(F32)
-    for k in range(1, nx):
-        mixed = mixed + parts[k].astype(F32)
-    return (gate * mixed).astype(BF16)[None]
+    return update[None]
 
 
 def solution(mesh):

time: 57.7 us -> 55.9 us (0.969)
  other arithmetic: 1.83 us -> 0 us
  Pallas kernels: 55.3 us -> 54.6 us
  local copies, waits for them, and re-layouts: 0 us -> 0.66 us
    convert_element_type x1 -> x0, other arithmetic: 1.83 us -> none  [shards(): return (gate * mixed).astype(BF16)[None]]
    pallas_call x1, Pallas kernels: 55.3 us -> 54.6 us  [shards(): pl.pallas_call(functools.partial(mixer, (nz, ny, nx, model)), out_shape=p...]
    unnamed x0 -> x1, local copies, waits for them, and re-layouts: none -> 0.66 us
where the time goes in v5:
time: 55.9 us; the launch traced here: 55.3 us
  Pallas kernels  54.6 us (98%)
  local copies, waits for them, and re-layouts  0.66 us (1%)
    pallas_call x1, Pallas kernels, shards(): pl.pallas_call(functools.partial(mixer, (nz, ny, nx, model)), out_shape=p...  54.6 us

profile of v5, /device:TPU:6, one launch (start us, length us, event | category | flops | bytes accessed | tf_op | source)
XLA Modules:
  0.0 55.3 jit_solution(9119632567465541697)
XLA Ops:
  0.0 54.6 %shard_map.163 = bf16[32,2048]{1,0:T(8,128)(2,1)S(1)} custom-call(bf16[1,2048]{1,0:T(2,128)(2,1)} %condition_in.1, bf16[16,128]{1,0:T(8,128)(2,1)} %bitcast.11, bf16[16,128]{1,0:T(8,128)(2,1)} %bitcast.12, bf16[4,128]{1,0:T(4,128)(2,1)} %bitcast.13, bf16[3,512]{1,0:T(4,128)(2,1)} %conv_x_in.1, bf16[3,128]{1,0:T(4,128)(2,1)} %conv_b_in.1, ...), custom_call_target="tpu_custom_call" | custom-call | tf_op jit(solution)/shard_map/pallas_call | solution.py:823
  54.7 0.7 %copy.19 = bf16[1,32,2048]{2,1,0:T(8,128)(2,1)} copy(bf16[1,32,2048]{2,1,0:T(8,128)(2,1)S(1)} %bitcast.7) | data formatting | bytes 262144

commit v6 on v5

--- a/solution.py
+++ b/solution.py
@@ -108,35 +108,36 @@
 
 class Totals:
     def __init__(self, way, buf, size, place, sems):
-        self.sends, self.gets, self.copies = [], [], []
-        for k in range(1, size):
-            later = place + k < size
-            passed = place >= k
-            self.sends.append(later if way == 0 else jnp.logical_not(later))
-            self.gets.append(passed if way == 0 else jnp.logical_not(passed))
-            self.copies.append(
-                pltpu.make_async_remote_copy(
-                    src_ref=buf.at[place],
-                    dst_ref=buf.at[place],
-                    send_sem=sems.at[0, k - 1],
-                    recv_sem=sems.at[1, k - 1],
-                    device_id={"sp_0": lax.rem(place + k, size)},
-                    device_id_type=MESH,
-                )
+        def copy(peer, ref):
+            return pltpu.make_async_remote_copy(
+                src_ref=ref,
+                dst_ref=ref,
+                send_sem=sems.at[0],
+                recv_sem=sems.at[1],
+                device_id={"sp_0": peer},
+                device_id_type=MESH,
             )
 
+        later, passed = size - 1 - place, place
+        self.sends, self.gets = (later, passed) if way == 0 else (passed, later)
+        self.way, self.size, self.place = way, size, place
+        peers = [lax.rem(place + k, size) for k in range(1, size)]
+        self.copies = [copy(peer, buf.at[place]) for peer in peers]
+        self.wholes = [copy(peers[0], buf.at[pl.ds(0, m)]) for m in range(1, size)]
+
     def start(self):
-        for taken, c in zip(self.sends, self.copies):
-            pl.when(taken)(c.start)
+        for k, c in enumerate(self.copies, 1):
+            later = self.place + k < self.size
+            pl.when(later if self.way == 0 else jnp.logical_not(later))(c.start)
         return self
 
     def arrived(self):
-        for taken, c in zip(self.gets, self.copies):
-            pl.when(taken)(c.wait_recv)
+        for m, c in enumerate(self.wholes, 1):
+            pl.when(self.gets == m)(c.wait_recv)
 
     def left(self):
-        for taken, c in zip(self.sends, self.copies):
-            pl.when(taken)(c.wait_send)
+        for m, c in enumerate(self.wholes, 1):
+            pl.when(self.sends == m)(c.wait_send)
 
 
 def mixer(
@@ -179,6 +180,9 @@
     mod_z,
     mod_y,
     mod_x,
+    gate_y,
+    gate_z,
+    gate_x,
     edge_send,
     edge_recv,
     misc,
@@ -208,6 +212,7 @@
     edge_sems,
     edge_got,
     tot_sems,
+    last_sems,
 ):
     nz, ny, nx, model = dims
     width = model // nx
@@ -221,20 +226,6 @@
     core = lax.axis_index("dp")
     place = z * ny + y
     count = nz * ny
-
-    barrier = pltpu.get_barrier_semaphore()
-    up_place = lax.rem(place + 1, count)
-    down_place = lax.rem(place + count - 1, count)
-    above = {"sp_0": up_place // ny, "sp_1": lax.rem(up_place, ny)}
-    below = {"sp_0": down_place // ny, "sp_1": lax.rem(down_place, ny)}
-    peers = [{"sp_1": lax.rem(y + k, ny)} for k in range(1, ny)]
-    peers += [{"sp_0": lax.rem(z + k, nz)} for k in range(1, nz)]
-    peers += [{"tp": lax.rem(x + k, nx)} for k in range(1, nx)]
-    peers += [{"dp": 1 - core}]
-    for k in range(nx):
-        peers += [dict(above, tp=k), dict(below, tp=k)]
-    for peer in peers:
-        pl.semaphore_signal(barrier, inc=1, device_id=peer, device_id_type=MESH)
 
     loads = [
         pltpu.make_async_copy(origin, target, local_sem.at[5 + i])
@@ -257,6 +248,21 @@
     for c in loads[:3]:
         c.start()
     own_latent.start()
+    barrier = pltpu.get_barrier_semaphore()
+    up_place = lax.rem(place + 1, count)
+    down_place = lax.rem(place + count - 1, count)
+    above = {"sp_0": up_place // ny, "sp_1": lax.rem(up_place, ny)}
+    below = {"sp_0": down_place // ny, "sp_1": lax.rem(down_place, ny)}
+    peers = [{"sp_1": lax.rem(y + k, ny)} for k in range(1, ny)]
+    peers += [{"sp_0": lax.rem(z + k, nz)} for k in range(1, nz)]
+    peers += [{"tp": lax.rem(x + k, nx)} for k in range(1, nx)]
+    peers += [{"dp": 1 - core}]
+    for k in range(nx):
+        peers += [dict(above, tp=k), dict(below, tp=k)]
+    z_up, z_down = lax.rem(z + 1, nz), lax.rem(z + nz - 1, nz)
+    for peer in peers:
+        pl.semaphore_signal(barrier, inc=1, device_id=peer, device_id_type=MESH)
+
     for c in loads[3:]:
         c.start()
     half = model // 2
@@ -303,14 +309,15 @@
     row8 = rows_of((8, chunk))
     partial = jnp.zeros((8, width), F32)
     for k in range(3):
-        left = jnp.where(row8 == k, act, 0.0)
+        left = jnp.where(row8 == (0, 1, 4)[k], act, 0.0)
         if k < 2:
-            left = jnp.where(row8 == 3 + k, act_ctx, left)
+            left = jnp.where(row8 == 2 + k, act_ctx, left)
         partial = partial + jnp.dot(
             left.astype(BF16), placed[k], preferred_element_type=F32
         )
-    for r in range(5):
+    for r in range(4):
         mod_y[y, r] = partial[r : r + 1]
+    gate_y[y, 0] = partial[4:5]
 
     pl.semaphore_wait(barrier, len(peers))
     pairs = iter(range(32))
@@ -327,6 +334,18 @@
         gather("sp_0", nz, z, mod_z),
         gather("tp", nx, x, mod_x),
     ]
+    gates = [
+        gather("sp_1", ny, y, gate_y),
+        gather("sp_0", nz, z, gate_z),
+        gather("tp", nx, x, gate_x),
+    ]
+
+    def summed(buf, size):
+        total = buf[0]
+        for k in range(1, size):
+            total = total + buf[k]
+        return total
+
     mods[0].start()
     ctx_copies = along(
         "sp_1", ny, y, lambda peer: context, ctx.at[y], ctx.at[pl.ds(0, ny - 1)]
@@ -361,32 +380,41 @@
         c.start()
         d.start()
 
-    def edge(slot, k, to):
-        return pltpu.make_async_remote_copy(
-            src_ref=edge_send.at[slot],
-            dst_ref=edge_recv.at[slot],
-            send_sem=edge_sems.at[slot, k],
-            recv_sem=edge_got.at[slot],
-            device_id=to,
-            device_id_type=MESH,
-        )
-
-    to_above = [edge(0, k, dict(above, tp=k)) for k in range(nx)]
-    to_below = [edge(1, k, dict(below, tp=k)) for k in range(nx)]
+    def edge(slot, to, bulk):
+        def copy(origin, target, peer):
+            return pltpu.make_async_remote_copy(
+                src_ref=origin,
+                dst_ref=target,
+                send_sem=edge_sems.at[slot],
+                recv_sem=edge_got.at[slot],
+                device_id=peer,
+                device_id_type=MESH,
+            )
+
+        each = [copy(edge_send.at[slot], edge_recv.at[slot], peer) for peer in to]
+        return each, None if bulk is None else copy(bulk, bulk, to[0])
+
+    lat_bulk = edge_send.at[pl.ds(0, nx)]
+    edges = (
+        (x == nx - 1, edge(0, [dict(above, tp=k) for k in range(nx)], lat_bulk)),
+        (x == 0, edge(1, [dict(below, tp=k) for k in range(nx)], lat_bulk)),
+    )
+    ctx_edges = [
+        edge(2, [{"sp_0": z_up}], None)[0][0],
+        edge(3, [{"sp_0": z_down}], None)[0][0],
+    ]
     own_latent.wait()
-
-    @pl.when(x == nx - 1)
-    def _():
-        edge_send[0] = lat[x].astype(F32)[own_rows - 1 : own_rows, :]
-        for c in to_above:
-            c.start()
-
-    @pl.when(x == 0)
-    def _():
-        edge_send[1] = lat[x].astype(F32)[0:1, :]
-        for c in to_below:
-            c.start()
-
+    for slot, (owner, (each, _)) in enumerate(edges):
+
+        @pl.when(owner)
+        def _(slot=slot, each=each):
+            held = lat[x].astype(F32)
+            at = 0 if slot == 1 else own_rows - 1
+            edge_send[slot] = held[at : at + 1, :]
+            for c in each:
+                c.start()
+
+    gates[0].start()
     small[2:7, :] = jnp.zeros((5, small.shape[1]), F32)
     for c in loads[3:]:
         c.wait()
@@ -402,42 +430,31 @@
             rates = jnp.where(lane == way * HEADS + h, rate[way : way + 1, h : h + 1], rates)
 
     mods[0].arrived()
-    total = mod_y[0]
-    for k in range(1, ny):
-        total = total + mod_y[k]
-    mod_z[z] = total
+    mod_z[z] = summed(mod_y, ny)
     mods[1].start()
 
     def inverse(v):
         return lax.rsqrt(jnp.mean(v * v, axis=1, keepdims=True) + EPSILON)
 
     mods[1].arrived()
-    total = mod_z[0]
-    for k in range(1, nz):
-        total = total + mod_z[k]
-    mod_x[x] = total
+    mod_x[x] = summed(mod_z, nz)
     mods[2].start()
 
     ctx_copies.arrived()
     edge_send[2] = ctx[ny - 1].astype(F32)[CTX_ROWS - 1 : CTX_ROWS, :]
     edge_send[3] = ctx[0].astype(F32)[0:1, :]
-    ctx_edges = [
-        edge(2, 0, {"sp_0": lax.rem(z + 1, nz)}),
-        edge(3, 0, {"sp_0": lax.rem(z + nz - 1, nz)}),
-    ]
     for c in ctx_edges:
         c.start()
-
+    ctx_scales = [inverse(ctx[j].astype(F32)) for j in range(ny)]
     lat_copies.arrived()
     scales = [inverse(lat[t].astype(F32)) for t in range(nx)]
     misc[...] = jnp.zeros_like(misc)
-    for c in (to_above[0], to_below[0], *ctx_edges):
+    for c in (edges[0][1][0][0], edges[1][1][0][0], *ctx_edges):
         c.wait_recv()
     has = (place > 0, place < count - 1, z > 0, z < nz - 1)
     for slot in range(4):
         misc[slot : slot + 1, :] = jnp.where(has[slot], edge_recv[slot], 0.0)
     misc_scale = inverse(misc[...])
-    ctx_scales = [inverse(ctx[j].astype(F32)) for j in range(ny)]
     row16 = rows_of((16, 1))
     kept = jnp.zeros((16, 1), jnp.bool_)
     for slot in range(4):
@@ -462,7 +479,7 @@
 
     for c in range(nx):
         cols, scale, shift = modulations(c, 0, 1)
-        _, scale_ctx, shift_ctx = modulations(c, 3, 4)
+        _, scale_ctx, shift_ctx = modulations(c, 2, 3)
         for t in range(nx):
             value = lat[t, :, cols].astype(F32) * scales[t] * scale + shift
             hidden[t * own_rows : (t + 1) * own_rows, cols] = value.astype(BF16)
@@ -496,8 +513,10 @@
         )
 
     own = slice(0, TOKENS)
-    project(slice(0, ctx_at + lines), 0, COL_C)
-    for at in range(0, COL_DT, LANES):
+    every = slice(0, ctx_at + lines)
+    project(every, COL_B, COL_C)
+    project(every, 0, PIECE)
+    for at in (COL_B, 0, LANES):
         smooth(own, TOKENS, at, at)
     b_turned = feats[own, COL_B:COL_DT].T.astype(BF16)
     steps = softplus(feats[own, COL_DT:COL_C])
@@ -521,8 +540,8 @@
 
     state_copies = []
 
-    def send_states(way):
-        for q in range(PAIRS):
+    def send_states(way, pairs):
+        for q in pairs:
             cols = slice(q * LANES, (q + 1) * LANES)
             piece = way * 2 + q // 2
             at = slice(q % 2 * LANES, (q % 2 + 1) * LANES)
@@ -543,7 +562,11 @@
                 )
                 state_recv[piece, y] = state_send[piece, y]
 
-    send_states(0)
+    send_states(0, (0, 1))
+    project(every, PIECE, INNER)
+    for at in range(PIECE, INNER, LANES):
+        smooth(own, TOKENS, at, at)
+    send_states(0, (2, 3))
 
     ctx_rows = slice(ctx_at, ctx_at + lines)
     for at in range(0, COL_DT, LANES):
@@ -557,7 +580,22 @@
         ctx_dz[z, r : r + 1, :] = spread(ctx_ends, 2 * r)
     ctx_dz_copies = gather("sp_0", nz, z, ctx_dz).start()
     ctx_copies_z = []
-    for way in range(2):
+    is_last = z == nz - 1
+
+    def last_copy(ref, peer):
+        return pltpu.make_async_remote_copy(
+            src_ref=ref,
+            dst_ref=ref,
+            send_sem=last_sems.at[0],
+            recv_sem=last_sems.at[1],
+            device_id={"sp_0": peer},
+            device_id_type=MESH,
+        )
+
+    to_last = last_copy(ctx_z.at[1, z], nz - 1)
+    at_last = last_copy(ctx_z.at[1, pl.ds(0, nz - 1)], z_down)
+
+    def send_context(way):
         for q in range(PAIRS):
             cols = slice(q * LANES, (q + 1) * LANES)
             head = way * HEADS + 2 * q
@@ -570,10 +608,18 @@
                 preferred_element_type=F32,
                 precision=lax.Precision.HIGHEST,
             ).astype(BF16)
-        ctx_copies_z.append(gather("sp_0", nz, z, ctx_z.at[way]).start())
-
-    send_states(1)
+        if way == 0:
+            ctx_copies_z.append(gather("sp_0", nz, z, ctx_z.at[0]).start())
+        else:
+            pl.when(jnp.logical_not(is_last))(to_last.start)
+
+    send_context(0)
+    send_context(1)
+    send_states(1, (0, 1, 2, 3))
     project(slice(0, ctx_at), COL_C, COL_Z)
+    gates[0].arrived()
+    gate_z[z] = summed(gate_y, ny)
+    gates[1].start()
 
     smooth(own, TOKENS, COL_C, INNER + STATE)
     c_vals = feats[own, COL_C:COL_Z].astype(BF16)
@@ -619,9 +665,28 @@
     tot_dz_copies = gather("sp_0", nz, z, tot_dz).start()
     factors = [jnp.exp(d) for d in decays]
     tot_copies = []
+    ctx_factors = []
+    line_factor = jnp.exp(acc_f)
+
+    def context_start(way, r):
+        order = range(nz) if way == 0 else reversed(range(nz))
+        at = (r - way * PAIRS) * LANES
+        state = jnp.zeros((slab, LANES), F32)
+        for j in order:
+            fresh = ctx_z[way, j, :, at : at + LANES].astype(F32)
+            state = state * ctx_factors[j][r : r + 1] + fresh
+        return state
+
+    last_starts = []
     for piece in range(4):
         way = piece // 2
         state_copies[piece].arrived()
+        if piece == 2:
+            ctx_dz_copies.arrived()
+            ctx_factors += [jnp.exp(ctx_dz[j]) for j in range(nz)]
+            pl.when(is_last)(at_last.wait_recv)
+            for r in range(PAIRS, 2 * PAIRS):
+                last_starts.append(jnp.where(is_last, context_start(1, r), 0.0))
         for q in range(2):
             cols = slice(q * LANES, (q + 1) * LANES)
             r = piece * 2 + q
@@ -629,31 +694,28 @@
             for j in range(ny) if way == 0 else reversed(range(ny)):
                 before[piece, j, :, cols] = state
                 state = state * factors[j][r : r + 1] + state_recv[piece, j, :, cols].astype(F32)
+            if way == 1:
+                state = state + line_factor[r : r + 1] * last_starts[r - PAIRS]
             tot_z[piece, z, :, cols] = state.astype(BF16)
         tot_copies.append(
-            Totals(way, tot_z.at[piece], nz, z, tot_sems.at[piece % 2]).start()
+            Totals(way, tot_z.at[piece], nz, z, tot_sems.at[piece]).start()
         )
 
-    ctx_dz_copies.arrived()
-    ctx_factors = [jnp.exp(ctx_dz[j]) for j in range(nz)]
+    gates[1].arrived()
+    gate_x[x] = summed(gate_z, nz)
+    gates[2].start()
     tot_dz_copies.arrived()
     tot_factors = [jnp.exp(tot_dz[j]) for j in range(nz)]
     enter_copies = []
     for piece in range(4):
         way = piece // 2
         order = list(range(nz)) if way == 0 else list(reversed(range(nz)))
-        if piece % 2 == 0:
-            ctx_copies_z[way].arrived()
-        starts = []
-        for q in range(2):
-            cols = slice(q * LANES, (q + 1) * LANES)
-            r = piece * 2 + q
-            at = (piece % 2) * PIECE + q * LANES
-            state = jnp.zeros((slab, LANES), F32)
-            for j in order:
-                fresh = ctx_z[way, j, :, at : at + LANES].astype(F32)
-                state = state * ctx_factors[j][r : r + 1] + fresh
-            starts.append(state)
+        if piece == 0:
+            ctx_copies_z[0].arrived()
+        starts = [
+            context_start(0, r) if way == 0 else last_starts[r - PAIRS]
+            for r in (piece * 2, piece * 2 + 1)
+        ]
         tot_copies[piece].arrived()
         for q in range(2):
             cols = slice(q * LANES, (q + 1) * LANES)
@@ -713,18 +775,12 @@
     parts[x] = part_send[x]
     for e in bulk_swaps + ctx_edges:
         e.wait_send()
-
-    @pl.when(x == nx - 1)
-    def _():
-        for c in to_above:
-            c.wait_send()
-
-    @pl.when(x == 0)
-    def _():
-        for c in to_below:
-            c.wait_send()
-
-    done = mods + [ctx_copies, lat_copies, decay_copies, ctx_dz_copies, tot_dz_copies]
+    pl.when(jnp.logical_not(is_last))(to_last.wait_send)
+    gates[2].arrived()
+    for owner, (_, whole) in edges:
+        pl.when(owner)(whole.wait_send)
+
+    done = mods + gates + [ctx_copies, lat_copies, decay_copies, ctx_dz_copies, tot_dz_copies]
     done += ctx_copies_z + state_copies + tot_copies + enter_copies
     for e in done + part_copies:
         e.left()
@@ -734,7 +790,7 @@
         value = parts[0, :, cols].astype(F32)
         for t in range(1, nx):
             value = value + parts[t, :, cols].astype(F32)
-        update[:, cols] = (mod_x[c, 2] * value).astype(BF16)
+        update[:, cols] = (gate_x[c, 0] * value).astype(BF16)
 
 
 def shards(
@@ -787,9 +843,12 @@
         pltpu.VMEM((nx, own_rows, model), BF16),
         pltpu.VMEM((ny, CTX_ROWS, model), BF16),
         pltpu.VMEM((3, max(rows, LANES), width), BF16),
-        pltpu.VMEM((nz, 5, 1, width), F32),
-        pltpu.VMEM((ny, 5, 1, width), F32),
-        pltpu.VMEM((nx, 5, 1, width), F32),
+        pltpu.VMEM((nz, 4, 1, width), F32),
+        pltpu.VMEM((ny, 4, 1, width), F32),
+        pltpu.VMEM((nx, 4, 1, width), F32),
+        pltpu.VMEM((ny, 1, 1, width), F32),
+        pltpu.VMEM((nz, 1, 1, width), F32),
+        pltpu.VMEM((nx, 1, 1, width), F32),
         pltpu.VMEM((4, 1, model), F32),
         pltpu.VMEM((4, 1, model), F32),
         pltpu.VMEM((16, model), F32),
@@ -815,10 +874,11 @@
         dma((15,)),
         dma((3,)),
         dma((3,)),
-        dma((18 + nx, 2)),
-        dma((4, nx)),
+        dma((20 + nx, 2)),
         dma((4,)),
-        dma((2, 2, nz - 1)),
+        dma((4,)),
+        dma((4, 2)),
+        dma((2,)),
     ]
     update = pl.pallas_call(
         functools.partial(mixer, (nz, ny, nx, model)),

time: 55.9 us -> 55.8 us (level)
  the two profiles are of different devices: /device:TPU:6 before, /device:TPU:2 now
where the time goes in v6:
time: 55.8 us; the launch traced here: 55.7 us
  Pallas kernels  55 us (99%)
  local copies, waits for them, and re-layouts  0.66 us (1%)
    pallas_call x1, Pallas kernels, shards(): pl.pallas_call(functools.partial(mixer, (nz, ny, nx, model)), out_shape=p...  55 us

profile of v6, /device:TPU:2, one launch (start us, length us, event | category | flops | bytes accessed | tf_op | source)
XLA Modules:
  0.0 55.7 jit_solution(2938776683464168286)
XLA Ops:
  0.0 55.0 %shard_map.163 = bf16[32,2048]{1,0:T(8,128)(2,1)S(1)} custom-call(bf16[1,2048]{1,0:T(2,128)(2,1)} %condition_in.1, bf16[16,128]{1,0:T(8,128)(2,1)} %bitcast.11, bf16[16,128]{1,0:T(8,128)(2,1)} %bitcast.12, bf16[4,128]{1,0:T(4,128)(2,1)} %bitcast.13, bf16[3,512]{1,0:T(4,128)(2,1)} %conv_x_in.1, bf16[3,128]{1,0:T(4,128)(2,1)} %conv_b_in.1, ...), custom_call_target="tpu_custom_call" | custom-call | tf_op jit(solution)/shard_map/pallas_call | solution.py:883
  55.0 0.7 %copy.19 = bf16[1,32,2048]{2,1,0:T(8,128)(2,1)} copy(bf16[1,32,2048]{2,1,0:T(8,128)(2,1)S(1)} %bitcast.7) | data formatting | bytes 262144

commit v7 on v6

--- a/solution.py
+++ b/solution.py
@@ -185,6 +185,7 @@
     gate_x,
     edge_send,
     edge_recv,
+    line_edge,
     misc,
     hidden,
     feats,
@@ -213,6 +214,7 @@
     edge_got,
     tot_sems,
     last_sems,
+    line_sems,
 ):
     nz, ny, nx, model = dims
     width = model // nx
@@ -259,7 +261,7 @@
     peers += [{"dp": 1 - core}]
     for k in range(nx):
         peers += [dict(above, tp=k), dict(below, tp=k)]
-    z_up, z_down = lax.rem(z + 1, nz), lax.rem(z + nz - 1, nz)
+    z_down = lax.rem(z + nz - 1, nz)
     for peer in peers:
         pl.semaphore_signal(barrier, inc=1, device_id=peer, device_id_type=MESH)
 
@@ -392,31 +394,30 @@
             )
 
         each = [copy(edge_send.at[slot], edge_recv.at[slot], peer) for peer in to]
-        return each, None if bulk is None else copy(bulk, bulk, to[0])
+        return each, copy(bulk, bulk, to[0])
 
     lat_bulk = edge_send.at[pl.ds(0, nx)]
     edges = (
         (x == nx - 1, edge(0, [dict(above, tp=k) for k in range(nx)], lat_bulk)),
         (x == 0, edge(1, [dict(below, tp=k) for k in range(nx)], lat_bulk)),
+        (y == ny - 1, edge(2, [above], edge_send.at[2])),
+        (y == 0, edge(3, [below], edge_send.at[3])),
     )
-    ctx_edges = [
-        edge(2, [{"sp_0": z_up}], None)[0][0],
-        edge(3, [{"sp_0": z_down}], None)[0][0],
-    ]
     own_latent.wait()
+    loads[9].wait()
     for slot, (owner, (each, _)) in enumerate(edges):
 
         @pl.when(owner)
         def _(slot=slot, each=each):
-            held = lat[x].astype(F32)
-            at = 0 if slot == 1 else own_rows - 1
+            held = (lat[x] if slot < 2 else ctx[y]).astype(F32)
+            at = 0 if slot % 2 == 1 else held.shape[0] - 1
             edge_send[slot] = held[at : at + 1, :]
             for c in each:
                 c.start()
 
     gates[0].start()
     small[2:7, :] = jnp.zeros((5, small.shape[1]), F32)
-    for c in loads[3:]:
+    for c in loads[3:9]:
         c.wait()
     unpack(2, gain)
     unpack(3, out_gain)
@@ -429,6 +430,31 @@
         for h in range(HEADS):
             rates = jnp.where(lane == way * HEADS + h, rate[way : way + 1, h : h + 1], rates)
 
+    line = []
+    for slot, owner in ((0, y == 0), (1, y == ny - 1)):
+
+        def line_copy(origin, target, k, slot=slot):
+            return pltpu.make_async_remote_copy(
+                src_ref=origin,
+                dst_ref=target,
+                send_sem=line_sems.at[slot, 0],
+                recv_sem=line_sems.at[slot, 1],
+                device_id={"sp_1": lax.rem(y + k, ny)},
+                device_id_type=MESH,
+            )
+
+        origin, target = edge_recv.at[2 + slot], line_edge.at[slot]
+        each = [line_copy(origin, target, k) for k in range(1, ny)]
+        line_bulk = line_edge.at[pl.ds(0, ny - 1)]
+        line.append((owner, each[0], line_copy(line_bulk, line_bulk, 1)))
+
+        @pl.when(owner)
+        def _(slot=slot, each=each):
+            edges[2 + slot][1][0][0].wait_recv()
+            line_edge[slot] = edge_recv[2 + slot]
+            for c in each:
+                c.start()
+
     mods[0].arrived()
     mod_z[z] = summed(mod_y, ny)
     mods[1].start()
@@ -440,20 +466,19 @@
     mod_x[x] = summed(mod_z, nz)
     mods[2].start()
 
-    ctx_copies.arrived()
-    edge_send[2] = ctx[ny - 1].astype(F32)[CTX_ROWS - 1 : CTX_ROWS, :]
-    edge_send[3] = ctx[0].astype(F32)[0:1, :]
-    for c in ctx_edges:
-        c.start()
-    ctx_scales = [inverse(ctx[j].astype(F32)) for j in range(ny)]
     lat_copies.arrived()
     scales = [inverse(lat[t].astype(F32)) for t in range(nx)]
+    ctx_copies.arrived()
+    ctx_scales = [inverse(ctx[j].astype(F32)) for j in range(ny)]
     misc[...] = jnp.zeros_like(misc)
-    for c in (edges[0][1][0][0], edges[1][1][0][0], *ctx_edges):
+    for c in (edges[0][1][0][0], edges[1][1][0][0]):
         c.wait_recv()
+    for owner, c, _ in line:
+        pl.when(jnp.logical_not(owner))(c.wait_recv)
     has = (place > 0, place < count - 1, z > 0, z < nz - 1)
     for slot in range(4):
-        misc[slot : slot + 1, :] = jnp.where(has[slot], edge_recv[slot], 0.0)
+        edge_row = edge_recv[slot] if slot < 2 else line_edge[slot - 2]
+        misc[slot : slot + 1, :] = jnp.where(has[slot], edge_row, 0.0)
     misc_scale = inverse(misc[...])
     row16 = rows_of((16, 1))
     kept = jnp.zeros((16, 1), jnp.bool_)
@@ -773,7 +798,9 @@
             ).start()
         )
     parts[x] = part_send[x]
-    for e in bulk_swaps + ctx_edges:
+    for owner, _, whole in line:
+        pl.when(owner)(whole.wait_send)
+    for e in bulk_swaps:
         e.wait_send()
     pl.when(jnp.logical_not(is_last))(to_last.wait_send)
     gates[2].arrived()
@@ -851,6 +878,7 @@
         pltpu.VMEM((nx, 1, 1, width), F32),
         pltpu.VMEM((4, 1, model), F32),
         pltpu.VMEM((4, 1, model), F32),
+        pltpu.VMEM((ny, 1, model), F32),
         pltpu.VMEM((16, model), F32),
         pltpu.VMEM((total_rows, model), BF16),
         pltpu.VMEM((total_rows, COLS), F32),
@@ -879,6 +907,7 @@
         dma((4,)),
         dma((4, 2)),
         dma((2,)),
+        dma((2, 2)),
     ]
     update = pl.pallas_call(
         functools.partial(mixer, (nz, ny, nx, model)),

time: 55.8 us -> 59.4 us (1.065)
  the two profiles are of different devices: /device:TPU:2 before, /device:TPU:6 now
where the time goes in v7:
time: 59.4 us; the launch traced here: 59.3 us
  Pallas kernels  58.6 us (99%)
  local copies, waits for them, and re-layouts  0.66 us (1%)
    pallas_call x1, Pallas kernels, shards(): pl.pallas_call(functools.partial(mixer, (nz, ny, nx, model)), out_shape=p...  58.6 us

profile of v7, /device:TPU:6, one launch (start us, length us, event | category | flops | bytes accessed | tf_op | source)
XLA Modules:
  0.0 59.3 jit_solution(2070316871890490467)
XLA Ops:
  0.0 58.6 %shard_map.163 = bf16[32,2048]{1,0:T(8,128)(2,1)S(1)} custom-call(bf16[1,2048]{1,0:T(2,128)(2,1)} %condition_in.1, bf16[16,128]{1,0:T(8,128)(2,1)} %bitcast.11, bf16[16,128]{1,0:T(8,128)(2,1)} %bitcast.12, bf16[4,128]{1,0:T(4,128)(2,1)} %bitcast.13, bf16[3,512]{1,0:T(4,128)(2,1)} %conv_x_in.1, bf16[3,128]{1,0:T(4,128)(2,1)} %conv_b_in.1, ...), custom_call_target="tpu_custom_call" | custom-call | tf_op jit(solution)/shard_map/pallas_call | solution.py:912
  58.6 0.7 %copy.19 = bf16[1,32,2048]{2,1,0:T(8,128)(2,1)} copy(bf16[1,32,2048]{2,1,0:T(8,128)(2,1)S(1)} %bitcast.7) | data formatting | bytes 262144

commit v8 on v7

--- a/solution.py
+++ b/solution.py
@@ -349,6 +349,40 @@
         return total
 
     mods[0].start()
+
+    def edge(slot, to, bulk):
+        def copy(origin, target, peer):
+            return pltpu.make_async_remote_copy(
+                src_ref=origin,
+                dst_ref=target,
+                send_sem=edge_sems.at[slot],
+                recv_sem=edge_got.at[slot],
+                device_id=peer,
+                device_id_type=MESH,
+            )
+
+        each = [copy(edge_send.at[slot], edge_recv.at[slot], peer) for peer in to]
+        return each, copy(bulk, bulk, to[0])
+
+    lat_bulk = edge_send.at[pl.ds(0, nx)]
+    edges = (
+        (x == nx - 1, edge(0, [dict(above, tp=k) for k in range(nx)], lat_bulk)),
+        (x == 0, edge(1, [dict(below, tp=k) for k in range(nx)], lat_bulk)),
+        (y == ny - 1, edge(2, [above], edge_send.at[2])),
+        (y == 0, edge(3, [below], edge_send.at[3])),
+    )
+    own_latent.wait()
+    loads[9].wait()
+    for slot, (owner, (each, _)) in enumerate(edges):
+
+        @pl.when(owner)
+        def _(slot=slot, each=each):
+            held = (lat[x] if slot < 2 else ctx[y]).astype(F32)
+            at = 0 if slot % 2 == 1 else held.shape[0] - 1
+            edge_send[slot] = held[at : at + 1, :]
+            for c in each:
+                c.start()
+
     ctx_copies = along(
         "sp_1", ny, y, lambda peer: context, ctx.at[y], ctx.at[pl.ds(0, ny - 1)]
     ).start()
@@ -382,39 +416,6 @@
         c.start()
         d.start()
 
-    def edge(slot, to, bulk):
-        def copy(origin, target, peer):
-            return pltpu.make_async_remote_copy(
-                src_ref=origin,
-                dst_ref=target,
-                send_sem=edge_sems.at[slot],
-                recv_sem=edge_got.at[slot],
-                device_id=peer,
-                device_id_type=MESH,
-            )
-
-        each = [copy(edge_send.at[slot], edge_recv.at[slot], peer) for peer in to]
-        return each, copy(bulk, bulk, to[0])
-
-    lat_bulk = edge_send.at[pl.ds(0, nx)]
-    edges = (
-        (x == nx - 1, edge(0, [dict(above, tp=k) for k in range(nx)], lat_bulk)),
-        (x == 0, edge(1, [dict(below, tp=k) for k in range(nx)], lat_bulk)),
-        (y == ny - 1, edge(2, [above], edge_send.at[2])),
-        (y == 0, edge(3, [below], edge_send.at[3])),
-    )
-    own_latent.wait()
-    loads[9].wait()
-    for slot, (owner, (each, _)) in enumerate(edges):
-
-        @pl.when(owner)
-        def _(slot=slot, each=each):
-            held = (lat[x] if slot < 2 else ctx[y]).astype(F32)
-            at = 0 if slot % 2 == 1 else held.shape[0] - 1
-            edge_send[slot] = held[at : at + 1, :]
-            for c in each:
-                c.start()
-
     gates[0].start()
     small[2:7, :] = jnp.zeros((5, small.shape[1]), F32)
     for c in loads[3:9]:
@@ -430,6 +431,10 @@
         for h in range(HEADS):
             rates = jnp.where(lane == way * HEADS + h, rate[way : way + 1, h : h + 1], rates)
 
+    mods[0].arrived()
+    mod_z[z] = summed(mod_y, ny)
+    mods[1].start()
+
     line = []
     for slot, owner in ((0, y == 0), (1, y == ny - 1)):
 
@@ -455,9 +460,6 @@
             for c in each:
                 c.start()
 
-    mods[0].arrived()
-    mod_z[z] = summed(mod_y, ny)
-    mods[1].start()
 
     def inverse(v):
         return lax.rsqrt(jnp.mean(v * v, axis=1, keepdims=True) + EPSILON)

time: 59.4 us -> 54.9 us (0.924)
  Pallas kernels: 58.6 us -> 53.8 us
    pallas_call x1, Pallas kernels: 58.6 us -> 53.8 us  [shards(): pl.pallas_call(functools.partial(mixer, (nz, ny, nx, model)), out_shape=p...]
where the time goes in v8:
time: 54.9 us; the launch traced here: 54.5 us
  Pallas kernels  53.8 us (98%)
  local copies, waits for them, and re-layouts  0.66 us (1%)
    pallas_call x1, Pallas kernels, shards(): pl.pallas_call(functools.partial(mixer, (nz, ny, nx, model)), out_shape=p...  53.8 us

profile of v8, /device:TPU:6, one launch (start us, length us, event | category | flops | bytes accessed | tf_op | source)
XLA Modules:
  0.0 54.5 jit_solution(928551794769335237)
XLA Ops:
  0.0 53.8 %shard_map.163 = bf16[32,2048]{1,0:T(8,128)(2,1)S(1)} custom-call(bf16[1,2048]{1,0:T(2,128)(2,1)} %condition_in.1, bf16[16,128]{1,0:T(8,128)(2,1)} %bitcast.11, bf16[16,128]{1,0:T(8,128)(2,1)} %bitcast.12, bf16[4,128]{1,0:T(4,128)(2,1)} %bitcast.13, bf16[3,512]{1,0:T(4,128)(2,1)} %conv_x_in.1, bf16[3,128]{1,0:T(4,128)(2,1)} %conv_b_in.1, ...), custom_call_target="tpu_custom_call" | custom-call | tf_op jit(solution)/shard_map/pallas_call | solution.py:914
  53.8 0.7 %copy.19 = bf16[1,32,2048]{2,1,0:T(8,128)(2,1)} copy(bf16[1,32,2048]{2,1,0:T(8,128)(2,1)S(1)} %bitcast.7) | data formatting | bytes 262144
